TPU v7x, 512 devices: a whole 4x8x8 slice. The times are simulated.
512 devices in a mesh: sp: 32 (over z, x), tp: 16 (over y, core).
Axes of the slice: x: 4, y: 8, z: 8, core: 2. Of those that a mesh axis runs over, the one named last changes fastest.
Arguments:
- expert_input: bfloat16 [4096, 2048], P('sp'), may hold values from -6 to 6
- cotangent: bfloat16 [4096, 2048], P('sp'), may hold values from -6 to 6
- routes: int32 [4096, 2], P('sp'), may hold values from 0 to 15, all different within a row; in each aligned block of 128 rows (0 to 127, 128 to 255, ...) at most 20 rows name the same one
- route_weight: float32 [4096, 2], P('sp'), may hold values from 0.1 to 1
- gate_weight: bfloat16 [32, 2048, 2048], P('sp', None, 'tp'), may hold values from -0.125 to 0.125
- up_weight: bfloat16 [32, 2048, 2048], P('sp', None, 'tp'), may hold values from -0.125 to 0.125
- down_weight: bfloat16 [32, 2048, 2048], P('sp', 'tp'), may hold values from -0.09375 to 0.09375
- out_weight: bfloat16 [2048, 2048], P(None, 'tp'), may hold values from -0.125 to 0.125
- queries: bfloat16 [4096, 16, 64], P('sp', 'tp'), may hold values from -6 to 6
- key_vectors: bfloat16 [4096, 16, 64], P('sp', 'tp'), may hold values from -6 to 6
- value_rows: bfloat16 [4096, 16, 128], P('sp', 'tp'), may hold values from -6 to 6
- log_decay: float32 [4096, 16, 64], P('sp', 'tp'), may hold values from -2 to 0
- start_state: float32 [32, 16, 64, 128], P('sp', 'tp'), may hold values from -24 to 24
Outputs:
- gate_grad: bfloat16 [32, 2048, 2048], P('sp', None, 'tp')
- up_grad: bfloat16 [32, 2048, 2048], P('sp', None, 'tp')
- down_grad: bfloat16 [32, 2048, 2048], P('sp', 'tp')
- out_grad: float32 [2048, 2048], P('sp', 'tp')
- query_grad: bfloat16 [4096, 16, 64], P('sp', 'tp')
- key_grad: bfloat16 [4096, 16, 64], P('sp', 'tp')
- value_grad: bfloat16 [4096, 16, 128], P('sp', 'tp')
- decay_grad: float32 [4096, 16, 64], P('sp', 'tp')
Inputs may be any that keep to these rules, and one draw needn't show every extreme that they name: `routes`: in each aligned block of 128 rows, no number is named by more than 20 rows, and in some blocks one number is named by exactly 20 rows.
All inputs are finite; a program needn't handle non-finite values.
Results may differ from a plain program's by a relative error of at most 0.02.
Values may be sent and summed in bfloat16 or wider, within the bound.
No kernel may reach another device: no remote copies, remote signals or barrier semaphores. Data moves between devices by JAX's collectives and lax.ppermute only.
A program may use at most 64 MiB of HBM per device.

v0:
```python
import jax
import jax.numpy as jnp
from jax import lax
from jax.sharding import Mesh
from jax.sharding import PartitionSpec as P

BLOCK = 32
SP = ("sp_0", "sp_1")


def sent_together(arrays, axis, split_dim, concat_dim, along):
    ends, at = ([], 0)
    for a in arrays[:-1]:
        at += a.shape[along]
        ends.append(at)
    both = jnp.concatenate(arrays, axis=along)
    return tuple(
        jnp.split(
            lax.all_to_all(both, axis, split_axis=split_dim, concat_axis=concat_dim, tiled=True),
            ends,
            axis=along,
        )
    )


def side_by_side(arrays, axis, dim, along):
    ends, at = ([], 0)
    for a in arrays[:-1]:
        at += a.shape[along]
        ends.append(at)
    both = jnp.concatenate(arrays, axis=along)
    return tuple(jnp.split(lax.all_gather(both, axis, axis=dim, tiled=True), ends, axis=along))


def split_up(shard, dim, devices):
    dims = shard.shape
    tiles = shard.reshape(*dims[:dim], devices, dims[dim] // devices, *dims[dim + 1 :])
    return jnp.moveaxis(tiles, dim, 0)


def sent_and_summed(shard, axis, dim):
    devices = lax.axis_size(axis)
    tiles = lax.all_to_all(split_up(shard, dim, devices), axis, 0, 0, tiled=True)
    return jnp.sum(tiles.astype(jnp.float32), axis=0)


def from_everyone(shard, axis):
    devices = lax.axis_size(axis)
    return lax.all_to_all(
        jnp.broadcast_to(shard[None], (devices, *shard.shape)), axis, 0, 0, tiled=True
    )


def laid_out(tiles, dim):
    dims = list(tiles.shape[1:])
    dims[dim] *= tiles.shape[0]
    return jnp.moveaxis(tiles, 0, dim).reshape(dims)


def gathered_copies(shard, axis, dim):
    tiles = from_everyone(shard, axis)
    return laid_out(tiles, dim)


def neutral_like(shard, identity):
    return jax.tree.map(
        lambda part, zero: jnp.zeros_like(part) + jnp.asarray(zero, part.dtype), shard, identity
    )


def entering(shard, axes, combine, identity):
    before = start = neutral_like(shard, identity)
    so_far = shard
    for axis in reversed(axes):
        devices, place = (lax.axis_size(axis), lax.axis_index(axis))
        pieces = jax.tree.map(
            lambda part, kind: lax.all_gather(part.astype(kind), axis),
            so_far,
            (jnp.bfloat16, jnp.bfloat16),
        )
        inside, so_far = (start, start)
        for k in reversed(range(devices)):
            passed = k > place
            so_far = combine(
                so_far, jax.tree.map(lambda part, own: part[k].astype(own.dtype), pieces, shard)
            )
            inside = jax.tree.map(lambda new, old: jnp.where(passed, new, old), so_far, inside)
        before = combine(inside, before)
    return before


def slot_table(routes_local, experts, capacity):
    flat_ids = routes_local.reshape(-1)
    onehot = (flat_ids[:, None] == jnp.arange(experts, dtype=jnp.int32)[None, :]).astype(jnp.int32)
    running = jnp.cumsum(onehot, axis=0)
    slot_rank = jnp.sum((running - 1) * onehot, axis=1)
    destination = flat_ids * capacity + slot_rank
    source = (
        jnp.full((experts * capacity,), -1, jnp.int32)
        .at[destination]
        .set(jnp.arange(flat_ids.shape[0], dtype=jnp.int32))
    )
    return (destination, source)


def input_slots(features, token_rows, present, experts, capacity):
    taken_rows = jnp.take(features, token_rows, axis=0)
    taken_rows = jnp.where(present, taken_rows, jnp.zeros_like(taken_rows))
    return jnp.repeat(taken_rows.reshape(experts, capacity, features.shape[1]), 2, axis=0)


def grad_slots(features, token_rows, present, picked_weight, experts, capacity):
    taken_rows = jnp.take(features, token_rows, axis=0).astype(jnp.float32) * picked_weight[:, None]
    taken_rows = jnp.where(present, taken_rows, 0.0).astype(jnp.bfloat16)
    return jnp.repeat(taken_rows.reshape(experts, capacity, features.shape[1]), 2, axis=0)


def collect(returned, residual, destination, experts, capacity, topk_count):
    feature_width = returned.shape[2]
    paired = returned.astype(jnp.float32).reshape(experts, 2, capacity, feature_width)
    merged = (paired[:, 0] + paired[:, 1]).reshape(experts * capacity, feature_width)
    per_pair = jnp.take(merged, destination, axis=0).reshape(-1, topk_count, feature_width)
    return (residual.astype(jnp.float32) + jnp.sum(per_pair, axis=1)).astype(jnp.bfloat16)


def to_blocks(stacked):
    tokens_here, heads_here, feature_width = stacked.shape
    return (
        stacked.astype(jnp.float32)
        .reshape(tokens_here // BLOCK, BLOCK, heads_here, feature_width)
        .transpose(0, 2, 1, 3)
    )


def from_blocks(stacked):
    blocks_here, heads_here, block_len, feature_width = stacked.shape
    return stacked.transpose(0, 2, 1, 3).reshape(blocks_here * block_len, heads_here, feature_width)


def block_decay(decay_block):
    cumulative_decay = jnp.cumsum(decay_block, axis=1)
    causal = jnp.tril(jnp.ones((BLOCK, BLOCK), dtype=bool))
    differ = cumulative_decay[:, :, None, :] - cumulative_decay[:, None, :, :]
    decay_table = jnp.exp(jnp.where(causal[None, :, :, None], differ, -jnp.inf))
    return (cumulative_decay, causal, decay_table)


def forward_block(current_state, inputs):
    query_tile, key_tile, value_tile, g_block, output_grad_block = inputs
    cumulative_decay, causal, decay_table = block_decay(g_block)
    scores = jnp.sum(query_tile[:, :, None, :] * key_tile[:, None, :, :] * decay_table, axis=-1)
    expanded_decay = jnp.exp(cumulative_decay)
    mixed_block = jnp.einsum(
        "wzg,wgb->wzb", query_tile * expanded_decay, current_state
    ) + jnp.einsum("hts,hsv->htv", scores, value_tile)
    inner = jnp.where(causal[None], jnp.einsum("htv,hsv->hts", output_grad_block, value_tile), 0.0)
    query_part = expanded_decay * jnp.einsum(
        "xlf,xqf->xlq", output_grad_block, current_state
    ) + jnp.sum(inner[:, :, :, None] * key_tile[:, None, :, :] * decay_table, axis=2)
    remaining_decay = jnp.exp(cumulative_decay[:, -1:, :] - cumulative_decay)
    following_state = jnp.exp(cumulative_decay[:, -1, :])[:, :, None] * current_state + jnp.einsum(
        "apo,apg->aog", key_tile * remaining_decay, value_tile
    )
    return (following_state, (mixed_block, query_part))


def backward_block(carried_state, inputs):
    query_tile, key_tile, value_tile, g_block, output_grad_block = inputs
    cumulative_decay, causal, decay_table = block_decay(g_block)
    scores = jnp.sum(query_tile[:, :, None, :] * key_tile[:, None, :, :] * decay_table, axis=-1)
    inner = jnp.where(causal[None], jnp.einsum("htv,hsv->hts", output_grad_block, value_tile), 0.0)
    remaining_decay = jnp.exp(cumulative_decay[:, -1:, :] - cumulative_decay)
    key_part = jnp.sum(
        inner[:, :, :, None] * query_tile[:, :, None, :] * decay_table, axis=1
    ) + remaining_decay * jnp.einsum("xgy,xcy->xcg", carried_state, value_tile)
    value_part = jnp.einsum("hts,htv->hsv", scores, output_grad_block) + jnp.einsum(
        "wby,wyg->wbg", key_tile * remaining_decay, carried_state
    )
    carried_next = jnp.exp(cumulative_decay[:, -1, :])[:, :, None] * carried_state + jnp.einsum(
        "aye,ayz->aez", query_tile * jnp.exp(cumulative_decay), output_grad_block
    )
    return (carried_next, (key_part, value_part))


def compose(earlier, later):
    return (later[0] * earlier[0], later[0][..., None] * earlier[1] + later[1])


def on_device(
    expert_input,
    cotangent,
    routes,
    route_weight,
    gate_weight,
    up_weight,
    down_weight,
    out_weight,
    queries,
    key_vectors,
    value_rows,
    log_decay,
    start_state,
):
    tok_dev, model_width = expert_input.shape
    topk_count = routes.shape[1]
    sp_devices = lax.axis_size(SP)
    tp_devices = lax.axis_size("tp")
    experts = sp_devices // 2
    capacity = 5 * tok_dev * topk_count // (4 * experts)
    feature_slice = model_width // tp_devices
    destination, source = slot_table(routes, experts, capacity)
    present = (source >= 0)[:, None]
    picked = jnp.maximum(source, 0)
    token_rows = picked // topk_count
    picked_weight = jnp.take(route_weight.reshape(-1), picked)
    first_col = lax.axis_index("tp") * feature_slice
    input_part = lax.dynamic_slice_in_dim(expert_input, first_col, feature_slice, 1)
    grad_part = lax.dynamic_slice_in_dim(cotangent, first_col, feature_slice, 1)
    sent_input = input_slots(input_part, token_rows, present, experts, capacity)
    sent_grad = grad_slots(grad_part, token_rows, present, picked_weight, experts, capacity)
    piece_input, piece_grad = sent_together((sent_input, sent_grad), SP, 0, 0, 1)
    got_input, got_grad = side_by_side((piece_input, piece_grad), "tp", 2, 0)
    row_count = sp_devices * capacity
    rows_in = got_input.reshape(row_count, model_width)
    rows_grad = got_grad.reshape(row_count, model_width)
    w_gate = gate_weight[0]
    w_up = up_weight[0]
    w_down = down_weight[0]
    pre_gate = jnp.dot(rows_in, w_gate, preferred_element_type=jnp.float32)
    pre_up = jnp.dot(rows_in, w_up, preferred_element_type=jnp.float32)
    sigmoid_gate = jax.nn.sigmoid(pre_gate)
    activated = pre_gate * sigmoid_gate
    hidden = (activated * pre_up).astype(jnp.bfloat16)
    down_sum = lax.dot_general(
        hidden, rows_grad, (((0,), (0,)), ((), ())), preferred_element_type=jnp.float32
    )
    hidden_grad = lax.dot_general(
        rows_grad, w_down, (((1,), (1,)), ((), ())), preferred_element_type=jnp.float32
    )
    gate_delta = (
        hidden_grad * pre_up * sigmoid_gate * (1.0 + pre_gate * (1.0 - sigmoid_gate))
    ).astype(jnp.bfloat16)
    up_delta = (hidden_grad * activated).astype(jnp.bfloat16)
    gate_sum = lax.dot_general(
        rows_in, gate_delta, (((0,), (0,)), ((), ())), preferred_element_type=jnp.float32
    )
    up_sum = lax.dot_general(
        rows_in, up_delta, (((0,), (0,)), ((), ())), preferred_element_type=jnp.float32
    )
    partial_input = lax.dot_general(
        gate_delta, w_gate, (((1,), (1,)), ((), ())), preferred_element_type=jnp.float32
    ) + lax.dot_general(
        up_delta, w_up, (((1,), (1,)), ((), ())), preferred_element_type=jnp.float32
    )
    scattered = sent_and_summed(
        partial_input.reshape(sp_devices, capacity, model_width).astype(jnp.bfloat16), "tp", 2
    )
    returned = lax.all_to_all(
        scattered.astype(jnp.bfloat16), SP, split_axis=0, concat_axis=0, tiled=True
    )
    first_col = lax.axis_index("tp") * feature_slice
    cotangent_part = lax.dynamic_slice_in_dim(cotangent, first_col, feature_slice, 1)
    slice_grad = collect(returned, cotangent_part, destination, experts, capacity, topk_count)
    total_grad = gathered_copies(slice_grad, "tp", 1)
    head_grad = jnp.dot(total_grad, out_weight, preferred_element_type=jnp.float32).astype(
        jnp.bfloat16
    )
    heads_local = queries.shape[1]
    key_width = queries.shape[2]
    value_width = value_rows.shape[2]
    query_scale = key_width ** (-0.5)
    dout_rows = head_grad.reshape(tok_dev, heads_local, value_width)
    query_rows_wide = queries.astype(jnp.float32)
    keys_f = key_vectors.astype(jnp.float32)
    output_grad_wide = dout_rows.astype(jnp.float32)
    segment_cumulative = jnp.cumsum(log_decay, axis=0)
    total_decay = jnp.exp(segment_cumulative[-1])
    local_carry = jnp.einsum(
        "mxj,mxw->xjw",
        query_rows_wide * query_scale * jnp.exp(segment_cumulative),
        output_grad_wide,
    )
    identity = (jnp.ones_like(total_decay), jnp.zeros_like(local_carry))
    _, incoming = entering((total_decay, local_carry), SP, compose, identity)
    blocked = (
        to_blocks(queries) * query_scale,
        to_blocks(key_vectors),
        to_blocks(value_rows),
        to_blocks(log_decay),
        to_blocks(dout_rows),
    )
    state_end, (mixed_blocks, query_blocks) = lax.scan(forward_block, start_state[0], blocked)
    _, (key_blocks, value_blocks) = lax.scan(backward_block, incoming, blocked, reverse=True)
    query_raw = from_blocks(query_blocks) * query_scale
    key_raw = from_blocks(key_blocks)
    value_raw = from_blocks(value_blocks)
    mixed = (
        from_blocks(mixed_blocks).astype(jnp.bfloat16).reshape(tok_dev, heads_local * value_width)
    )
    local_terms = query_rows_wide * query_raw - keys_f * key_raw
    position = jnp.arange(tok_dev)
    later_mask = (position[None, :] >= position[:, None]).astype(jnp.float32)
    reversed_sum = jnp.dot(later_mask, local_terms.reshape(tok_dev, -1)).reshape(local_terms.shape)
    cross_term = jnp.sum(state_end * incoming, axis=-1)
    decay_grad = reversed_sum + cross_term[None]
    out_grad = sent_and_summed(
        lax.dot_general(
            total_grad, mixed, (((0,), (0,)), ((), ())), preferred_element_type=jnp.float32
        ).astype(jnp.bfloat16),
        SP,
        0,
    )
    return (
        gate_sum.astype(jnp.bfloat16)[None],
        up_sum.astype(jnp.bfloat16)[None],
        down_sum.astype(jnp.bfloat16)[None],
        out_grad,
        query_raw.astype(jnp.bfloat16),
        key_raw.astype(jnp.bfloat16),
        value_raw.astype(jnp.bfloat16),
        decay_grad,
    )


def solution(mesh):
    torus = Mesh(mesh.devices.reshape(8, 4, mesh.shape["tp"]), ("sp_0", "sp_1", "tp"))
    in_specs = (
        P(SP, None),
        P(SP, None),
        P(SP, None),
        P(SP, None),
        P(SP, None, "tp"),
        P(SP, None, "tp"),
        P(SP, "tp", None),
        P(None, "tp"),
        P(SP, "tp", None),
        P(SP, "tp", None),
        P(SP, "tp", None),
        P(SP, "tp", None),
        P(SP, "tp", None, None),
    )
    out_specs = (
        P(SP, None, "tp"),
        P(SP, None, "tp"),
        P(SP, "tp", None),
        P(SP, "tp"),
        P(SP, "tp", None),
        P(SP, "tp", None),
        P(SP, "tp", None),
        P(SP, "tp", None),
    )
    return jax.shard_map(
        on_device, mesh=torus, in_specs=in_specs, out_specs=out_specs, check_vma=False
    )
```

profile of v0, /device:TPU:2, one launch (start us, length us, event | category | flops | bytes accessed | tf_op | source)
XLA Modules:
  0.0 315.1 jit_solution(7692559562779848123)
XLA Ops:
  8.0 0.8 copy.120
  10.8 1.4 scatter_custom_fusion
  12.2 0.8 copy.123
  13.2 2.5 gather_fusion
  15.7 0.8 constant_dynamic-slice_fusion
  16.4 1.4 gather_fusion.3
  18.1 1.4 gather_fusion.2
  19.8 25.9 %all_to_all.25 = bf16[32,40,128]{2,1,0:T(8,128)(2,1)S(1)} all-to-all(bf16[32,40,128]{2,1,0:T(8,128)(2,1)S(1)} %pad_maximum_fusion.1), channel_id=1, replica_groups=mesh['sp_0'=8,'sp_1'=4,'tp'=16] {'sp_0','sp_1'}, dimensions={0} | all-to-all | bytes 655360 | tf_op jit(solution)/shard_map/all_to_all | solution.py:19
  45.8 0.8 pad_maximum_fusion
  46.6 56.3 %all-gather.3.cloned.1.call-done = bf16[64,20,2048]{2,1,0:T(8,128)(2,1)} async-done(((bf16[64,20,128]{2,1,0:T(8,128)(2,1)}), bf16[64,20,2048]{2,1,0:T(8,128)(2,1)}) %all-gather.3.cloned.1.call-update) | async-done | bytes 5242896 | tf_op jit(solution)/shard_map/all_gather | solution.py:32
  102.9 6.6 %fusion.139 = (bf16[32,20,2048]{2,1,0:T(8,128)(2,1)}, bf16[32,20,2048]{2,1,0:T(8,128)(2,1)}) fusion(bf16[64,20,2048]{2,1,0:T(8,128)(2,1)} %all-gather.3.cloned.1.call-done), kind=kLoop, calls=%fused_computation.255 | loop fusion | bytes 10485760 | tf_op jit(solution)/shard_map/split | solution.py:32
  109.6 3.6 %reshape.1453 = bf16[640,2048]{1,0:T(8,128)(2,1)S(1)} reshape(bf16[32,20,2048]{2,1,0:T(8,128)(2,1)} %get-tuple-element.448) | data formatting | bytes 5242880 | tf_op jit(solution)/shard_map/reshape | solution.py:224
  113.2 0.8 fusion.77
  114.3 1.6 fusion.80
  115.8 5.2 %reshape.1454 = bf16[640,2048]{1,0:T(8,128)(2,1)} reshape(bf16[32,20,2048]{2,1,0:T(8,128)(2,1)} %get-tuple-element.447) | data formatting | bytes 5242880 | tf_op jit(solution)/shard_map/reshape | solution.py:225
  121.0 2.8 multiply_convert_fusion.1
  123.9 0.8 fusion.75
  125.0 0.8 fusion.73
  125.8 0.8 copy.145
  126.7 3.2 %copy.148 = bf16[32,20,16,128]{3,0,1,2:T(8,128)(2,1)} copy(bf16[32,20,16,128]{3,2,1,0:T(8,128)(2,1)S(1)} %bitcast.530) | data formatting | bytes 5242880 | tf_op jit(solution)/shard_map/convert_element_type | solution.py:256
  129.8 5.1 %all-to-all-start.1 = ((bf16[16,32,20,128]{3,1,2,0:T(8,128)(2,1)}), bf16[16,32,20,128]{3,1,2,0:T(8,128)(2,1)}, u32[]{:S(2)}, u32[]{:S(2)}) async-start(bf16[16,32,20,128]{3,1,2,0:T(8,128)(2,1)} %bitcast.529), calls=%async_computation.1 | async-start | bytes 5242880 | tf_op jit(solution)/shard_map/all_to_all | solution.py:43
  135.8 1.5 copy.133
  137.4 7.8 %all_gather.22 = bf16[4,1,64]{2,1,0:T(2,128)(2,1)S(1)} all-gather(bf16[1,1,64]{2,1,0:T(2,128)(2,1)S(1)} %fusion.129), channel_id=1, replica_groups=mesh['sp_0'=8,'sp_1'=4,'tp'=16] {'sp_1'}, dimensions={0}, use_global_device_ids=true | all-gather | bytes 640 | tf_op jit(solution)/shard_map/all_gather | solution.py:77
  145.3 17.2 %all_gather.23 = bf16[8,1,64]{2,1,0:T(2,128)(2,1)S(1)} all-gather(bf16[1,1,64]{2,1,0:T(2,128)(2,1)S(1)} %multiply_convert_fusion.4), channel_id=1, replica_groups=mesh['sp_0'=8,'sp_1'=4,'tp'=16] {'sp_0'}, dimensions={0}, use_global_device_ids=true | all-gather | bytes 1152 | tf_op jit(solution)/shard_map/all_gather | solution.py:77
  164.2 31.3 %all-to-all-done.1 = bf16[16,32,20,128]{3,1,2,0:T(8,128)(2,1)} async-done(((bf16[16,32,20,128]{3,1,2,0:T(8,128)(2,1)}), bf16[16,32,20,128]{3,1,2,0:T(8,128)(2,1)}, u32[]{:S(2)}, u32[]{:S(2)}) %all-to-all-start.1) | async-done | bytes 2621472 | tf_op jit(solution)/shard_map/all_to_all | solution.py:43
  195.6 2.1 reduce_sum.91
  198.4 10.6 %all-to-all-start.2 = ((bf16[32,20,128]{2,1,0:T(8,128)(2,1)}), bf16[32,20,128]{2,1,0:T(8,128)(2,1)}, u32[]{:S(2)}, u32[]{:S(2)}) async-start(bf16[32,20,128]{2,1,0:T(8,128)(2,1)} %copy.143), calls=%async_computation.2 | async-start | bytes 393216 | tf_op jit(solution)/shard_map/all_to_all | solution.py:258
  209.0 1.3 pad_clamp_fusion
  210.3 1.7 exponential_multiply_fusion
  211.9 6.6 %all-to-all-done.2 = bf16[32,20,128]{2,1,0:T(8,128)(2,1)} async-done(((bf16[32,20,128]{2,1,0:T(8,128)(2,1)}), bf16[32,20,128]{2,1,0:T(8,128)(2,1)}, u32[]{:S(2)}, u32[]{:S(2)}) %all-to-all-start.2) | async-done | bytes 163872 | tf_op jit(solution)/shard_map/all_to_all | solution.py:258
  218.5 0.9 copy.128
  220.5 0.9 add.317
  221.5 1.5 gather_fusion.1
  222.9 1.2 select_reduce_fusion
  224.2 0.9 broadcast_in_dim.189
  225.2 5.3 %all-to-all-start.3 = ((bf16[16,128,128]{1,2,0:T(8,128)(2,1)}), bf16[16,128,128]{1,2,0:T(8,128)(2,1)}, u32[]{:S(2)}, u32[]{:S(2)}) async-start(bf16[16,128,128]{1,2,0:T(8,128)(2,1)} %broadcast_in_dim.189), calls=%async_computation.3 | async-start | bytes 1048576 | tf_op jit(solution)/shard_map/all_to_all | solution.py:49
  231.1 2.6 fusion.70
  233.8 1.7 fusion.71
  235.8 1.4 fusion.72
  237.2 9.2 %all-to-all-done.3 = bf16[16,128,128]{1,2,0:T(8,128)(2,1)} async-done(((bf16[16,128,128]{1,2,0:T(8,128)(2,1)}), bf16[16,128,128]{1,2,0:T(8,128)(2,1)}, u32[]{:S(2)}, u32[]{:S(2)}) %all-to-all-start.3) | async-done | bytes 524320 | tf_op jit(solution)/shard_map/all_to_all | solution.py:49
  246.4 1.4 convolution_convert_fusion.4
  248.0 5.4 %while.32 = (s32[]{:T(128)}, f32[1,64,128]{2,1,0:T(8,128)S(1)}, bf16[4,1,32,128]{3,2,1,0:T(8,128)(2,1)S(1)}, f32[4,1,32,64]{3,2,1,0:T(8,128)S(1)}, f32[4,1,32,64...) while((s32[]{:T(128)}, f32[1,64,128]{2,1,0:T(8,128)S(1)}, ...), condition=%wide.region_10.12_spmd, body=%wide.region_6.11_spmd.sunk | while | flops 2715650 | bytes 460933 | solution.py:292
  253.4 2.1 convolution_convert_fusion
  255.5 5.6 %all-to-all-start.4 = ((bf16[32,64,128]{2,1,0:T(8,128)(2,1)}), bf16[32,64,128]{2,1,0:T(8,128)(2,1)S(1)}, u32[]{:S(2)}, u32[]{:S(2)}) async-start(bf16[32,64,128]{2,1,0:T(8,128)(2,1)} %bitcast.56), calls=%async_computation.4 | async-start | bytes 1048576 | tf_op jit(solution)/shard_map/all_to_all | solution.py:43
  261.3 12.5 %all-gather = bf16[256,128]{1,0:T(8,128)(2,1)S(1)} all-gather(bf16[64,128]{1,0:T(8,128)(2,1)S(1)} %fusion.150), channel_id=2, replica_groups=mesh['sp_0'=8,'sp_1'=4,'tp'=16] {'sp_1'}, dimensions={0}, use_global_device_ids=true | all-gather | bytes 81920 | tf_op jit(solution)/shard_map/all_gather | solution.py:77
  273.9 25.2 %all_gather.26 = bf16[8,1,64,128]{3,2,1,0:T(8,128)(2,1)S(1)} all-gather(bf16[1,1,64,128]{3,2,1,0:T(8,128)(2,1)S(1)} %fusion.93), channel_id=1, replica_groups=mesh['sp_0'=8,'sp_1'=4,'tp'=16] {'sp_0'}, dimensions={0}, use_global_device_ids=true | all-gather | bytes 147456 | tf_op jit(solution)/shard_map/all_gather | solution.py:77
  299.5 5.6 %while.33 = (s32[]{:T(128)}, f32[1,64,128]{2,1,0:T(8,128)S(1)}, f32[4,1,32,64]{3,2,1,0:T(8,128)S(1)}, bf16[4,1,32,128]{3,2,1,0:T(8,128)(2,1)S(1)}, f32[4,1,32,64...) while((s32[]{:T(128)}, f32[1,64,128]{2,1,0:T(8,128)S(1)}, ...), condition=%wide.region_17.19_spmd, body=%wide.region_13.18_spmd.sunk | while | flops 2717699 | bytes 461465 | solution.py:293
  306.7 0.8 fusion.74
  (233 shorter events, 23.3 us)
Async XLA Ops:
  7.2 106.0 %copy-start = (bf16[1,2048,128]{2,1,0:T(8,128)(2,1)S(1)}, bf16[1,2048,128]{2,1,0:T(8,128)(2,1)}, u32[]{:S(2)}) copy-start(bf16[1,2048,128]{2,1,0:T(8,128)(2,1)} %param.23) | copy-start | bytes 1572868
  7.2 95.8 %all-gather.3.cloned.1.call-start = ((), (), s32[]{:S(2)}) async-start(), calls=%async_computation.5 | async-start | bytes 6684672 | tf_op jit(solution)/shard_map/all_gather | solution.py:32
  10.2 0.6 copy-start.27
  113.2 1.0 copy-start.6
  114.3 6.8 %copy-start.3 = (f32[640,128]{1,0:T(8,128)}, f32[640,128]{1,0:T(8,128)S(1)}, u32[]{:S(2)}) copy-start(f32[640,128]{1,0:T(8,128)S(1)} %fusion.77) | copy-start | bytes 983044
  123.8 0.9 copy-start.9
  123.8 0.9 copy-start.10
  123.8 1.2 copy-start.7
  129.8 5.3 %copy-start.18 = (f32[128,1,64]{0,2,1:T(8,128)S(1)}, f32[128,1,64]{0,2,1:T(8,128)}, u32[]{:S(2)}) copy-start(f32[128,1,64]{0,2,1:T(8,128)} %param.30) | copy-start | bytes 98308
  129.8 5.6 %copy-start.22 = (s32[128,2]{0,1:T(2,128)S(1)}, s32[128,2]{0,1:T(2,128)}, u32[]{:S(2)}) copy-start(s32[128,2]{0,1:T(2,128)} %param.21) | copy-start | bytes 3076
  129.8 5.7 %copy-start.20 = (bf16[128,1,64]{0,2,1:T(8,128)(2,1)S(1)}, bf16[128,1,64]{0,2,1:T(8,128)(2,1)}, u32[]{:S(2)}) copy-start(bf16[128,1,64]{0,2,1:T(8,128)(2,1)} %param.28) | copy-start | bytes 49156
  129.8 65.7 %all-to-all-start.1 = ((bf16[16,32,20,128]{3,1,2,0:T(8,128)(2,1)}), bf16[16,32,20,128]{3,1,2,0:T(8,128)(2,1)}, u32[]{:S(2)}, u32[]{:S(2)}) async-start(bf16[16,32,20,128]{3,1,2,0:T(8,128)(2,1)} %bitcast.529), calls=%async_computation.1 | async-start | bytes 5242880 | tf_op jit(solution)/shard_map/all_to_all | solution.py:43
  135.7 73.3 %copy-start.12 = (bf16[128,1,64]{2,1,0:T(2,128)(2,1)}, bf16[128,1,64]{2,1,0:T(2,128)(2,1)S(1)}, u32[]{:S(2)}) copy-start(bf16[128,1,64]{2,1,0:T(2,128)(2,1)S(1)} %copy.132) | copy-start | bytes 49156
  137.4 26.8 %copy-start.17 = (f32[128,1,64]{2,1,0:T(1,128)}, f32[128,1,64]{2,1,0:T(1,128)S(1)}, u32[]{:S(2)}) copy-start(f32[128,1,64]{2,1,0:T(1,128)S(1)} %fusion.149) | copy-start | bytes 98308
  162.5 1.7 copy-start.21
  198.4 20.1 %all-to-all-start.2 = ((bf16[32,20,128]{2,1,0:T(8,128)(2,1)}), bf16[32,20,128]{2,1,0:T(8,128)(2,1)}, u32[]{:S(2)}, u32[]{:S(2)}) async-start(bf16[32,20,128]{2,1,0:T(8,128)(2,1)} %copy.143), calls=%async_computation.2 | async-start | bytes 393216 | tf_op jit(solution)/shard_map/all_to_all | solution.py:258
  225.2 21.3 %all-to-all-start.3 = ((bf16[16,128,128]{1,2,0:T(8,128)(2,1)}), bf16[16,128,128]{1,2,0:T(8,128)(2,1)}, u32[]{:S(2)}, u32[]{:S(2)}) async-start(bf16[16,128,128]{1,2,0:T(8,128)(2,1)} %broadcast_in_dim.189), calls=%async_computation.3 | async-start | bytes 1048576 | tf_op jit(solution)/shard_map/all_to_all | solution.py:49
  231.1 2.6 copy-start.11
  233.8 1.7 copy-start.1
  233.8 1.8 copy-start.4
  233.8 2.0 copy-start.5
  235.8 10.7 %copy-start.15 = (bf16[2048,128]{1,0:T(8,128)(2,1)S(1)}, bf16[2048,128]{1,0:T(8,128)(2,1)}, u32[]{:S(2)}) copy-start(bf16[2048,128]{1,0:T(8,128)(2,1)} %param.26) | copy-start | bytes 1572868
  235.8 12.1 %copy-start.2 = (f32[1,1,64,128]{3,2,1,0:T(8,128)S(1)}, f32[1,1,64,128]{3,2,1,0:T(8,128)}, u32[]{:S(2)}) copy-start(f32[1,1,64,128]{3,2,1,0:T(8,128)} %param.31) | copy-start | bytes 98308
  235.8 12.1 %copy-start.8 = (bf16[128,1,128]{2,0,1:T(8,128)(2,1)S(1)}, bf16[128,1,128]{2,0,1:T(8,128)(2,1)}, u32[]{:S(2)}) copy-start(bf16[128,1,128]{2,0,1:T(8,128)(2,1)} %param.29) | copy-start | bytes 98308
  247.9 13.2 %copy-start.16 = (f32[128,1,64]{2,1,0:T(1,128)S(1)}, f32[128,1,64]{2,1,0:T(1,128)}, u32[]{:S(2)}) copy-start(f32[128,1,64]{2,1,0:T(1,128)} %get-tuple-element.453) | copy-start | bytes 98308
  247.9 25.9 %copy-start.23 = (f32[64]{0:T(128)S(1)}, f32[64]{0:T(128)}, u32[]{:S(2)}) copy-start(f32[64]{0:T(128)} %get-tuple-element.463) | copy-start | bytes 772
  247.9 25.9 %copy-start.24 = (f32[64]{0:T(128)S(1)}, f32[64]{0:T(128)}, u32[]{:S(2)}) copy-start(f32[64]{0:T(128)} %get-tuple-element.464) | copy-start | bytes 772
  247.9 25.9 %copy-start.25 = (f32[64]{0:T(128)S(1)}, f32[64]{0:T(128)}, u32[]{:S(2)}) copy-start(f32[64]{0:T(128)} %get-tuple-element.465) | copy-start | bytes 772
  247.9 25.9 %copy-start.26 = (f32[64]{0:T(128)S(1)}, f32[64]{0:T(128)}, u32[]{:S(2)}) copy-start(f32[64]{0:T(128)} %get-tuple-element.466) | copy-start | bytes 772
  247.9 51.2 %copy-start.28 = (f32[64]{0:T(128)S(1)}, f32[64]{0:T(128)}, u32[]{:S(2)}) copy-start(f32[64]{0:T(128)} %get-tuple-element.455) | copy-start | bytes 772
  247.9 51.1 %copy-start.29 = (f32[64]{0:T(128)S(1)}, f32[64]{0:T(128)}, u32[]{:S(2)}) copy-start(f32[64]{0:T(128)} %get-tuple-element.456) | copy-start | bytes 772
  247.9 51.1 %copy-start.30 = (f32[64]{0:T(128)S(1)}, f32[64]{0:T(128)}, u32[]{:S(2)}) copy-start(f32[64]{0:T(128)} %get-tuple-element.457) | copy-start | bytes 772
  248.0 51.1 %copy-start.31 = (f32[64]{0:T(128)S(1)}, f32[64]{0:T(128)}, u32[]{:S(2)}) copy-start(f32[64]{0:T(128)} %get-tuple-element.458) | copy-start | bytes 772
  248.0 51.1 %copy-start.32 = (f32[64]{0:T(128)S(1)}, f32[64]{0:T(128)}, u32[]{:S(2)}) copy-start(f32[64]{0:T(128)} %get-tuple-element.459) | copy-start | bytes 772
  248.0 51.1 %copy-start.33 = (f32[64]{0:T(128)S(1)}, f32[64]{0:T(128)}, u32[]{:S(2)}) copy-start(f32[64]{0:T(128)} %get-tuple-element.460) | copy-start | bytes 772
  248.0 51.1 %copy-start.34 = (f32[64]{0:T(128)S(1)}, f32[64]{0:T(128)}, u32[]{:S(2)}) copy-start(f32[64]{0:T(128)} %get-tuple-element.461) | copy-start | bytes 772
  248.0 51.1 %copy-start.35 = (f32[64]{0:T(128)S(1)}, f32[64]{0:T(128)}, u32[]{:S(2)}) copy-start(f32[64]{0:T(128)} %get-tuple-element.462) | copy-start | bytes 772
  255.5 52.0 %all-to-all-start.4 = ((bf16[32,64,128]{2,1,0:T(8,128)(2,1)}), bf16[32,64,128]{2,1,0:T(8,128)(2,1)S(1)}, u32[]{:S(2)}, u32[]{:S(2)}) async-start(bf16[32,64,128]{2,1,0:T(8,128)(2,1)} %bitcast.56), calls=%async_computation.4 | async-start | bytes 1048576 | tf_op jit(solution)/shard_map/all_to_all | solution.py:43
  261.1 45.5 %copy-start.13 = (bf16[128,1,64]{2,1,0:T(2,128)(2,1)S(1)}, bf16[128,1,64]{2,1,0:T(2,128)(2,1)}, u32[]{:S(2)}) copy-start(bf16[128,1,64]{2,1,0:T(2,128)(2,1)} %copy-done.12) | copy-start | bytes 49156
  261.1 45.5 %copy-start.14 = (bf16[128,1,64]{2,1,0:T(2,128)(2,1)S(1)}, bf16[128,1,64]{2,1,0:T(2,128)(2,1)}, u32[]{:S(2)}) copy-start(bf16[128,1,64]{2,1,0:T(2,128)(2,1)} %copy.133) | copy-start | bytes 49156
  305.0 3.2 %copy-start.19 = (bf16[4,1,32,128]{3,2,1,0:T(8,128)(2,1)}, bf16[4,1,32,128]{3,2,1,0:T(8,128)(2,1)S(1)}, u32[]{:S(2)}) copy-start(bf16[4,1,32,128]{3,2,1,0:T(8,128)(2,1)S(1)} %get-tuple-element.241) | copy-start | bytes 98308
Sparse Core Ops, SparseCore 0:
  46.7 56.1 all-gather.2
where the time goes:
time: 316 us; the launch traced here: 315 us
  waiting for transfers between devices  103 us (33%)
  blocking collectives  88.6 us (28%)
  local copies, waits for them, and re-layouts  40.6 us (13%)
  starting transfers between devices  26.6 us (8%)
  matrix products  23 us (7%)
  other arithmetic  17.9 us (6%)
  between operations  14.8 us (5%)
    all_gather x4, blocking collectives, entering(): lax.all_gather(part.astype(kind), axis)  62.7 us
    all_gather x1, waiting for transfers between devices, side_by_side(): lax.all_gather(both, axis, axis=dim, tiled=True)  56.3 us
    all_to_all x2, waiting for transfers between devices, sent_and_summed(): lax.all_to_all(split_up(shard, dim, devices), axis, 0, 0, tiled=True)  31.3 us
    all_to_all x1, blocking collectives, sent_together(): lax.all_to_all(both, axis, split_axis=split_dim, concat_axis=concat_dim,...  25.9 us
    all_to_all x2, starting transfers between devices, sent_and_summed(): lax.all_to_all(split_up(shard, dim, devices), axis, 0, 0, tiled=True)  10.7 us
    all_to_all x1, starting transfers between devices, on_device(): lax.all_to_all(scattered.astype(jnp.bfloat16), SP, split_axis=0, concat_a...  10.6 us
    all_to_all x1, waiting for transfers between devices, from_everyone(): lax.all_to_all(jnp.broadcast_to(shard[None], (devices, *shard.shape)), ax...  9.21 us
    unnamed x82, local copies, waits for them, and re-layouts  7.8 us
  transfers between devices with their start and end apart: 5, of which 4 were waited for; matrix products, arithmetic and copies ran while one was open for 7% of the time, Pallas kernels for 0%

commit v1 on v0

v1 whole, which is shorter than its diff:
```python
from functools import partial

import jax
import jax.numpy as jnp
from jax import lax
from jax.experimental import pallas as pl
from jax.experimental.pallas import tpu as pltpu
from jax.sharding import Mesh
from jax.sharding import PartitionSpec as P

SP = ("z", "x")
TP = ("y", "c")
BF = jnp.bfloat16
F32 = jnp.float32
HI = lax.Precision.HIGHEST
BLOCK = 32
LIMIT = 56 * 1024 * 1024


def dot(a, b, precision=None):
    return lax.dot_general(
        a, b, (((1,), (0,)), ((), ())), precision=precision, preferred_element_type=F32
    )


def dot_nt(a, b, precision=None):
    return lax.dot_general(
        a, b, (((1,), (1,)), ((), ())), precision=precision, preferred_element_type=F32
    )


def dot_tn(a, b, precision=None):
    return lax.dot_general(
        a, b, (((0,), (0,)), ((), ())), precision=precision, preferred_element_type=F32
    )


def iota(shape, dim):
    return lax.broadcasted_iota(jnp.int32, shape, dim)


def params(**kw):
    return pltpu.CompilerParams(vmem_limit_bytes=LIMIT, **kw)


def call(kernel, name, outs, scalars, *args, blocks=None, scratch=(), after=()):
    blocks = blocks or {}
    specs = []
    used, waits = len(args), len(after)

    def body(at, *refs):
        kernel(at, *refs[:used], *refs[used + waits :])

    for n, a in enumerate(args):
        if n in blocks:
            specs.append(pl.BlockSpec(*blocks[n]))
        else:
            specs.append(pl.BlockSpec(a.shape, lambda i, s, nd=a.ndim: (0,) * nd))
    specs += [pl.BlockSpec(memory_space=pl.ANY)] * waits
    out_specs = tuple(pl.BlockSpec(o.shape, lambda i, s, nd=len(o.shape): (0,) * nd) for o in outs)
    return pl.pallas_call(
        body,
        name=name,
        out_shape=outs,
        grid_spec=pltpu.PrefetchScalarGridSpec(
            num_scalar_prefetch=1,
            grid=(1,),
            in_specs=specs,
            out_specs=out_specs,
            scratch_shapes=list(scratch),
        ),
        compiler_params=params(),
    )(scalars, *args, *after)


def sds(shape, dtype):
    return jax.ShapeDtypeStruct(shape, dtype)


def slots_of(routes):
    tokens = routes.shape[1]
    experts = iota((16, tokens), 0)
    r0, r1 = routes[0:1, :], routes[1:2, :]
    one0, one1 = r0 == experts, r1 == experts
    both = jnp.where(one0 | one1, 1.0, 0.0).astype(BF)
    earlier = jnp.where(iota((tokens, tokens), 0) < iota((tokens, tokens), 1), 1.0, 0.0).astype(BF)
    count = dot(both, earlier)
    s0 = jnp.sum(jnp.where(one0, count, 0.0), axis=0, keepdims=True)
    s1 = jnp.sum(jnp.where(one1, count, 0.0), axis=0, keepdims=True)
    return r0.astype(F32), r1.astype(F32), s0, s1


def column(row):
    return jnp.broadcast_to(row, (row.shape[1], row.shape[1])).T


def dispatch_kernel(at, routes_ref, weight_ref, x_ref, y_ref, out_ref):
    tokens = routes_ref.shape[1]
    r0, r1, s0, s1 = slots_of(routes_ref[...])
    key0 = r0 * 32.0 + s0
    key1 = r1 * 32.0 + s1
    y = y_ref[...].astype(F32)
    w = weight_ref[...]
    table = jnp.concatenate(
        [x_ref[...], (column(w[0:1]) * y).astype(BF), (column(w[1:2]) * y).astype(BF)], axis=0
    )
    q = iota((40, tokens), 0)
    is_input = q < 20
    slot = jnp.where(is_input, q, jnp.where(q < 24, q - 4, q - 24)).astype(F32)
    for e in range(out_ref.shape[0] // 2):
        key = slot + 32.0 * e
        m0, m1 = key0 == key, key1 == key
        a = jnp.concatenate(
            [
                jnp.where(is_input & (m0 | m1), 1.0, 0.0).astype(BF),
                jnp.where(is_input, 0.0, jnp.where(m0, 1.0, 0.0)).astype(BF),
                jnp.where(is_input, 0.0, jnp.where(m1, 1.0, 0.0)).astype(BF),
            ],
            axis=1,
        )
        rows = dot(a, table).astype(BF)
        out_ref[2 * e] = rows
        out_ref[2 * e + 1] = rows


def swap_halves(a):
    return jnp.concatenate([a[4:8], a[0:4]], axis=0)


def delta_kernel(at, g_ref, wg_ref, wu_ref, wd_ref, delta_ref, pack_ref, wgu_ref):
    slices, rows, _ = g_ref.shape
    wgu_ref[:, 0:128] = wg_ref[0]
    wgu_ref[:, 128:256] = wu_ref[0]
    low = iota((8, 128), 0) < 4
    zero8 = jnp.zeros((8, 128), F32)

    def step(i, carry):
        at_row = pl.multiple_of(i * 160, 32)
        a = jnp.concatenate([g_ref[t, pl.ds(at_row, 160), :] for t in range(slices)], axis=1)
        gu = dot(a, wgu_ref[...])
        yh = dot_nt(a, wd_ref[0])
        dgs, dus, dhs, pgs, pus = [], [], [], [], []
        mixed = []
        for d in range(4):
            b = 40 * d
            pg, pu = gu[b : b + 24, 0:128], gu[b : b + 24, 128:256]
            hg = jnp.concatenate([yh[b + 24 : b + 40], swap_halves(yh[b + 16 : b + 24])], axis=0)
            s = jax.nn.sigmoid(pg)
            act = pg * s
            hid = act * pu
            gd = hg * pu * s * (1.0 + pg * (1.0 - s))
            ud = hg * act
            dgs += [gd[0:16], jnp.where(low, gd[16:24], 0.0), zero8, zero8]
            dus += [ud[0:16], jnp.where(low, ud[16:24], 0.0), zero8, zero8]
            dhs += [zero8, zero8, jnp.where(low, 0.0, swap_halves(hid[16:24])), hid[0:16]]
            mixed.append((gd, ud))
        for d in (0, 2):
            for n, parts in ((0, pgs), (1, pus)):
                even, odd = mixed[d][n], mixed[d + 1][n]
                parts += [
                    even[0:16],
                    jnp.where(low, even[16:24], swap_halves(odd[16:24])),
                    odd[0:16],
                ]
        delta_ref[pl.ds(at_row, 160), 0:128] = jnp.concatenate(dgs, axis=0).astype(BF)
        delta_ref[pl.ds(at_row, 160), 128:256] = jnp.concatenate(dus, axis=0).astype(BF)
        delta_ref[pl.ds(at_row, 160), 256:384] = jnp.concatenate(dhs, axis=0).astype(BF)
        at_pack = pl.multiple_of(i * 80, 16)
        pack_ref[pl.ds(at_pack, 80), 0:128] = jnp.concatenate(pgs, axis=0).astype(BF)
        pack_ref[pl.ds(at_pack, 80), 128:256] = jnp.concatenate(pus, axis=0).astype(BF)
        return carry

    lax.fori_loop(0, rows // 160, step, 0)


def partial_kernel(at, pack_ref, wg_ref, wu_ref, woth_ref, out_ref):
    core = at[1]
    lhs = jnp.concatenate([pack_ref[core], pack_ref[1 - core]], axis=1)
    for y in range(0, out_ref.shape[0], 2):
        sides = []
        for v in (y, y + 1):
            first = pl.multiple_of((2 * v + core) * 128, 128)
            sides.append(
                jnp.concatenate(
                    [
                        wg_ref[0, pl.ds(first, 128), :],
                        wu_ref[0, pl.ds(first, 128), :],
                        woth_ref[0, v],
                        woth_ref[1, v],
                    ],
                    axis=1,
                )
            )
        o = dot_nt(lhs, jnp.concatenate(sides, axis=0)).astype(BF)
        out_ref[y] = o[:, 0:128]
        out_ref[y + 1] = o[:, 128:256]


def weight_kernel(at, delta_ref, g_ref, gate_ref, up_ref, down_ref, dt_ref):
    rows = delta_ref.shape[0]
    for r in range(0, rows, 128):
        dt_ref[:, r : r + 128] = delta_ref[r : r + 128, :].astype(F32).T.astype(BF)

    def step(p, carry):
        g2 = jnp.concatenate([g_ref[2 * p], g_ref[2 * p + 1]], axis=1)
        o = dot(dt_ref[...], g2)
        first = pl.multiple_of(p * 256, 256)
        gate_ref[0, pl.ds(first, 256), :] = o[0:128].T.astype(BF)
        up_ref[0, pl.ds(first, 256), :] = o[128:256].T.astype(BF)
        down_ref[0, :, pl.ds(first, 256)] = o[256:384].astype(BF)
        return carry

    lax.fori_loop(0, g_ref.shape[0] // 2, step, 0)


def sum_kernel(at, got_ref, out_ref):
    total = got_ref[0].astype(F32)
    for y in range(1, got_ref.shape[0]):
        total = total + got_ref[y].astype(F32)
    for p in range(out_ref.shape[0] // 2):
        b = 40 * p
        out_ref[2 * p] = total[b : b + 24].astype(BF)
        out_ref[2 * p + 1] = jnp.concatenate(
            [total[b + 24 : b + 40], total[b + 16 : b + 24]], axis=0
        ).astype(BF)


def collect_kernel(at, routes_ref, got_ref, cot_ref, out_ref):
    halves = got_ref.shape[0]
    r0, r1, s0, s1 = slots_of(routes_ref[...])
    shift = (at[2] % 2).astype(F32) * 4.0
    cols = halves * 24
    lanes = iota((routes_ref.shape[1], cols), 1).astype(F32)
    hit = None
    for r, s in ((r0, s0), (r1, s1)):
        first = column(r * 48.0 + s + jnp.where(s >= 16.0, shift, 0.0))[:, 0:1]
        match = (lanes == first) | (lanes == first + 24.0)
        hit = match if hit is None else hit | match
    pick = jnp.where(hit, 1.0, 0.0).astype(BF)
    table = got_ref[...].astype(F32).reshape(cols, 128).astype(BF)
    out_ref[...] = (cot_ref[...].astype(F32) + dot(pick, table)).astype(BF)


def block_of(shape):
    return iota(shape, 1) // BLOCK


def mids_of(gc):
    return [gc[:, b + BLOCK // 2 - 1 : b + BLOCK // 2] for b in range(0, gc.shape[1], BLOCK)]


def growth(gc):
    blocks = block_of(gc.shape)
    mid = jnp.zeros(gc.shape, F32)
    for n, m in enumerate(mids_of(gc)):
        mid = jnp.where(blocks == n, m, mid)
    return jnp.exp(gc - mid)


def causal(tokens):
    return iota((tokens, tokens), 1) <= iota((tokens, tokens), 0)


def forward_kernel(at, q_ref, k_ref, v_ref, g_ref, s_ref, mixed_ref, p_ref, last_ref, gc_ref, tot_ref):
    width, tokens = q_ref.shape
    g = g_ref[...]
    before = jnp.where(iota((tokens, tokens), 0) <= iota((tokens, tokens), 1), 1.0, 0.0)
    gc = dot(g, before, HI)
    gc_ref[...] = gc
    q = q_ref[...].astype(F32) * (width**-0.5)
    k = k_ref[...].astype(F32)
    v = v_ref[...].astype(F32)
    s0 = s_ref[0, 0]
    qt = q * growth(gc)
    parts = []
    for n, mid in enumerate(mids_of(gc)):
        whole = dot_tn(qt, k * jnp.exp(jnp.minimum(mid - gc, 40.0)), HI)
        parts.append(whole[n * BLOCK : (n + 1) * BLOCK])
    p = jnp.where(causal(tokens), jnp.concatenate(parts, axis=0), 0.0)
    p_ref[...] = p.astype(BF)
    mixed_ref[...] = (dot_tn(q * jnp.exp(gc), s0, HI) + dot(p, v, HI)).astype(BF)
    end = gc[:, tokens - 1 : tokens]
    last_ref[...] = jnp.exp(end) * s0 + dot(k * jnp.exp(end - gc), v, HI)
    row = dot_nt(jnp.ones((8, tokens), F32), g, HI)
    tot_ref[...] = jnp.zeros(tot_ref.shape, F32)
    for d in range(tot_ref.shape[0]):
        tot_ref[d, :, 0:width] = row


def decay_kernel(at, tot_ref, out_ref):
    spans = tot_ref.shape[0]
    z, x, nx = at[3], at[4], at[5]
    nz = spans // nx
    k = iota((128, spans), 0)
    u = iota((128, spans), 1)
    own = z * nx + x
    low = jnp.where((k >= nx) & (k < 2 * nx), z * nx - 1, own)
    high = jnp.where(k < nx, z * nx + k, jnp.where(k < 2 * nx, z * nx + k - nx, (k - 2 * nx) * nx))
    inside = jnp.where((u > low) & (u < high), 1.0, 0.0)
    sums = dot(inside, tot_ref[:, 0, :], HI)
    kk = iota((128, 128), 0)
    valid = (
        ((kk < nx) & (kk > x))
        | ((kk >= nx) & (kk < 2 * nx))
        | ((kk > 2 * nx + z) & (kk < 2 * nx + nz))
    )
    out_ref[...] = jnp.where(valid, jnp.exp(sums), 0.0).T


def head_kernel(piece, at, tg_ref, w_ref, q_ref, gc_ref, mixed_ref, rows_ref, send_ref):
    slices = tg_ref.shape[0]
    width = q_ref.shape[0]
    nx = send_ref.shape[0]
    tg = jnp.concatenate([tg_ref[t] for t in range(slices)], axis=1)
    rows = dot(tg, w_ref[...]).astype(BF)
    rows_ref[...] = rows
    qe = q_ref[...].astype(F32) * (width**-0.5) * jnp.exp(gc_ref[...])
    carry = dot(qe, rows.astype(F32), HI).astype(BF)
    own = send_ref.shape[1] - width
    for n in range(nx):
        send_ref[n, own : own + width, :] = carry
    mixed = mixed_ref[...]
    for t in range(slices):
        o = dot_tn(tg_ref[t], mixed).astype(BF)
        for r in range(0, 128, piece):
            d = (t * 128 + r) // piece
            send_ref[d % nx, (d // nx) * piece : (d // nx + 1) * piece, :] = o[r : r + piece]


def local_kernel(at, rows_ref, q_ref, k_ref, v_ref, gc_ref, s_ref, p_ref, qraw_ref, qq_ref, kl_ref, vl_ref):
    width, tokens = q_ref.shape
    scale = width**-0.5
    rows = rows_ref[...]
    gc = gc_ref[...]
    q = q_ref[...].astype(F32)
    k = k_ref[...].astype(F32)
    a = jnp.where(causal(tokens), dot_nt(rows, v_ref[...]), 0.0)
    grow = growth(gc)
    qt = q * scale * grow
    blocks = block_of(gc.shape)
    inner = jnp.zeros((width, tokens), F32)
    key_local = jnp.zeros((width, tokens), F32)
    for n, mid in enumerate(mids_of(gc)):
        fall = jnp.exp(jnp.minimum(mid - gc, 40.0))
        inner = jnp.where(blocks == n, dot_nt(k * fall, a, HI), inner)
        key_local = key_local + fall * dot(jnp.where(blocks == n, qt, 0.0), a, HI)
    qraw = scale * (jnp.exp(gc) * dot_nt(s_ref[0, 0], rows.astype(F32), HI) + grow * inner)
    qraw_ref[...] = qraw.astype(BF)
    qq_ref[...] = q * qraw
    kl_ref[...] = key_local
    vl_ref[...] = dot_tn(p_ref[...], rows)


def group_kernel(at, got_ref, cols_ref, inside_ref, send_ref):
    nx, rows, _ = got_ref.shape
    nz = send_ref.shape[0]
    width = inside_ref.shape[0]
    own = rows - width
    piece = own // nz
    inside = jnp.zeros((width, 128), F32)
    whole = jnp.zeros((width, 128), F32)
    for i in range(nx):
        part = got_ref[i, own:rows, :].astype(F32)
        inside = inside + cols_ref[0:width, i : i + 1] * part
        whole = whole + cols_ref[0:width, nx + i : nx + i + 1] * part
    inside_ref[...] = inside
    whole = whole.astype(BF)
    for i in range(nz):
        total = got_ref[0, i * piece : (i + 1) * piece, :].astype(F32)
        for j in range(1, nx):
            total = total + got_ref[j, i * piece : (i + 1) * piece, :].astype(F32)
        send_ref[i, 0:piece, :] = total.astype(BF)
        send_ref[i, piece : piece + width, :] = whole


def last_kernel(first, at, got_ref, cols_ref, inside_ref, k_ref, v_ref, gc_ref, last_ref, qq_ref, kl_ref, vl_ref, og_ref, key_ref, value_ref, decay_ref):
    width, tokens = k_ref.shape
    piece = og_ref.shape[0]
    incoming = inside_ref[...]
    total = jnp.zeros((piece, 128), F32)
    for i in range(got_ref.shape[0]):
        total = total + got_ref[i, 0:piece, :].astype(F32)
        part = got_ref[i, piece : piece + width, :].astype(F32)
        incoming = incoming + cols_ref[0:width, first + i : first + i + 1] * part
    og_ref[...] = total
    gc = gc_ref[...]
    k = k_ref[...].astype(F32)
    rest = jnp.exp(gc[:, tokens - 1 : tokens] - gc)
    key = kl_ref[...] + rest * dot_nt(incoming, v_ref[...].astype(F32), HI)
    key_ref[...] = key.astype(BF)
    value_ref[...] = (vl_ref[...] + dot_tn(k * rest, incoming, HI)).astype(BF)
    later = jnp.where(causal(tokens), 1.0, 0.0)
    cross = jnp.sum(last_ref[...] * incoming, axis=1, keepdims=True)
    decay_ref[...] = dot(qq_ref[...] - k * key, later, HI) + cross


def on_device(
    expert_input,
    cotangent,
    routes,
    route_weight,
    gate_weight,
    up_weight,
    down_weight,
    out_weight,
    queries,
    key_vectors,
    value_rows,
    log_decay,
    start_state,
):
    tokens = expert_input.shape[0]
    nz, nx, ny = lax.axis_size("z"), lax.axis_size("x"), lax.axis_size("y")
    spans = nz * nx
    slices = ny * 2
    core = lax.axis_index("c")
    at = jnp.stack(
        [
            lax.axis_index(TP),
            core,
            lax.axis_index(SP),
            lax.axis_index("z"),
            lax.axis_index("x"),
            jnp.int32(nx),
        ]
    ).astype(jnp.int32)
    width = queries.shape[2]
    piece_rows = slices * 128 // spans
    routes = routes.T
    route_weight = route_weight.T
    q = queries.reshape(tokens, width).T
    k = key_vectors.reshape(tokens, width).T
    v = value_rows.reshape(tokens, 128)
    g = log_decay.reshape(tokens, width).T
    slice_block = ((tokens, 128), lambda i, s: (0, s[0]))

    (sent,) = call(
        dispatch_kernel,
        "dispatch",
        (sds((spans, 40, 128), BF),),
        at,
        routes,
        route_weight,
        expert_input,
        cotangent,
        blocks={2: slice_block, 3: slice_block},
    )
    piece = lax.all_to_all(sent, SP, 0, 0, tiled=True)
    got = lax.all_gather(piece.reshape(spans * 40, 128), TP, axis=0)

    other = jnp.stack([gate_weight[0], up_weight[0]]).reshape(2, ny, 2, 128, 128)
    other = lax.dynamic_index_in_dim(other, 1 - core, 2, keepdims=False)
    other = lax.ppermute(other, "c", [(0, 1), (1, 0)])
    mixed, p, last, gc, totals = call(
        forward_kernel,
        "forward",
        (
            sds((tokens, 128), BF),
            sds((tokens, tokens), BF),
            sds((width, 128), F32),
            sds((width, tokens), F32),
            sds((spans, 8, 128), F32),
        ),
        at,
        q,
        k,
        v,
        g,
        start_state,
        after=(piece,),
    )
    totals = lax.all_to_all(totals, SP, 0, 0, tiled=True)
    (cols,) = call(decay_kernel, "decays", (sds((128, 128), F32),), at, totals)

    delta, pack = call(
        delta_kernel,
        "deltas",
        (sds((spans * 40, 384), BF), sds((spans * 20, 256), BF)),
        at,
        got,
        gate_weight,
        up_weight,
        down_weight,
        scratch=[pltpu.VMEM((slices * 128, 256), BF)],
        after=(cols, other),
    )
    packs = lax.all_gather(pack, "c", axis=0)
    (terms,) = call(
        partial_kernel,
        "partials",
        (sds((ny, spans * 20, 128), BF),),
        at,
        packs,
        gate_weight,
        up_weight,
        other,
    )
    partials = lax.all_to_all(terms, "y", 0, 0, tiled=True)
    gate_grad, up_grad, down_grad = call(
        weight_kernel,
        "weights",
        (
            sds((1, slices * 128, 128), BF),
            sds((1, slices * 128, 128), BF),
            sds((1, 128, slices * 128), BF),
        ),
        at,
        delta,
        got,
        scratch=[pltpu.VMEM((384, spans * 40), BF)],
        after=(terms,),
    )
    (summed,) = call(
        sum_kernel, "sums", (sds((spans, 24, 128), BF),), at, partials, after=(down_grad,)
    )
    returned = lax.all_to_all(summed, SP, 0, 0, tiled=True)
    (slice_grad,) = call(
        collect_kernel,
        "collect",
        (sds((tokens, 128), BF),),
        at,
        routes,
        returned,
        cotangent,
        blocks={2: slice_block},
    )
    total_grad = lax.all_gather(slice_grad, TP, axis=0)

    rows, leaving = call(
        partial(head_kernel, piece_rows),
        "head",
        (sds((tokens, 128), BF), sds((nx, nz * piece_rows + width, 128), BF)),
        at,
        total_grad,
        out_weight,
        q,
        gc,
        mixed,
    )
    crossing = lax.all_to_all(leaving, "x", 0, 0, tiled=True)
    qraw, qq, key_local, value_local = call(
        local_kernel,
        "local",
        (
            sds((width, tokens), BF),
            sds((width, tokens), F32),
            sds((width, tokens), F32),
            sds((tokens, 128), F32),
        ),
        at,
        rows,
        q,
        k,
        v,
        gc,
        start_state,
        p,
        after=(leaving,),
    )
    inside, group = call(
        group_kernel,
        "group",
        (sds((width, 128), F32), sds((nz, piece_rows + width, 128), BF)),
        at,
        crossing,
        cols,
        after=(qq,),
    )
    group = lax.all_to_all(group, "z", 0, 0, tiled=True)
    out_grad, key, value, decay = call(
        partial(last_kernel, 2 * nx),
        "last",
        (
            sds((piece_rows, 128), F32),
            sds((width, tokens), BF),
            sds((tokens, 128), BF),
            sds((width, tokens), F32),
        ),
        at,
        group,
        cols,
        inside,
        k,
        v,
        gc,
        last,
        qq,
        key_local,
        value_local,
    )
    return (
        gate_grad,
        up_grad,
        down_grad,
        out_grad,
        qraw.T[:, None, :],
        key.T[:, None, :],
        value[:, None, :],
        decay.T[:, None, :],
    )


def solution(mesh):
    torus = Mesh(mesh.devices.reshape(8, 4, mesh.shape["tp"] // 2, 2), ("z", "x", "y", "c"))
    in_specs = (
        P(SP, None),
        P(SP, None),
        P(SP, None),
        P(SP, None),
        P(SP, None, TP),
        P(SP, None, TP),
        P(SP, TP, None),
        P(None, TP),
        P(SP, TP, None),
        P(SP, TP, None),
        P(SP, TP, None),
        P(SP, TP, None),
        P(SP, TP, None, None),
    )
    out_specs = (
        P(SP, None, TP),
        P(SP, None, TP),
        P(SP, TP, None),
        P(SP, TP),
        P(SP, TP, None),
        P(SP, TP, None),
        P(SP, TP, None),
        P(SP, TP, None),
    )
    return jax.shard_map(
        on_device, mesh=torus, in_specs=in_specs, out_specs=out_specs, check_vma=False
    )
```

time: 316 us -> 230 us (0.73)
  the two profiles are of different devices: /device:TPU:2 before, /device:TPU:8 now
where the time goes in v1:
time: 230 us; the launch traced here: 229 us
  blocking collectives  104 us (45%)
  waiting for transfers between devices  49.8 us (22%)
  Pallas kernels  48 us (21%)
  between operations  14.1 us (6%)
  starting transfers between devices  10.3 us (4%)
  local copies, waits for them, and re-layouts  2.59 us (1%)
    pallas_call x12, Pallas kernels, call(): pl.pallas_call(body, name=name, out_shape=outs, grid_spec=pltpu.PrefetchS...  48 us
    all_to_all x1, blocking collectives, on_device(): piece = lax.all_to_all(sent, SP, 0, 0, tiled=True)  27.3 us
    all_to_all x1, waiting for transfers between devices, on_device(): partials = lax.all_to_all(terms, 'y', 0, 0, tiled=True)  24.7 us
    all_to_all x1, blocking collectives, on_device(): returned = lax.all_to_all(summed, SP, 0, 0, tiled=True)  21.6 us
    all_gather x1, blocking collectives, on_device(): total_grad = lax.all_gather(slice_grad, TP, axis=0)  19.1 us
    all_gather x1, waiting for transfers between devices, on_device(): got = lax.all_gather(piece.reshape(spans * 40, 128), TP, axis=0)  17.4 us
    all_to_all x1, blocking collectives, on_device(): totals = lax.all_to_all(totals, SP, 0, 0, tiled=True)  16 us
    all_to_all x1, blocking collectives, on_device(): group = lax.all_to_all(group, 'z', 0, 0, tiled=True)  15.8 us
  transfers between devices with their start and end apart: 4, of which 3 were waited for; matrix products, arithmetic and copies ran while one was open for 0% of the time, Pallas kernels for 8%

profile of v1, /device:TPU:8, one launch (start us, length us, event | category | flops | bytes accessed | tf_op | source)
XLA Modules:
  0.0 228.7 jit_solution(354588187718050122)
XLA Ops:
  7.2 0.0 copy-start.2
  7.2 0.0 copy-start.1
  7.2 0.0 all-gather.4.cloned.1.call-start
  7.2 0.6 stack.26.at
  7.9 2.8 %dispatch.1 = bf16[32,40,128]{2,1,0:T(8,128)(2,1)} custom-call(s32[6]{0:T(128)} %stack.26.at, s32[2,128]{1,0:T(2,128)} %bitcast.49, f32[2,128]{1,0:T(2,128)} %bitcast.51, bf16[128,2048]{1,0:T(8,128)(2,1)} %refs_2_.4, bf16[128,2048]{1,0:T(8,128)(2,1)} %refs_2_.7), custom_call_target="tpu_custom_call" | custom-call | tf_op jit(solution)/shard_map/dispatch/pallas_call | solution.py:61
  10.6 27.3 %all_to_all.30.refs_5_ = bf16[32,40,128]{2,1,0:T(8,128)(2,1)} all-to-all(bf16[32,40,128]{2,1,0:T(8,128)(2,1)} %dispatch.1), channel_id=1, replica_groups=mesh['z'=8,'x'=4,'y'=8,'c'=2] {'z','x'}, dimensions={0} | all-to-all | bytes 655360 | tf_op jit(solution)/shard_map/all_to_all | solution.py:448
  38.0 0.0 all-gather.4.cloned.1.call-update
  38.0 0.0 copy-done.2
  38.0 0.0 copy-done.1
  38.0 0.1 pad_maximum_fusion
  38.2 1.9 collective-permute-start
  40.1 3.2 %forward.1 = (bf16[128,128]{1,0:T(8,128)(2,1)}, bf16[128,128]{1,0:T(8,128)(2,1)}, f32[64,128]{1,0:T(8,128)}, f32[64,128]{1,0:T(8,128)}, f32[32,8,128]{2,1,0:T(8,128)}) custom-call(s32[6]{0:T(128)} %stack.26.at, bf16[64,128]{1,0:T(8,128)(2,1)} %bitcast.42, bf16[64,128]{1,0:T(8,128)(2,1)} %bitcast.45, bf16[128,128]{1,0:T(8,128)(2,1)} %bitcast.39, ...), custom_call_target="tpu_custom_call" | custom-call | tf_op jit(solution)/shard_map/forward/pallas_call | solution.py:61
  43.3 16.0 %all_to_all.31.refs_0_ = f32[32,8,128]{2,1,0:T(8,128)} all-to-all(f32[32,8,128]{2,1,0:T(8,128)} %get-tuple-element.30), channel_id=1, replica_groups=mesh['z'=8,'x'=4,'y'=8,'c'=2] {'z','x'}, dimensions={0} | all-to-all | bytes 262144 | tf_op jit(solution)/shard_map/all_to_all | solution.py:472
  59.2 2.5 %decays.1.refs_4_.refs_1_ = f32[128,128]{1,0:T(8,128)} custom-call(s32[6]{0:T(128)} %stack.26.at, f32[32,8,128]{2,1,0:T(8,128)} %all_to_all.31.refs_0_), custom_call_target="tpu_custom_call" | custom-call | tf_op jit(solution)/shard_map/decays/pallas_call | solution.py:61
  61.8 0.0 collective-permute-done.refs_5_.refs_3_
  61.8 0.0 copy-start.4
  61.8 17.4 %all-gather.4.cloned.1.call-done.refs_0_.refs_1_ = bf16[16,1280,128]{2,1,0:T(8,128)(2,1)} async-done(((bf16[1,1280,128]{2,1,0:T(8,128)(2,1)}), bf16[16,1280,128]{2,1,0:T(8,128)(2,1)}) %all-gather.4.cloned.1.call-update) | async-done | bytes 5242896 | tf_op jit(solution)/shard_map/all_gather | solution.py:449
  79.2 0.0 copy-done.4
  79.2 9.0 %deltas.1 = (bf16[1280,384]{1,0:T(8,128)(2,1)}, bf16[640,256]{1,0:T(8,128)(2,1)}) custom-call(s32[6]{0:T(128)} %stack.26.at, bf16[16,1280,128]{2,1,0:T(8,128)(2,1)} %all-gather.4.cloned.1.call-done.refs_0_.refs_1_, bf16[1,2048,128]{2,1,0:T(8,128)(2,1)} %refs_1_.4, bf16[1,2048,128]{2,1,0:T(8,128)(2,1)} %refs_2_.6, bf16[1,128,2048]{2,1,0:T(8,128)(2,1)} %refs_3_.3, ...), custom_call_target="tpu_custom_call" | custom-call | tf_op jit(solution)/shard_map/deltas/pallas_call | solution.py:61
  88.2 4.0 %all-gather = bf16[1280,256]{1,0:T(8,128)(2,1)} all-gather(bf16[640,256]{1,0:T(8,128)(2,1)} %get-tuple-element.32), channel_id=2, replica_groups=mesh['z'=8,'x'=4,'y'=8,'c'=2] {'c'}, dimensions={0}, use_global_device_ids=true | all-gather | bytes 983040 | tf_op jit(solution)/shard_map/all_gather | solution.py:487
  92.2 4.2 %partials.1.refs_2_ = bf16[8,640,128]{2,1,0:T(8,128)(2,1)} custom-call(s32[6]{0:T(128)} %stack.26.at, bf16[2,640,256]{2,1,0:T(8,128)(2,1)} %bitcast.36, bf16[1,2048,128]{2,1,0:T(8,128)(2,1)} %refs_1_.4, bf16[1,2048,128]{2,1,0:T(8,128)(2,1)} %refs_2_.6, bf16[2,8,128,128]{3,2,1,0:T(8,128)(2,1)} %copy-done.4), custom_call_target="tpu_custom_call" | custom-call | tf_op jit(solution)/shard_map/partials/pallas_call | solution.py:61
  96.4 4.9 %all-to-all-start.2 = ((bf16[8,640,128]{2,1,0:T(8,128)(2,1)}), bf16[8,640,128]{2,1,0:T(8,128)(2,1)S(1)}, u32[]{:S(2)}, u32[]{:S(2)}) async-start(bf16[8,640,128]{2,1,0:T(8,128)(2,1)} %partials.1.refs_2_), calls=%async_computation.2 | async-start | bytes 2621440 | tf_op jit(solution)/shard_map/all_to_all | solution.py:498
  101.2 8.7 %weights.1 = (bf16[1,2048,128]{2,1,0:T(8,128)(2,1)}, bf16[1,2048,128]{2,1,0:T(8,128)(2,1)}, bf16[1,128,2048]{2,1,0:T(8,128)(2,1)}) custom-call(s32[6]{0:T(128)} %stack.26.at, bf16[1280,384]{1,0:T(8,128)(2,1)} %get-tuple-element.31.refs_0_, bf16[16,1280,128]{2,1,0:T(8,128)(2,1)} %all-gather.4.cloned.1.call-done.refs_0_.refs_1_, ...), custom_call_target="tpu_custom_call" | custom-call | tf_op jit(solution)/shard_map/weights/pallas_call | solution.py:61
  109.9 24.7 %all-to-all-done.2.refs_0_ = bf16[8,640,128]{2,1,0:T(8,128)(2,1)S(1)} async-done(((bf16[8,640,128]{2,1,0:T(8,128)(2,1)}), bf16[8,640,128]{2,1,0:T(8,128)(2,1)S(1)}, u32[]{:S(2)}, u32[]{:S(2)}) %all-to-all-start.2) | async-done | bytes 1310752 | tf_op jit(solution)/shard_map/all_to_all | solution.py:498
  134.6 0.0 copy-start
  134.6 1.1 copy-done
  135.6 2.8 %sums.1 = bf16[32,24,128]{2,1,0:T(8,128)(2,1)} custom-call(s32[6]{0:T(128)} %stack.26.at, bf16[8,640,128]{2,1,0:T(8,128)(2,1)} %copy-done, bf16[1,128,2048]{2,1,0:T(8,128)(2,1)} %get-tuple-element.24.refs_1_), custom_call_target="tpu_custom_call" | custom-call | tf_op jit(solution)/shard_map/sums/pallas_call | solution.py:61
  138.5 21.6 %all_to_all.32.refs_1_ = bf16[32,24,128]{2,1,0:T(8,128)(2,1)} all-to-all(bf16[32,24,128]{2,1,0:T(8,128)(2,1)} %sums.1), channel_id=1, replica_groups=mesh['z'=8,'x'=4,'y'=8,'c'=2] {'z','x'}, dimensions={0} | all-to-all | bytes 393216 | tf_op jit(solution)/shard_map/all_to_all | solution.py:516
  160.0 2.8 %collect.1 = bf16[128,128]{1,0:T(8,128)(2,1)} custom-call(s32[6]{0:T(128)} %stack.26.at, s32[2,128]{1,0:T(2,128)} %bitcast.50, bf16[32,24,128]{2,1,0:T(8,128)(2,1)} %all_to_all.32.refs_1_, bf16[128,2048]{1,0:T(8,128)(2,1)} %refs_2_.7), custom_call_target="tpu_custom_call" | custom-call | tf_op jit(solution)/shard_map/collect/pallas_call | solution.py:61
  162.8 19.1 %all-gather.1 = bf16[2048,128]{1,0:T(8,128)(2,1)} all-gather(bf16[128,128]{1,0:T(8,128)(2,1)} %collect.1), channel_id=3, replica_groups=mesh['z'=8,'x'=4,'y'=8,'c'=2] {'y','c'}, dimensions={0}, use_global_device_ids=true | all-gather | bytes 557056 | tf_op jit(solution)/shard_map/all_gather | solution.py:527
  181.9 3.3 %head.1 = (bf16[128,128]{1,0:T(8,128)(2,1)}, bf16[4,576,128]{2,1,0:T(8,128)(2,1)}) custom-call(s32[6]{0:T(128)} %stack.26.at, bf16[16,128,128]{2,1,0:T(8,128)(2,1)} %bitcast.38, bf16[2048,128]{1,0:T(8,128)(2,1)} %refs_1_.5, bf16[64,128]{1,0:T(8,128)(2,1)} %bitcast.43, f32[64,128]{1,0:T(8,128)} %get-tuple-element.36.refs_3_.refs_4_.refs_5_, ...), custom_call_target="tpu_custom_call" | custom-call | tf_op jit(solution)/shard_map/head/pallas_call | solution.py:61
  185.2 3.5 %all-to-all-start.4 = ((bf16[4,576,128]{2,1,0:T(8,128)(2,1)}), bf16[4,576,128]{2,1,0:T(8,128)(2,1)S(1)}, u32[]{:S(2)}, u32[]{:S(2)}) async-start(bf16[4,576,128]{2,1,0:T(8,128)(2,1)} %get-tuple-element.38.refs_7_), calls=%async_computation.4 | async-start | bytes 1179648 | tf_op jit(solution)/shard_map/all_to_all | solution.py:540
  188.7 3.3 %local.1 = (bf16[64,128]{1,0:T(8,128)(2,1)}, f32[64,128]{1,0:T(8,128)}, f32[64,128]{1,0:T(8,128)}, f32[128,128]{1,0:T(8,128)}) custom-call(s32[6]{0:T(128)} %stack.26.at, bf16[128,128]{1,0:T(8,128)(2,1)} %get-tuple-element.39.refs_0_, bf16[64,128]{1,0:T(8,128)(2,1)} %bitcast.44, bf16[64,128]{1,0:T(8,128)(2,1)} %bitcast.46, bf16[128,128]{1,0:T(8,128)(2,1)} %bitcast.40, ...), custom_call_target="tpu_custom_call" | custom-call | tf_op jit(solution)/shard_map/local/pallas_call | solution.py:61
  192.0 7.7 %all-to-all-done.4.refs_0_ = bf16[4,576,128]{2,1,0:T(8,128)(2,1)S(1)} async-done(((bf16[4,576,128]{2,1,0:T(8,128)(2,1)}), bf16[4,576,128]{2,1,0:T(8,128)(2,1)S(1)}, u32[]{:S(2)}, u32[]{:S(2)}) %all-to-all-start.4) | async-done | bytes 589856 | tf_op jit(solution)/shard_map/all_to_all | solution.py:540
  199.6 0.0 copy-start.3
  199.6 0.8 copy-done.3
  200.5 2.6 %group.1 = (f32[64,128]{1,0:T(8,128)}, bf16[8,128,128]{2,1,0:T(8,128)(2,1)}) custom-call(s32[6]{0:T(128)} %stack.26.at, bf16[4,576,128]{2,1,0:T(8,128)(2,1)} %copy-done.3, f32[128,128]{1,0:T(8,128)} %decays.1.refs_4_.refs_1_, f32[64,128]{1,0:T(8,128)} %get-tuple-element.41.refs_2_.refs_7_), custom_call_target="tpu_custom_call" | custom-call | tf_op jit(solution)/shard_map/group/pallas_call | solution.py:61
  203.0 15.8 %all_to_all.33.refs_0_ = bf16[8,128,128]{2,1,0:T(8,128)(2,1)} all-to-all(bf16[8,128,128]{2,1,0:T(8,128)(2,1)} %get-tuple-element.42), channel_id=1, replica_groups=mesh['z'=8,'x'=4,'y'=8,'c'=2] {'z'}, dimensions={0} | all-to-all | bytes 524288 | tf_op jit(solution)/shard_map/all_to_all | solution.py:569
  218.9 3.0 %last.1 = (f32[64,128]{1,0:T(8,128)}, bf16[64,128]{1,0:T(8,128)(2,1)}, bf16[128,128]{1,0:T(8,128)(2,1)}, f32[64,128]{1,0:T(8,128)}) custom-call(s32[6]{0:T(128)} %stack.26.at, bf16[8,128,128]{2,1,0:T(8,128)(2,1)} %all_to_all.33.refs_0_, f32[128,128]{1,0:T(8,128)} %decays.1.refs_4_.refs_1_, f32[64,128]{1,0:T(8,128)} %get-tuple-element.43.refs_2_, ...), custom_call_target="tpu_custom_call" | custom-call | tf_op jit(solution)/shard_map/last/pallas_call | solution.py:61
  (1 shorter events, 0.0 us)
Async XLA Ops:
  7.2 30.8 %copy-start.2 = (bf16[1,2048,128]{2,1,0:T(8,128)(2,1)S(1)}, bf16[1,2048,128]{2,1,0:T(8,128)(2,1)}, u32[]{:S(2)}) copy-start(bf16[1,2048,128]{2,1,0:T(8,128)(2,1)} %refs_2_.6) | copy-start | bytes 1572868
  7.2 30.8 %copy-start.1 = (bf16[1,2048,128]{2,1,0:T(8,128)(2,1)S(1)}, bf16[1,2048,128]{2,1,0:T(8,128)(2,1)}, u32[]{:S(2)}) copy-start(bf16[1,2048,128]{2,1,0:T(8,128)(2,1)} %refs_1_.4) | copy-start | bytes 1572868
  7.2 72.0 %all-gather.4.cloned.1.call-start = ((), (), s32[]{:S(2)}) async-start(), calls=%async_computation.6 | async-start | bytes 5570560 | tf_op jit(solution)/shard_map/all_gather | solution.py:449
  38.2 23.6 %collective-permute-start = (bf16[2,8,128,128]{3,2,1,0:T(8,128)(2,1)S(1)}, bf16[2,8,128,128]{3,2,1,0:T(8,128)(2,1)S(1)}, u32[]{:S(2)}, u32[]{:S(2)}) collective-permute-start(bf16[2,8,128,128]{3,2,1,0:T(8,128)(2,1)S(1)} %dynamic-slice_bitcast_fusion), channel_id=1, source_target_pairs={{0,1},{1,0},{2,3},{3,2},{4,5},{5,4},{6,7},{7,6},{8,9},{9,8},{10,11... | collective-permute-start | bytes 1572872 | tf_op jit(solution)/shard_map/ppermute | solution.py:453
  61.8 17.4 %copy-start.4 = (bf16[2,8,128,128]{3,2,1,0:T(8,128)(2,1)}, bf16[2,8,128,128]{3,2,1,0:T(8,128)(2,1)S(1)}, u32[]{:S(2)}) copy-start(bf16[2,8,128,128]{3,2,1,0:T(8,128)(2,1)S(1)} %collective-permute-done.refs_5_.refs_3_) | copy-start | bytes 1572868
  96.4 38.2 %all-to-all-start.2 = ((bf16[8,640,128]{2,1,0:T(8,128)(2,1)}), bf16[8,640,128]{2,1,0:T(8,128)(2,1)S(1)}, u32[]{:S(2)}, u32[]{:S(2)}) async-start(bf16[8,640,128]{2,1,0:T(8,128)(2,1)} %partials.1.refs_2_), calls=%async_computation.2 | async-start | bytes 2621440 | tf_op jit(solution)/shard_map/all_to_all | solution.py:498
  134.6 1.1 copy-start
  185.2 14.4 %all-to-all-start.4 = ((bf16[4,576,128]{2,1,0:T(8,128)(2,1)}), bf16[4,576,128]{2,1,0:T(8,128)(2,1)S(1)}, u32[]{:S(2)}, u32[]{:S(2)}) async-start(bf16[4,576,128]{2,1,0:T(8,128)(2,1)} %get-tuple-element.38.refs_7_), calls=%async_computation.4 | async-start | bytes 1179648 | tf_op jit(solution)/shard_map/all_to_all | solution.py:540
  199.6 0.8 copy-start.3
Sparse Core Ops, SparseCore 0:
  38.1 41.0 all-gather.3

commit v2 on v1

--- a/solution.py
+++ b/solution.py
@@ -43,8 +43,11 @@
     return pltpu.CompilerParams(vmem_limit_bytes=LIMIT, **kw)
 
 
-def call(kernel, name, outs, scalars, *args, blocks=None, scratch=(), after=()):
+def call(
+    kernel, name, outs, scalars, *args, blocks=None, out_blocks=None, scratch=(), after=(), grid=1
+):
     blocks = blocks or {}
+    out_blocks = out_blocks or {}
     specs = []
     used, waits = len(args), len(after)
 
@@ -57,14 +60,19 @@
         else:
             specs.append(pl.BlockSpec(a.shape, lambda i, s, nd=a.ndim: (0,) * nd))
     specs += [pl.BlockSpec(memory_space=pl.ANY)] * waits
-    out_specs = tuple(pl.BlockSpec(o.shape, lambda i, s, nd=len(o.shape): (0,) * nd) for o in outs)
+    out_specs = tuple(
+        pl.BlockSpec(*out_blocks[n])
+        if n in out_blocks
+        else pl.BlockSpec(o.shape, lambda i, s, nd=len(o.shape): (0,) * nd)
+        for n, o in enumerate(outs)
+    )
     return pl.pallas_call(
         body,
         name=name,
         out_shape=outs,
         grid_spec=pltpu.PrefetchScalarGridSpec(
             num_scalar_prefetch=1,
-            grid=(1,),
+            grid=(grid,),
             in_specs=specs,
             out_specs=out_specs,
             scratch_shapes=list(scratch),
@@ -102,81 +110,97 @@
     y = y_ref[...].astype(F32)
     w = weight_ref[...]
     table = jnp.concatenate(
-        [x_ref[...], (column(w[0:1]) * y).astype(BF), (column(w[1:2]) * y).astype(BF)], axis=0
+        [
+            x_ref[...],
+            (column(w[0:1])[:, 0:1] * y).astype(BF),
+            (column(w[1:2])[:, 0:1] * y).astype(BF),
+        ],
+        axis=0,
     )
     q = iota((40, tokens), 0)
     is_input = q < 20
     slot = jnp.where(is_input, q, jnp.where(q < 24, q - 4, q - 24)).astype(F32)
-    for e in range(out_ref.shape[0] // 2):
+    experts = out_ref.shape[0] // 2
+    picks = []
+    for e in range(experts):
         key = slot + 32.0 * e
         m0, m1 = key0 == key, key1 == key
-        a = jnp.concatenate(
-            [
-                jnp.where(is_input & (m0 | m1), 1.0, 0.0).astype(BF),
-                jnp.where(is_input, 0.0, jnp.where(m0, 1.0, 0.0)).astype(BF),
-                jnp.where(is_input, 0.0, jnp.where(m1, 1.0, 0.0)).astype(BF),
-            ],
-            axis=1,
+        picks.append(
+            jnp.concatenate(
+                [
+                    jnp.where(is_input & (m0 | m1), 1.0, 0.0),
+                    jnp.where(is_input, 0.0, jnp.where(m0, 1.0, 0.0)),
+                    jnp.where(is_input, 0.0, jnp.where(m1, 1.0, 0.0)),
+                ],
+                axis=1,
+            )
         )
-        rows = dot(a, table).astype(BF)
-        out_ref[2 * e] = rows
-        out_ref[2 * e + 1] = rows
+    pick = jnp.concatenate(picks, axis=0).astype(BF)
+    for f in range(0, out_ref.shape[2], 256):
+        rows = dot(pick, table[:, f : f + 256])
+        for e in range(experts):
+            block = rows[40 * e : 40 * e + 40].astype(BF)
+            out_ref[2 * e, :, f : f + 256] = block
+            out_ref[2 * e + 1, :, f : f + 256] = block
 
 
 def swap_halves(a):
     return jnp.concatenate([a[4:8], a[0:4]], axis=0)
 
 
-def delta_kernel(at, g_ref, wg_ref, wu_ref, wd_ref, delta_ref, pack_ref, wgu_ref):
-    slices, rows, _ = g_ref.shape
-    wgu_ref[:, 0:128] = wg_ref[0]
-    wgu_ref[:, 128:256] = wu_ref[0]
+def three_products(g_ref, wg_ref, wu_ref, wd_ref):
+    g = g_ref[...]
+    return dot(g, jnp.concatenate([wg_ref[0], wu_ref[0]], axis=1)), dot_nt(g, wd_ref[0])
+
+
+def first_kernel(at, g_ref, wg_ref, wu_ref, wd_ref, gu_ref, yh_ref):
+    gu, yh = three_products(g_ref, wg_ref, wu_ref, wd_ref)
+    gu_ref[...] = gu
+    yh_ref[...] = yh
+
+
+def delta_kernel(at, g_ref, wg_ref, wu_ref, wd_ref, gu_ref, yh_ref, delta_ref, pack_ref):
+    gu, yh = three_products(g_ref, wg_ref, wu_ref, wd_ref)
+    gu = gu + gu_ref[...]
+    yh = yh + yh_ref[...]
     low = iota((8, 128), 0) < 4
     zero8 = jnp.zeros((8, 128), F32)
-
-    def step(i, carry):
-        at_row = pl.multiple_of(i * 160, 32)
-        a = jnp.concatenate([g_ref[t, pl.ds(at_row, 160), :] for t in range(slices)], axis=1)
-        gu = dot(a, wgu_ref[...])
-        yh = dot_nt(a, wd_ref[0])
-        dgs, dus, dhs, pgs, pus = [], [], [], [], []
-        mixed = []
-        for d in range(4):
-            b = 40 * d
-            pg, pu = gu[b : b + 24, 0:128], gu[b : b + 24, 128:256]
-            hg = jnp.concatenate([yh[b + 24 : b + 40], swap_halves(yh[b + 16 : b + 24])], axis=0)
-            s = jax.nn.sigmoid(pg)
-            act = pg * s
-            hid = act * pu
-            gd = hg * pu * s * (1.0 + pg * (1.0 - s))
-            ud = hg * act
-            dgs += [gd[0:16], jnp.where(low, gd[16:24], 0.0), zero8, zero8]
-            dus += [ud[0:16], jnp.where(low, ud[16:24], 0.0), zero8, zero8]
-            dhs += [zero8, zero8, jnp.where(low, 0.0, swap_halves(hid[16:24])), hid[0:16]]
-            mixed.append((gd, ud))
-        for d in (0, 2):
-            for n, parts in ((0, pgs), (1, pus)):
-                even, odd = mixed[d][n], mixed[d + 1][n]
-                parts += [
-                    even[0:16],
-                    jnp.where(low, even[16:24], swap_halves(odd[16:24])),
-                    odd[0:16],
-                ]
-        delta_ref[pl.ds(at_row, 160), 0:128] = jnp.concatenate(dgs, axis=0).astype(BF)
-        delta_ref[pl.ds(at_row, 160), 128:256] = jnp.concatenate(dus, axis=0).astype(BF)
-        delta_ref[pl.ds(at_row, 160), 256:384] = jnp.concatenate(dhs, axis=0).astype(BF)
-        at_pack = pl.multiple_of(i * 80, 16)
-        pack_ref[pl.ds(at_pack, 80), 0:128] = jnp.concatenate(pgs, axis=0).astype(BF)
-        pack_ref[pl.ds(at_pack, 80), 128:256] = jnp.concatenate(pus, axis=0).astype(BF)
-        return carry
-
-    lax.fori_loop(0, rows // 160, step, 0)
+    dgs, dus, dhs, pgs, pus = [], [], [], [], []
+    mixed = []
+    spans = g_ref.shape[0] // 40
+    for d in range(spans):
+        b = 40 * d
+        pg, pu = gu[b : b + 24, 0:128], gu[b : b + 24, 128:256]
+        hg = jnp.concatenate([yh[b + 24 : b + 40], swap_halves(yh[b + 16 : b + 24])], axis=0)
+        s = jax.nn.sigmoid(pg)
+        act = pg * s
+        hid = act * pu
+        gd = hg * pu * s * (1.0 + pg * (1.0 - s))
+        ud = hg * act
+        dgs += [gd[0:16], jnp.where(low, gd[16:24], 0.0), zero8, zero8]
+        dus += [ud[0:16], jnp.where(low, ud[16:24], 0.0), zero8, zero8]
+        dhs += [zero8, zero8, jnp.where(low, 0.0, swap_halves(hid[16:24])), hid[0:16]]
+        mixed.append((gd, ud))
+    for d in range(0, spans, 2):
+        for n, parts in ((0, pgs), (1, pus)):
+            even, odd = mixed[d][n], mixed[d + 1][n]
+            parts += [
+                even[0:16],
+                jnp.where(low, even[16:24], swap_halves(odd[16:24])),
+                odd[0:16],
+            ]
+    delta_ref[:, 0:128] = jnp.concatenate(dgs, axis=0).astype(BF)
+    delta_ref[:, 128:256] = jnp.concatenate(dus, axis=0).astype(BF)
+    delta_ref[:, 256:384] = jnp.concatenate(dhs, axis=0).astype(BF)
+    pack_ref[:, 0:128] = jnp.concatenate(pgs, axis=0).astype(BF)
+    pack_ref[:, 128:256] = jnp.concatenate(pus, axis=0).astype(BF)
 
 
 def partial_kernel(at, pack_ref, wg_ref, wu_ref, woth_ref, out_ref):
     core = at[1]
     lhs = jnp.concatenate([pack_ref[core], pack_ref[1 - core]], axis=1)
-    for y in range(0, out_ref.shape[0], 2):
+    nz, ny, rows, _ = out_ref.shape
+    for y in range(0, ny, 2):
         sides = []
         for v in (y, y + 1):
             first = pl.multiple_of((2 * v + core) * 128, 128)
@@ -192,49 +216,56 @@
                 )
             )
         o = dot_nt(lhs, jnp.concatenate(sides, axis=0)).astype(BF)
-        out_ref[y] = o[:, 0:128]
-        out_ref[y + 1] = o[:, 128:256]
-
-
-def weight_kernel(at, delta_ref, g_ref, gate_ref, up_ref, down_ref, dt_ref):
-    rows = delta_ref.shape[0]
+        for z in range(nz):
+            out_ref[z, y] = o[z * rows : (z + 1) * rows, 0:128]
+            out_ref[z, y + 1] = o[z * rows : (z + 1) * rows, 128:256]
+
+
+def weight_kernel(at, delta_ref, own_ref, other_ref, gate_ref, up_ref, down_ref, dt_ref):
+    rows, half = own_ref.shape
     for r in range(0, rows, 128):
         dt_ref[:, r : r + 128] = delta_ref[r : r + 128, :].astype(F32).T.astype(BF)
-
-    def step(p, carry):
-        g2 = jnp.concatenate([g_ref[2 * p], g_ref[2 * p + 1]], axis=1)
-        o = dot(dt_ref[...], g2)
-        first = pl.multiple_of(p * 256, 256)
-        gate_ref[0, pl.ds(first, 256), :] = o[0:128].T.astype(BF)
-        up_ref[0, pl.ds(first, 256), :] = o[128:256].T.astype(BF)
-        down_ref[0, :, pl.ds(first, 256)] = o[256:384].astype(BF)
-        return carry
-
-    lax.fori_loop(0, g_ref.shape[0] // 2, step, 0)
+    for g_ref, core in ((own_ref, at[1]), (other_ref, 1 - at[1])):
+
+        def step(p, carry, g_ref=g_ref, core=core):
+            o = dot(dt_ref[...], g_ref[:, pl.ds(pl.multiple_of(p * 256, 256), 256)])
+            first = pl.multiple_of(core * half + p * 256, 256)
+            gate_ref[0, pl.ds(first, 256), :] = o[0:128].T.astype(BF)
+            up_ref[0, pl.ds(first, 256), :] = o[128:256].T.astype(BF)
+            down_ref[0, :, pl.ds(first, 256)] = o[256:384].astype(BF)
+            return carry
+
+        lax.fori_loop(0, half // 256, step, 0)
 
 
 def sum_kernel(at, got_ref, out_ref):
-    total = got_ref[0].astype(F32)
-    for y in range(1, got_ref.shape[0]):
-        total = total + got_ref[y].astype(F32)
-    for p in range(out_ref.shape[0] // 2):
-        b = 40 * p
-        out_ref[2 * p] = total[b : b + 24].astype(BF)
-        out_ref[2 * p + 1] = jnp.concatenate(
-            [total[b + 24 : b + 40], total[b + 16 : b + 24]], axis=0
-        ).astype(BF)
+    nz, ny, _, _ = got_ref.shape
+    for z in range(nz):
+        total = got_ref[z, 0].astype(F32)
+        for y in range(1, ny):
+            total = total + got_ref[z, y].astype(F32)
+        for p in range(out_ref.shape[0] // 2):
+            b = 40 * p
+            out_ref[2 * p, z] = total[b : b + 24].astype(BF)
+            out_ref[2 * p + 1, z] = jnp.concatenate(
+                [total[b + 24 : b + 40], total[b + 16 : b + 24]], axis=0
+            ).astype(BF)
 
 
 def collect_kernel(at, routes_ref, got_ref, cot_ref, out_ref):
-    halves = got_ref.shape[0]
-    r0, r1, s0, s1 = slots_of(routes_ref[...])
-    shift = (at[2] % 2).astype(F32) * 4.0
-    cols = halves * 24
-    lanes = iota((routes_ref.shape[1], cols), 1).astype(F32)
+    nx, nz, _, _ = got_ref.shape
+    routes = routes_ref[...]
+    _, _, s0, s1 = slots_of(routes)
+    shift = (at[4] % 2).astype(F32) * 4.0
+    cols = nx * nz * 24
+    lanes = iota((routes.shape[1], cols), 1).astype(F32)
     hit = None
-    for r, s in ((r0, s0), (r1, s1)):
-        first = column(r * 48.0 + s + jnp.where(s >= 16.0, shift, 0.0))[:, 0:1]
-        match = (lanes == first) | (lanes == first + 24.0)
+    for n, s in ((0, s0), (1, s1)):
+        half = routes[n : n + 1, :] * 2
+        block = (half % nx) * nz + half // nx
+        row = block.astype(F32) * 24.0 + s + jnp.where(s >= 16.0, shift, 0.0)
+        first = column(row)[:, 0:1]
+        match = (lanes == first) | (lanes == first + 24.0 * nz)
         hit = match if hit is None else hit | match
     pick = jnp.where(hit, 1.0, 0.0).astype(BF)
     table = got_ref[...].astype(F32).reshape(cols, 128).astype(BF)
@@ -283,8 +314,7 @@
     last_ref[...] = jnp.exp(end) * s0 + dot(k * jnp.exp(end - gc), v, HI)
     row = dot_nt(jnp.ones((8, tokens), F32), g, HI)
     tot_ref[...] = jnp.zeros(tot_ref.shape, F32)
-    for d in range(tot_ref.shape[0]):
-        tot_ref[d, :, 0:width] = row
+    tot_ref[:, 0:width] = row
 
 
 def decay_kernel(at, tot_ref, out_ref):
@@ -433,24 +463,25 @@
     v = value_rows.reshape(tokens, 128)
     g = log_decay.reshape(tokens, width).T
     slice_block = ((tokens, 128), lambda i, s: (0, s[0]))
+    half = slices * 64
+    half_block = ((tokens, half), lambda i, s: (0, s[1]))
 
     (sent,) = call(
         dispatch_kernel,
         "dispatch",
-        (sds((spans, 40, 128), BF),),
+        (sds((spans, 40, half), BF),),
         at,
         routes,
         route_weight,
         expert_input,
         cotangent,
-        blocks={2: slice_block, 3: slice_block},
-    )
-    piece = lax.all_to_all(sent, SP, 0, 0, tiled=True)
-    got = lax.all_gather(piece.reshape(spans * 40, 128), TP, axis=0)
-
-    other = jnp.stack([gate_weight[0], up_weight[0]]).reshape(2, ny, 2, 128, 128)
-    other = lax.dynamic_index_in_dim(other, 1 - core, 2, keepdims=False)
-    other = lax.ppermute(other, "c", [(0, 1), (1, 0)])
+        blocks={2: half_block, 3: half_block},
+    )
+    own = lax.all_to_all(sent, SP, 0, 0, tiled=True).reshape(spans * 40, half)
+
+    weights = jnp.stack([gate_weight[0], up_weight[0]]).reshape(2, ny, 2, 128, 128)
+    weights = lax.dynamic_index_in_dim(weights, 1 - core, 2, keepdims=False)
+    weights = lax.ppermute(weights, "c", [(0, 1), (1, 0)])
     mixed, p, last, gc, totals = call(
         forward_kernel,
         "forward",
@@ -459,7 +490,7 @@
             sds((tokens, tokens), BF),
             sds((width, 128), F32),
             sds((width, tokens), F32),
-            sds((spans, 8, 128), F32),
+            sds((8, 128), F32),
         ),
         at,
         q,
@@ -467,35 +498,73 @@
         v,
         g,
         start_state,
-        after=(piece,),
-    )
-    totals = lax.all_to_all(totals, SP, 0, 0, tiled=True)
+        after=(sent,),
+    )
+    totals = lax.all_gather(lax.all_gather(totals, "x"), "z").reshape(spans, 8, 128)
     (cols,) = call(decay_kernel, "decays", (sds((128, 128), F32),), at, totals)
 
+    own, cols, weights = lax.optimization_barrier((own, cols, weights))
+    tiles = spans // 8
+    rows_block = ((320, half), lambda i, s: (i, 0))
+    acc_blocks = (((320, 256), lambda i, s: (i, 0)), ((320, 128), lambda i, s: (i, 0)))
+    gu, yh = call(
+        first_kernel,
+        "first",
+        (sds((spans * 40, 256), F32), sds((spans * 40, 128), F32)),
+        at,
+        own,
+        gate_weight,
+        up_weight,
+        down_weight,
+        blocks={
+            0: rows_block,
+            1: ((1, half, 128), lambda i, s: (0, s[1], 0)),
+            2: ((1, half, 128), lambda i, s: (0, s[1], 0)),
+            3: ((1, 128, half), lambda i, s: (0, 0, s[1])),
+        },
+        out_blocks={0: acc_blocks[0], 1: acc_blocks[1]},
+        grid=tiles,
+    )
+    other = lax.ppermute(own, "c", [(0, 1), (1, 0)])
     delta, pack = call(
         delta_kernel,
         "deltas",
         (sds((spans * 40, 384), BF), sds((spans * 20, 256), BF)),
         at,
-        got,
+        other,
         gate_weight,
         up_weight,
         down_weight,
-        scratch=[pltpu.VMEM((slices * 128, 256), BF)],
-        after=(cols, other),
+        gu,
+        yh,
+        blocks={
+            0: rows_block,
+            1: ((1, half, 128), lambda i, s: (0, 1 - s[1], 0)),
+            2: ((1, half, 128), lambda i, s: (0, 1 - s[1], 0)),
+            3: ((1, 128, half), lambda i, s: (0, 0, 1 - s[1])),
+            4: acc_blocks[0],
+            5: acc_blocks[1],
+        },
+        out_blocks={
+            0: ((320, 384), lambda i, s: (i, 0)),
+            1: ((160, 256), lambda i, s: (i, 0)),
+        },
+        grid=tiles,
     )
     packs = lax.all_gather(pack, "c", axis=0)
     (terms,) = call(
         partial_kernel,
         "partials",
-        (sds((ny, spans * 20, 128), BF),),
+        (sds((nz, ny, nx * 20, 128), BF),),
         at,
         packs,
         gate_weight,
         up_weight,
-        other,
-    )
-    partials = lax.all_to_all(terms, "y", 0, 0, tiled=True)
+        weights,
+    )
+    got = lax.all_to_all(
+        terms.reshape(nz * ny, nx * 20, 128), ("z", "y"), 0, 0, tiled=True
+    ).reshape(nz, ny, nx * 20, 128)
     gate_grad, up_grad, down_grad = call(
         weight_kernel,
         "weights",
@@ -506,21 +575,22 @@
         ),
         at,
         delta,
-        got,
+        own,
+        other,
         scratch=[pltpu.VMEM((384, spans * 40), BF)],
         after=(terms,),
     )
     (summed,) = call(
-        sum_kernel, "sums", (sds((spans, 24, 128), BF),), at, partials, after=(down_grad,)
-    )
-    returned = lax.all_to_all(summed, SP, 0, 0, tiled=True)
+        sum_kernel, "sums", (sds((nx, nz, 24, 128), BF),), at, got, after=(down_grad,)
+    )
+    returned = lax.all_to_all(summed.reshape(nx, nz * 24, 128), "x", 0, 0, tiled=True)
     (slice_grad,) = call(
         collect_kernel,
         "collect",
         (sds((tokens, 128), BF),),
         at,
         routes,
-        returned,
+        returned.reshape(nx, nz, 24, 128),
         cotangent,
         blocks={2: slice_block},
     )

time: 230 us -> 249 us (1.083)
  the two profiles are of different devices: /device:TPU:8 before, /device:TPU:2 now
where the time goes in v2:
time: 249 us; the launch traced here: 248 us
  blocking collectives  122 us (49%)
  Pallas kernels  52.2 us (21%)
  starting transfers between devices  34.4 us (14%)
  waiting for transfers between devices  33.5 us (13%)
  local copies, waits for them, and re-layouts  4.09 us (2%)
    all_gather x1, blocking collectives, on_device(): lax.all_gather(lax.all_gather(totals, 'x'), 'z').reshape(spans, 8, 128)  60.6 us
    pallas_call x13, Pallas kernels, call(): pl.pallas_call(body, name=name, out_shape=outs, grid_spec=pltpu.PrefetchS...  52.2 us
    all_to_all x1, waiting for transfers between devices, on_device(): lax.all_to_all(terms.reshape(nz * ny, nx * 20, 128), ('z', 'y'), 0, 0, ti...  27.2 us
    all_gather x1, blocking collectives, on_device(): total_grad = lax.all_gather(slice_grad, TP, axis=0)  18.7 us
    all_to_all x1, blocking collectives, on_device(): group = lax.all_to_all(group, 'z', 0, 0, tiled=True)  15.8 us
    all_to_all x1, starting transfers between devices, on_device(): own = lax.all_to_all(sent, SP, 0, 0, tiled=True).reshape(spans * 40, half)  13.6 us
    all_gather x1, blocking collectives, on_device(): lax.all_gather(totals, 'x')  12.3 us
    all_to_all x1, starting transfers between devices, on_device(): lax.all_to_all(terms.reshape(nz * ny, nx * 20, 128), ('z', 'y'), 0, 0, ti...  12 us
  transfers between devices with their start and end apart: 5, of which 2 were waited for; matrix products, arithmetic and copies ran while one was open for 0% of the time, Pallas kernels for 9%

profile of v2, /device:TPU:2, one launch (start us, length us, event | category | flops | bytes accessed | tf_op | source)
XLA Modules:
  0.0 247.6 jit_solution(8728754651908433380)
XLA Ops:
  0.6 0.6 stack.26.at
  1.3 4.2 %dispatch.1.refs_5_ = bf16[32,40,1024]{2,1,0:T(8,128)(2,1)} custom-call(s32[6]{0:T(128)} %stack.26.at, s32[2,128]{1,0:T(2,128)} %bitcast.61, f32[2,128]{1,0:T(2,128)} %bitcast.63, bf16[128,2048]{1,0:T(8,128)(2,1)} %refs_2_.5, bf16[128,2048]{1,0:T(8,128)(2,1)} %refs_2_.9), custom_call_target="tpu_custom_call" | custom-call | tf_op jit(solution)/shard_map/dispatch/pallas_call | solution.py:69
  5.5 0.0 copy-start.2
  5.5 13.6 %all-to-all-start = ((bf16[32,40,1024]{2,1,0:T(8,128)(2,1)}), bf16[32,40,1024]{2,1,0:T(8,128)(2,1)S(1)}, u32[]{:S(2)}, u32[]{:S(2)}) async-start(bf16[32,40,1024]{2,1,0:T(8,128)(2,1)} %dispatch.1.refs_5_), calls=%async_computation | async-start | bytes 5242880 | tf_op jit(solution)/shard_map/all_to_all | solution.py:480
  19.1 0.0 copy-done.2
  19.1 1.1 pad_maximum_fusion
  20.3 1.9 collective-permute-start
  22.2 3.1 %forward.1 = (bf16[128,128]{1,0:T(8,128)(2,1)}, bf16[128,128]{1,0:T(8,128)(2,1)}, f32[64,128]{1,0:T(8,128)}, f32[64,128]{1,0:T(8,128)}, f32[8,128]{1,0:T(8,128)}) custom-call(s32[6]{0:T(128)} %stack.26.at, bf16[64,128]{1,0:T(8,128)(2,1)} %bitcast.53, bf16[64,128]{1,0:T(8,128)(2,1)} %bitcast.56, bf16[128,128]{1,0:T(8,128)(2,1)} %bitcast.50, ...), custom_call_target="tpu_custom_call" | custom-call | tf_op jit(solution)/shard_map/forward/pallas_call | solution.py:69
  25.4 12.3 %all-gather = f32[32,128]{1,0:T(8,128)S(1)} all-gather(f32[8,128]{1,0:T(8,128)} %get-tuple-element.35), channel_id=2, replica_groups=mesh['z'=8,'x'=4,'y'=8,'c'=2] {'x'}, dimensions={0}, use_global_device_ids=true | all-gather | bytes 20480 | tf_op jit(solution)/shard_map/all_gather | solution.py:503
  37.7 60.6 %all-gather.1.refs_0_ = f32[32,8,128]{2,1,0:T(8,128)} all-gather(f32[4,8,128]{2,1,0:T(8,128)S(1)} %bitcast.59), channel_id=3, replica_groups=mesh['z'=8,'x'=4,'y'=8,'c'=2] {'z'}, dimensions={0}, use_global_device_ids=true | all-gather | bytes 147456 | tf_op jit(solution)/shard_map/all_gather | solution.py:503
  98.3 2.5 %decays.1.refs_1_ = f32[128,128]{1,0:T(8,128)} custom-call(s32[6]{0:T(128)} %stack.26.at, f32[32,8,128]{2,1,0:T(8,128)} %all-gather.1.refs_0_), custom_call_target="tpu_custom_call" | custom-call | tf_op jit(solution)/shard_map/decays/pallas_call | solution.py:69
  100.8 0.0 collective-permute-done.refs_3_
  100.8 0.0 copy-start.5
  100.8 0.0 all-to-all-done
  100.8 0.0 copy-start
  100.8 1.9 collective-permute-start.1
  102.7 0.0 copy-done
  102.7 5.7 %first.1 = (f32[1280,256]{1,0:T(8,128)}, f32[1280,128]{1,0:T(8,128)}) custom-call(s32[6]{0:T(128)} %stack.26.at, bf16[1280,1024]{1,0:T(8,128)(2,1)} %bitcast.41, bf16[1,2048,128]{2,1,0:T(8,128)(2,1)} %refs_1_.6, bf16[1,2048,128]{2,1,0:T(8,128)(2,1)} %refs_2_.8, bf16[1,128,2048]{2,1,0:T(8,128)(2,1)} %refs_3_.5), custom_call_target="tpu_custom_call" | custom-call | tf_op jit(solution)/shard_map/first/pallas_call | solution.py:69
  108.5 0.0 collective-permute-done.1.refs_0_.refs_2_
  108.5 0.0 copy-start.1
  108.5 1.5 copy-done.1
  110.0 6.0 %deltas.1 = (bf16[1280,384]{1,0:T(8,128)(2,1)}, bf16[640,256]{1,0:T(8,128)(2,1)}) custom-call(s32[6]{0:T(128)} %stack.26.at, bf16[1280,1024]{1,0:T(8,128)(2,1)} %copy-done.1, bf16[1,2048,128]{2,1,0:T(8,128)(2,1)} %refs_1_.6, bf16[1,2048,128]{2,1,0:T(8,128)(2,1)} %refs_2_.8, bf16[1,128,2048]{2,1,0:T(8,128)(2,1)} %refs_3_.5, ...), custom_call_target="tpu_custom_call" | custom-call | tf_op jit(solution)/shard_map/deltas/pallas_call | solution.py:69
  116.0 4.3 %all-gather.2 = bf16[1280,256]{1,0:T(8,128)(2,1)} all-gather(bf16[640,256]{1,0:T(8,128)(2,1)} %get-tuple-element.40), channel_id=4, replica_groups=mesh['z'=8,'x'=4,'y'=8,'c'=2] {'c'}, dimensions={0}, use_global_device_ids=true | all-gather | bytes 983040 | tf_op jit(solution)/shard_map/all_gather | solution.py:554
  120.3 0.0 copy-done.5
  120.3 4.2 %partials.1.refs_3_ = bf16[8,8,80,128]{3,2,1,0:T(8,128)(2,1)} custom-call(s32[6]{0:T(128)} %stack.26.at, bf16[2,640,256]{2,1,0:T(8,128)(2,1)} %bitcast.45, bf16[1,2048,128]{2,1,0:T(8,128)(2,1)} %refs_1_.6, bf16[1,2048,128]{2,1,0:T(8,128)(2,1)} %refs_2_.8, bf16[2,8,128,128]{3,2,1,0:T(8,128)(2,1)} %copy-done.5), custom_call_target="tpu_custom_call" | custom-call | tf_op jit(solution)/shard_map/partials/pallas_call | solution.py:69
  124.5 12.0 %all-to-all-start.1 = ((bf16[64,80,128]{2,1,0:T(8,128)(2,1)}), bf16[64,80,128]{2,1,0:T(8,128)(2,1)S(1)}, u32[]{:S(2)}, u32[]{:S(2)}) async-start(bf16[64,80,128]{2,1,0:T(8,128)(2,1)} %bitcast.43), calls=%async_computation.1 | async-start | bytes 2621440 | tf_op jit(solution)/shard_map/all_to_all | solution.py:565
  136.5 8.7 %weights.1 = (bf16[1,2048,128]{2,1,0:T(8,128)(2,1)}, bf16[1,2048,128]{2,1,0:T(8,128)(2,1)}, bf16[1,128,2048]{2,1,0:T(8,128)(2,1)}) custom-call(s32[6]{0:T(128)} %stack.26.at, bf16[1280,384]{1,0:T(8,128)(2,1)} %get-tuple-element.39.refs_0_, bf16[1280,1024]{1,0:T(8,128)(2,1)} %bitcast.42, bf16[1280,1024]{1,0:T(8,128)(2,1)} %copy-done.1, ...), custom_call_target="tpu_custom_call" | custom-call | tf_op jit(solution)/shard_map/weights/pallas_call | solution.py:69
  145.2 27.2 %all-to-all-done.1 = bf16[64,80,128]{2,1,0:T(8,128)(2,1)S(1)} async-done(((bf16[64,80,128]{2,1,0:T(8,128)(2,1)}), bf16[64,80,128]{2,1,0:T(8,128)(2,1)S(1)}, u32[]{:S(2)}, u32[]{:S(2)}) %all-to-all-start.1) | async-done | bytes 1310752 | tf_op jit(solution)/shard_map/all_to_all | solution.py:565
  172.4 0.0 copy-start.3
  172.4 1.1 copy-done.3
  173.5 2.8 %sums.1 = bf16[4,8,24,128]{3,2,1,0:T(8,128)(2,1)} custom-call(s32[6]{0:T(128)} %stack.26.at, bf16[8,8,80,128]{3,2,1,0:T(8,128)(2,1)} %bitcast.44, bf16[1,128,2048]{2,1,0:T(8,128)(2,1)} %get-tuple-element.29.refs_1_), custom_call_target="tpu_custom_call" | custom-call | tf_op jit(solution)/shard_map/sums/pallas_call | solution.py:69
  176.3 9.8 %all_to_all.25 = bf16[4,192,128]{2,1,0:T(8,128)(2,1)} all-to-all(bf16[4,192,128]{2,1,0:T(8,128)(2,1)} %bitcast.48), channel_id=1, replica_groups=mesh['z'=8,'x'=4,'y'=8,'c'=2] {'x'}, dimensions={0} | all-to-all | bytes 393216 | tf_op jit(solution)/shard_map/all_to_all | solution.py:586
  186.1 2.8 %collect.1 = bf16[128,128]{1,0:T(8,128)(2,1)} custom-call(s32[6]{0:T(128)} %stack.26.at, s32[2,128]{1,0:T(2,128)} %bitcast.62, bf16[4,8,24,128]{3,2,1,0:T(8,128)(2,1)} %bitcast.49, bf16[128,2048]{1,0:T(8,128)(2,1)} %refs_2_.9), custom_call_target="tpu_custom_call" | custom-call | tf_op jit(solution)/shard_map/collect/pallas_call | solution.py:69
  188.9 18.7 %all-gather.3 = bf16[2048,128]{1,0:T(8,128)(2,1)} all-gather(bf16[128,128]{1,0:T(8,128)(2,1)} %collect.1), channel_id=5, replica_groups=mesh['z'=8,'x'=4,'y'=8,'c'=2] {'y','c'}, dimensions={0}, use_global_device_ids=true | all-gather | bytes 557056 | tf_op jit(solution)/shard_map/all_gather | solution.py:597
  207.6 3.3 %head.1 = (bf16[128,128]{1,0:T(8,128)(2,1)}, bf16[4,576,128]{2,1,0:T(8,128)(2,1)}) custom-call(s32[6]{0:T(128)} %stack.26.at, bf16[16,128,128]{2,1,0:T(8,128)(2,1)} %bitcast.47, bf16[2048,128]{1,0:T(8,128)(2,1)} %refs_1_.7, bf16[64,128]{1,0:T(8,128)(2,1)} %bitcast.54, f32[64,128]{1,0:T(8,128)} %get-tuple-element.45.refs_3_.refs_4_.refs_5_, ...), custom_call_target="tpu_custom_call" | custom-call | tf_op jit(solution)/shard_map/head/pallas_call | solution.py:69
  210.9 4.9 %all-to-all-start.3 = ((bf16[4,576,128]{2,1,0:T(8,128)(2,1)}), bf16[4,576,128]{2,1,0:T(8,128)(2,1)S(1)}, u32[]{:S(2)}, u32[]{:S(2)}) async-start(bf16[4,576,128]{2,1,0:T(8,128)(2,1)} %get-tuple-element.47.refs_7_), calls=%async_computation.3 | async-start | bytes 1179648 | tf_op jit(solution)/shard_map/all_to_all | solution.py:610
  215.8 3.2 %local.1 = (bf16[64,128]{1,0:T(8,128)(2,1)}, f32[64,128]{1,0:T(8,128)}, f32[64,128]{1,0:T(8,128)}, f32[128,128]{1,0:T(8,128)}) custom-call(s32[6]{0:T(128)} %stack.26.at, bf16[128,128]{1,0:T(8,128)(2,1)} %get-tuple-element.49.refs_0_, bf16[64,128]{1,0:T(8,128)(2,1)} %bitcast.55, bf16[64,128]{1,0:T(8,128)(2,1)} %bitcast.57, bf16[128,128]{1,0:T(8,128)(2,1)} %bitcast.51, ...), custom_call_target="tpu_custom_call" | custom-call | tf_op jit(solution)/shard_map/local/pallas_call | solution.py:69
  219.0 6.3 %all-to-all-done.3.refs_0_ = bf16[4,576,128]{2,1,0:T(8,128)(2,1)S(1)} async-done(((bf16[4,576,128]{2,1,0:T(8,128)(2,1)}), bf16[4,576,128]{2,1,0:T(8,128)(2,1)S(1)}, u32[]{:S(2)}, u32[]{:S(2)}) %all-to-all-start.3) | async-done | bytes 589856 | tf_op jit(solution)/shard_map/all_to_all | solution.py:610
  225.3 0.0 copy-start.4
  225.3 0.8 copy-done.4
  226.1 2.6 %group.1 = (f32[64,128]{1,0:T(8,128)}, bf16[8,128,128]{2,1,0:T(8,128)(2,1)}) custom-call(s32[6]{0:T(128)} %stack.26.at, bf16[4,576,128]{2,1,0:T(8,128)(2,1)} %copy-done.4, f32[128,128]{1,0:T(8,128)} %decays.1.refs_1_, f32[64,128]{1,0:T(8,128)} %get-tuple-element.51.refs_2_.refs_7_), custom_call_target="tpu_custom_call" | custom-call | tf_op jit(solution)/shard_map/group/pallas_call | solution.py:69
  228.7 15.8 %all_to_all.26.refs_0_ = bf16[8,128,128]{2,1,0:T(8,128)(2,1)} all-to-all(bf16[8,128,128]{2,1,0:T(8,128)(2,1)} %get-tuple-element.52), channel_id=1, replica_groups=mesh['z'=8,'x'=4,'y'=8,'c'=2] {'z'}, dimensions={0} | all-to-all | bytes 524288 | tf_op jit(solution)/shard_map/all_to_all | solution.py:639
  244.6 3.0 %last.1 = (f32[64,128]{1,0:T(8,128)}, bf16[64,128]{1,0:T(8,128)(2,1)}, bf16[128,128]{1,0:T(8,128)(2,1)}, f32[64,128]{1,0:T(8,128)}) custom-call(s32[6]{0:T(128)} %stack.26.at, bf16[8,128,128]{2,1,0:T(8,128)(2,1)} %all_to_all.26.refs_0_, f32[128,128]{1,0:T(8,128)} %decays.1.refs_1_, f32[64,128]{1,0:T(8,128)} %get-tuple-element.53.refs_2_, ...), custom_call_target="tpu_custom_call" | custom-call | tf_op jit(solution)/shard_map/last/pallas_call | solution.py:69
  (1 shorter events, 0.0 us)
Async XLA Ops:
  5.5 13.6 %copy-start.2 = (bf16[1,2048,128]{2,1,0:T(8,128)(2,1)S(1)}, bf16[1,2048,128]{2,1,0:T(8,128)(2,1)}, u32[]{:S(2)}) copy-start(bf16[1,2048,128]{2,1,0:T(8,128)(2,1)} %refs_1_.6) | copy-start | bytes 1572868
  5.5 95.3 %all-to-all-start = ((bf16[32,40,1024]{2,1,0:T(8,128)(2,1)}), bf16[32,40,1024]{2,1,0:T(8,128)(2,1)S(1)}, u32[]{:S(2)}, u32[]{:S(2)}) async-start(bf16[32,40,1024]{2,1,0:T(8,128)(2,1)} %dispatch.1.refs_5_), calls=%async_computation | async-start | bytes 5242880 | tf_op jit(solution)/shard_map/all_to_all | solution.py:480
  20.3 80.5 %collective-permute-start = (bf16[2,8,128,128]{3,2,1,0:T(8,128)(2,1)S(1)}, bf16[2,8,128,128]{3,2,1,0:T(8,128)(2,1)S(1)}, u32[]{:S(2)}, u32[]{:S(2)}) collective-permute-start(bf16[2,8,128,128]{3,2,1,0:T(8,128)(2,1)S(1)} %dynamic-slice_bitcast_fusion), channel_id=1, source_target_pairs={{0,1},{1,0},{2,3},{3,2},{4,5},{5,4},{6,7},{7,6},{8,9},{9,8},{10,11... | collective-permute-start | bytes 1572872 | tf_op jit(solution)/shard_map/ppermute | solution.py:484
  100.8 19.5 %copy-start.5 = (bf16[2,8,128,128]{3,2,1,0:T(8,128)(2,1)}, bf16[2,8,128,128]{3,2,1,0:T(8,128)(2,1)S(1)}, u32[]{:S(2)}) copy-start(bf16[2,8,128,128]{3,2,1,0:T(8,128)(2,1)S(1)} %collective-permute-done.refs_3_) | copy-start | bytes 1572868
  100.8 1.9 copy-start
  100.8 7.7 %collective-permute-start.1 = (bf16[1280,1024]{1,0:T(8,128)(2,1)S(1)}, bf16[1280,1024]{1,0:T(8,128)(2,1)S(1)}, u32[]{:S(2)}, u32[]{:S(2)}) collective-permute-start(bf16[1280,1024]{1,0:T(8,128)(2,1)S(1)} %bitcast.40), channel_id=1, source_target_pairs={{0,1},{1,0},{2,3},{3,2},{4,5},{5,4},{6,7},{7,6},{8,9},{9,8},{10,11... | collective-permute-start | bytes 7864328 | tf_op jit(solution)/shard_map/ppermute | solution.py:528
  108.5 1.5 copy-start.1
  124.5 47.9 %all-to-all-start.1 = ((bf16[64,80,128]{2,1,0:T(8,128)(2,1)}), bf16[64,80,128]{2,1,0:T(8,128)(2,1)S(1)}, u32[]{:S(2)}, u32[]{:S(2)}) async-start(bf16[64,80,128]{2,1,0:T(8,128)(2,1)} %bitcast.43), calls=%async_computation.1 | async-start | bytes 2621440 | tf_op jit(solution)/shard_map/all_to_all | solution.py:565
  172.4 1.1 copy-start.3
  210.9 14.4 %all-to-all-start.3 = ((bf16[4,576,128]{2,1,0:T(8,128)(2,1)}), bf16[4,576,128]{2,1,0:T(8,128)(2,1)S(1)}, u32[]{:S(2)}, u32[]{:S(2)}) async-start(bf16[4,576,128]{2,1,0:T(8,128)(2,1)} %get-tuple-element.47.refs_7_), calls=%async_computation.3 | async-start | bytes 1179648 | tf_op jit(solution)/shard_map/all_to_all | solution.py:610
  225.3 0.8 copy-start.4

commit v3 on v2

--- a/solution.py
+++ b/solution.py
@@ -137,37 +137,49 @@
         )
     pick = jnp.concatenate(picks, axis=0).astype(BF)
     for f in range(0, out_ref.shape[2], 256):
-        rows = dot(pick, table[:, f : f + 256])
+        wide = slice(f, min(f + 256, out_ref.shape[2]))
+        rows = dot(pick, table[:, wide])
         for e in range(experts):
             block = rows[40 * e : 40 * e + 40].astype(BF)
-            out_ref[2 * e, :, f : f + 256] = block
-            out_ref[2 * e + 1, :, f : f + 256] = block
+            out_ref[2 * e, :, wide] = block
+            out_ref[2 * e + 1, :, wide] = block
 
 
 def swap_halves(a):
     return jnp.concatenate([a[4:8], a[0:4]], axis=0)
 
 
-def three_products(g_ref, wg_ref, wu_ref, wd_ref):
-    g = g_ref[...]
+def products(g, wg_ref, wu_ref, wd_ref):
     return dot(g, jnp.concatenate([wg_ref[0], wu_ref[0]], axis=1)), dot_nt(g, wd_ref[0])
 
 
-def first_kernel(at, g_ref, wg_ref, wu_ref, wd_ref, gu_ref, yh_ref):
-    gu, yh = three_products(g_ref, wg_ref, wu_ref, wd_ref)
-    gu_ref[...] = gu
-    yh_ref[...] = yh
-
-
-def delta_kernel(at, g_ref, wg_ref, wu_ref, wd_ref, gu_ref, yh_ref, delta_ref, pack_ref):
-    gu, yh = three_products(g_ref, wg_ref, wu_ref, wd_ref)
+def first_kernel(at, a_ref, b_ref, *refs):
+    gu0, yh0 = products(a_ref[...], *refs[0:3])
+    gu1, yh1 = products(b_ref[...], *refs[3:6])
+    refs[6][...] = gu0 + gu1
+    refs[7][...] = yh0 + yh1
+
+
+def chosen(low_ref, high_ref):
+    upper = pl.program_id(0) >= pl.num_programs(0) // 2
+    return jnp.where(upper, high_ref[...], low_ref[...])
+
+
+def second_kernel(at, low_ref, high_ref, wg_ref, wu_ref, wd_ref, gu_ref, yh_ref, gu_out, yh_out):
+    gu, yh = products(chosen(low_ref, high_ref), wg_ref, wu_ref, wd_ref)
+    gu_out[...] = gu + gu_ref[...]
+    yh_out[...] = yh + yh_ref[...]
+
+
+def delta_kernel(at, low_ref, high_ref, wg_ref, wu_ref, wd_ref, gu_ref, yh_ref, delta_ref, pack_ref):
+    gu, yh = products(chosen(low_ref, high_ref), wg_ref, wu_ref, wd_ref)
     gu = gu + gu_ref[...]
     yh = yh + yh_ref[...]
     low = iota((8, 128), 0) < 4
     zero8 = jnp.zeros((8, 128), F32)
     dgs, dus, dhs, pgs, pus = [], [], [], [], []
     mixed = []
-    spans = g_ref.shape[0] // 40
+    spans = low_ref.shape[0] // 40
     for d in range(spans):
         b = 40 * d
         pg, pu = gu[b : b + 24, 0:128], gu[b : b + 24, 128:256]
@@ -221,21 +233,27 @@
             out_ref[z, y + 1] = o[z * rows : (z + 1) * rows, 128:256]
 
 
-def weight_kernel(at, delta_ref, own_ref, other_ref, gate_ref, up_ref, down_ref, dt_ref):
-    rows, half = own_ref.shape
+def weight_kernel(at, delta_ref, a_ref, b_ref, c0_ref, c1_ref, d0_ref, d1_ref, gate_ref, up_ref, down_ref, dt_ref):
+    rows, part = a_ref.shape
     for r in range(0, rows, 128):
         dt_ref[:, r : r + 128] = delta_ref[r : r + 128, :].astype(F32).T.astype(BF)
-    for g_ref, core in ((own_ref, at[1]), (other_ref, 1 - at[1])):
-
-        def step(p, carry, g_ref=g_ref, core=core):
-            o = dot(dt_ref[...], g_ref[:, pl.ds(pl.multiple_of(p * 256, 256), 256)])
-            first = pl.multiple_of(core * half + p * 256, 256)
-            gate_ref[0, pl.ds(first, 256), :] = o[0:128].T.astype(BF)
-            up_ref[0, pl.ds(first, 256), :] = o[128:256].T.astype(BF)
-            down_ref[0, :, pl.ds(first, 256)] = o[256:384].astype(BF)
-            return carry
-
-        lax.fori_loop(0, half // 256, step, 0)
+    core, side = at[1], at[6]
+    for refs, quarter in (
+        ((a_ref,), 2 * side + core),
+        ((b_ref,), 2 * side + 1 - core),
+        ((c0_ref, c1_ref), 2 * (1 - side) + core),
+        ((d0_ref, d1_ref), 2 * (1 - side) + 1 - core),
+    ):
+        size = rows // len(refs)
+        for p in range(0, part, 256):
+            o = dot(dt_ref[:, 0:size], refs[0][:, p : p + 256])
+            for n in range(1, len(refs)):
+                o = o + dot(dt_ref[:, n * size : (n + 1) * size], refs[n][:, p : p + 256])
+            at_row = pl.multiple_of(quarter * part + p, 128)
+            wide = min(256, part - p)
+            gate_ref[0, pl.ds(at_row, wide), :] = o[0:128].T.astype(BF)
+            up_ref[0, pl.ds(at_row, wide), :] = o[128:256].T.astype(BF)
+            down_ref[0, :, pl.ds(at_row, wide)] = o[256:384].astype(BF)
 
 
 def sum_kernel(at, got_ref, out_ref):
@@ -290,6 +308,21 @@
 
 def causal(tokens):
     return iota((tokens, tokens), 1) <= iota((tokens, tokens), 0)
+
+
+def in_parts(rows):
+    high = rows.astype(BF)
+    rest = rows - high.astype(F32)
+    mid = rest.astype(BF)
+    low = (rest - mid.astype(F32)).astype(BF)
+    n = iota(rows.shape, 0)
+    parts = jnp.where(n == 0, high.astype(F32), jnp.where(n == 1, mid.astype(F32), low.astype(F32)))
+    return jnp.where(n < 3, parts, 0.0).astype(BF)
+
+
+def columns(rows):
+    rows = rows + [jnp.zeros((128 - len(rows), 128), F32)]
+    return jnp.concatenate(rows, axis=0).T
 
 
 def forward_kernel(at, q_ref, k_ref, v_ref, g_ref, s_ref, mixed_ref, p_ref, last_ref, gc_ref, tot_ref):
@@ -313,31 +346,11 @@
     end = gc[:, tokens - 1 : tokens]
     last_ref[...] = jnp.exp(end) * s0 + dot(k * jnp.exp(end - gc), v, HI)
     row = dot_nt(jnp.ones((8, tokens), F32), g, HI)
-    tot_ref[...] = jnp.zeros(tot_ref.shape, F32)
-    tot_ref[:, 0:width] = row
-
-
-def decay_kernel(at, tot_ref, out_ref):
-    spans = tot_ref.shape[0]
-    z, x, nx = at[3], at[4], at[5]
-    nz = spans // nx
-    k = iota((128, spans), 0)
-    u = iota((128, spans), 1)
-    own = z * nx + x
-    low = jnp.where((k >= nx) & (k < 2 * nx), z * nx - 1, own)
-    high = jnp.where(k < nx, z * nx + k, jnp.where(k < 2 * nx, z * nx + k - nx, (k - 2 * nx) * nx))
-    inside = jnp.where((u > low) & (u < high), 1.0, 0.0)
-    sums = dot(inside, tot_ref[:, 0, :], HI)
-    kk = iota((128, 128), 0)
-    valid = (
-        ((kk < nx) & (kk > x))
-        | ((kk >= nx) & (kk < 2 * nx))
-        | ((kk > 2 * nx + z) & (kk < 2 * nx + nz))
-    )
-    out_ref[...] = jnp.where(valid, jnp.exp(sums), 0.0).T
-
-
-def head_kernel(piece, at, tg_ref, w_ref, q_ref, gc_ref, mixed_ref, rows_ref, send_ref):
+    row = jnp.concatenate([row, jnp.zeros((8, 128 - width), F32)], axis=1)
+    tot_ref[...] = in_parts(row)
+
+
+def head_kernel(piece, at, tg_ref, w_ref, q_ref, gc_ref, mixed_ref, tot_ref, rows_ref, send_ref):
     slices = tg_ref.shape[0]
     width = q_ref.shape[0]
     nx = send_ref.shape[0]
@@ -346,9 +359,10 @@
     rows_ref[...] = rows
     qe = q_ref[...].astype(F32) * (width**-0.5) * jnp.exp(gc_ref[...])
     carry = dot(qe, rows.astype(F32), HI).astype(BF)
-    own = send_ref.shape[1] - width
+    own = send_ref.shape[1] - width - 8
     for n in range(nx):
         send_ref[n, own : own + width, :] = carry
+        send_ref[n, own + width : own + width + 8, :] = tot_ref[...]
     mixed = mixed_ref[...]
     for t in range(slices):
         o = dot_tn(tg_ref[t], mixed).astype(BF)
@@ -381,37 +395,60 @@
     vl_ref[...] = dot_tn(p_ref[...], rows)
 
 
-def group_kernel(at, got_ref, cols_ref, inside_ref, send_ref):
+def group_kernel(at, got_ref, inside_ref, after_ref, send_ref):
     nx, rows, _ = got_ref.shape
     nz = send_ref.shape[0]
     width = inside_ref.shape[0]
-    own = rows - width
+    own = rows - width - 8
     piece = own // nz
+    x = at[4]
+    zero = jnp.zeros((1, 128), F32)
+    before, later = zero, zero
+    weights, wholes = [], []
+    for i in range(nx):
+        weights.append(jnp.where(x < i, jnp.exp(later), 0.0))
+        wholes.append(jnp.exp(before))
+        part = got_ref[i, own + width : own + width + 8, :].astype(F32)
+        total = jnp.sum(part, axis=0, keepdims=True)
+        before = before + total
+        later = later + jnp.where(x < i, total, 0.0)
+    after_ref[...] = jnp.broadcast_to(later, (8, 128))
+    cols = columns(weights + wholes)
     inside = jnp.zeros((width, 128), F32)
     whole = jnp.zeros((width, 128), F32)
     for i in range(nx):
-        part = got_ref[i, own:rows, :].astype(F32)
-        inside = inside + cols_ref[0:width, i : i + 1] * part
-        whole = whole + cols_ref[0:width, nx + i : nx + i + 1] * part
+        part = got_ref[i, own : own + width, :].astype(F32)
+        inside = inside + cols[0:width, i : i + 1] * part
+        whole = whole + cols[0:width, nx + i : nx + i + 1] * part
     inside_ref[...] = inside
     whole = whole.astype(BF)
+    parts = in_parts(jnp.broadcast_to(before, (8, 128)))
     for i in range(nz):
         total = got_ref[0, i * piece : (i + 1) * piece, :].astype(F32)
         for j in range(1, nx):
             total = total + got_ref[j, i * piece : (i + 1) * piece, :].astype(F32)
         send_ref[i, 0:piece, :] = total.astype(BF)
         send_ref[i, piece : piece + width, :] = whole
-
-
-def last_kernel(first, at, got_ref, cols_ref, inside_ref, k_ref, v_ref, gc_ref, last_ref, qq_ref, kl_ref, vl_ref, og_ref, key_ref, value_ref, decay_ref):
+        send_ref[i, piece + width : piece + width + 8, :] = parts
+
+
+def last_kernel(at, got_ref, inside_ref, after_ref, k_ref, v_ref, gc_ref, last_ref, qq_ref, kl_ref, vl_ref, og_ref, key_ref, value_ref, decay_ref):
     width, tokens = k_ref.shape
     piece = og_ref.shape[0]
+    z = at[3]
+    sums = after_ref[0:1, :]
+    weights = []
+    for i in range(got_ref.shape[0]):
+        weights.append(jnp.where(z < i, jnp.exp(sums), 0.0))
+        part = got_ref[i, piece + width : piece + width + 8, :].astype(F32)
+        sums = sums + jnp.where(z < i, jnp.sum(part, axis=0, keepdims=True), 0.0)
+    cols = columns(weights)
     incoming = inside_ref[...]
     total = jnp.zeros((piece, 128), F32)
     for i in range(got_ref.shape[0]):
         total = total + got_ref[i, 0:piece, :].astype(F32)
         part = got_ref[i, piece : piece + width, :].astype(F32)
-        incoming = incoming + cols_ref[0:width, first + i : first + i + 1] * part
+        incoming = incoming + cols[0:width, i : i + 1] * part
     og_ref[...] = total
     gc = gc_ref[...]
     k = k_ref[...].astype(F32)
@@ -444,16 +481,10 @@
     spans = nz * nx
     slices = ny * 2
     core = lax.axis_index("c")
-    at = jnp.stack(
-        [
-            lax.axis_index(TP),
-            core,
-            lax.axis_index(SP),
-            lax.axis_index("z"),
-            lax.axis_index("x"),
-            jnp.int32(nx),
-        ]
-    ).astype(jnp.int32)
+    place = lax.axis_index(("z", "x", "y", "c"))
+    divide = jnp.array([1, 1, slices, slices * nx, slices, 1, 2], jnp.int32)
+    wrap = jnp.array([slices, 2, spans, nz, nx, 1, 2], jnp.int32)
+    at = (place // divide) % wrap
     width = queries.shape[2]
     piece_rows = slices * 128 // spans
     routes = routes.T
@@ -463,21 +494,21 @@
     v = value_rows.reshape(tokens, 128)
     g = log_decay.reshape(tokens, width).T
     slice_block = ((tokens, 128), lambda i, s: (0, s[0]))
-    half = slices * 64
-    half_block = ((tokens, half), lambda i, s: (0, s[1]))
+    part = slices * 32
+    part_block = ((tokens, part), lambda i, s: (0, 2 * s[6] + s[1]))
 
     (sent,) = call(
         dispatch_kernel,
         "dispatch",
-        (sds((spans, 40, half), BF),),
+        (sds((spans, 40, part), BF),),
         at,
         routes,
         route_weight,
         expert_input,
         cotangent,
-        blocks={2: half_block, 3: half_block},
-    )
-    own = lax.all_to_all(sent, SP, 0, 0, tiled=True).reshape(spans * 40, half)
+        blocks={2: part_block, 3: part_block},
+    )
+    own = lax.all_to_all(sent, SP, 0, 0, tiled=True).reshape(spans * 40, part)
 
     weights = jnp.stack([gate_weight[0], up_weight[0]]).reshape(2, ny, 2, 128, 128)
     weights = lax.dynamic_index_in_dim(weights, 1 - core, 2, keepdims=False)
@@ -490,7 +521,7 @@
             sds((tokens, tokens), BF),
             sds((width, 128), F32),
             sds((width, tokens), F32),
-            sds((8, 128), F32),
+            sds((8, 128), BF),
         ),
         at,
         q,
@@ -500,50 +531,89 @@
         start_state,
         after=(sent,),
     )
-    totals = lax.all_gather(lax.all_gather(totals, "x"), "z").reshape(spans, 8, 128)
-    (cols,) = call(decay_kernel, "decays", (sds((128, 128), F32),), at, totals)
-
-    own, cols, weights = lax.optimization_barrier((own, cols, weights))
+    own, mixed, weights = lax.optimization_barrier((own, mixed, weights))
+
+    swap = [(0, 1), (1, 0)]
+    rows_all = spans * 40
+    up = [(i, (i + 1) % ny) for i in range(ny)]
+    down = [(i, (i - 1) % ny) for i in range(ny)]
+    low = lax.ppermute(own[: rows_all // 2], "y", up)
+    high = lax.ppermute(own[rows_all // 2 :], "y", down)
+    beside = lax.ppermute(own, "c", swap)
+
     tiles = spans // 8
-    rows_block = ((320, half), lambda i, s: (i, 0))
+    last_low = tiles // 2 - 1
+    rows_block = ((320, part), lambda i, s: (i, 0))
+    low_block = ((320, part), lambda i, s: (jnp.minimum(i, last_low), 0))
+    high_block = ((320, part), lambda i, s: (jnp.maximum(i - last_low - 1, 0), 0))
     acc_blocks = (((320, 256), lambda i, s: (i, 0)), ((320, 128), lambda i, s: (i, 0)))
+    acc = (sds((rows_all, 256), F32), sds((rows_all, 128), F32))
+
+    def weight_blocks(first, quarter):
+        return {
+            first: ((1, part, 128), lambda i, s: (0, quarter(s), 0)),
+            first + 1: ((1, part, 128), lambda i, s: (0, quarter(s), 0)),
+            first + 2: ((1, 128, part), lambda i, s: (0, 0, quarter(s))),
+        }
+
+    experts = (gate_weight, up_weight, down_weight)
     gu, yh = call(
         first_kernel,
         "first",
-        (sds((spans * 40, 256), F32), sds((spans * 40, 128), F32)),
+        acc,
         at,
         own,
-        gate_weight,
-        up_weight,
-        down_weight,
+        beside,
+        *experts,
+        *experts,
         blocks={
             0: rows_block,
-            1: ((1, half, 128), lambda i, s: (0, s[1], 0)),
-            2: ((1, half, 128), lambda i, s: (0, s[1], 0)),
-            3: ((1, 128, half), lambda i, s: (0, 0, s[1])),
+            1: rows_block,
+            **weight_blocks(2, lambda s: 2 * s[6] + s[1]),
+            **weight_blocks(5, lambda s: 2 * s[6] + 1 - s[1]),
         },
         out_blocks={0: acc_blocks[0], 1: acc_blocks[1]},
         grid=tiles,
     )
-    other = lax.ppermute(own, "c", [(0, 1), (1, 0)])
+    low, high, gu, yh = lax.optimization_barrier((low, high, gu, yh))
+    low_beside = lax.ppermute(low, "c", swap)
+    high_beside = lax.ppermute(high, "c", swap)
+    gu, yh = call(
+        second_kernel,
+        "second",
+        acc,
+        at,
+        low,
+        high,
+        *experts,
+        gu,
+        yh,
+        blocks={
+            0: low_block,
+            1: high_block,
+            **weight_blocks(2, lambda s: 2 * (1 - s[6]) + s[1]),
+            5: acc_blocks[0],
+            6: acc_blocks[1],
+        },
+        out_blocks={0: acc_blocks[0], 1: acc_blocks[1]},
+        grid=tiles,
+    )
     delta, pack = call(
         delta_kernel,
         "deltas",
-        (sds((spans * 40, 384), BF), sds((spans * 20, 256), BF)),
-        at,
-        other,
-        gate_weight,
-        up_weight,
-        down_weight,
+        (sds((rows_all, 384), BF), sds((rows_all // 2, 256), BF)),
+        at,
+        low_beside,
+        high_beside,
+        *experts,
         gu,
         yh,
         blocks={
-            0: rows_block,
-            1: ((1, half, 128), lambda i, s: (0, 1 - s[1], 0)),
-            2: ((1, half, 128), lambda i, s: (0, 1 - s[1], 0)),
-            3: ((1, 128, half), lambda i, s: (0, 0, 1 - s[1])),
-            4: acc_blocks[0],
-            5: acc_blocks[1],
+            0: low_block,
+            1: high_block,
+            **weight_blocks(2, lambda s: 2 * (1 - s[6]) + 1 - s[1]),
+            5: acc_blocks[0],
+            6: acc_blocks[1],
         },
         out_blocks={
             0: ((320, 384), lambda i, s: (i, 0)),
@@ -576,7 +646,11 @@
         at,
         delta,
         own,
-        other,
+        beside,
+        low,
+        high,
+        low_beside,
+        high_beside,
         scratch=[pltpu.VMEM((384, spans * 40), BF)],
         after=(terms,),
     )
@@ -599,13 +673,14 @@
     rows, leaving = call(
         partial(head_kernel, piece_rows),
         "head",
-        (sds((tokens, 128), BF), sds((nx, nz * piece_rows + width, 128), BF)),
+        (sds((tokens, 128), BF), sds((nx, nz * piece_rows + width + 8, 128), BF)),
         at,
         total_grad,
         out_weight,
         q,
         gc,
         mixed,
+        totals,
     )
     crossing = lax.all_to_all(leaving, "x", 0, 0, tiled=True)
     qraw, qq, key_local, value_local = call(
@@ -627,18 +702,21 @@
         p,
         after=(leaving,),
     )
-    inside, group = call(
+    inside, later, group = call(
         group_kernel,
         "group",
-        (sds((width, 128), F32), sds((nz, piece_rows + width, 128), BF)),
+        (
+            sds((width, 128), F32),
+            sds((8, 128), F32),
+            sds((nz, piece_rows + width + 8, 128), BF),
+        ),
         at,
         crossing,
-        cols,
         after=(qq,),
     )
     group = lax.all_to_all(group, "z", 0, 0, tiled=True)
     out_grad, key, value, decay = call(
-        partial(last_kernel, 2 * nx),
+        last_kernel,
         "last",
         (
             sds((piece_rows, 128), F32),
@@ -648,8 +726,8 @@
         ),
         at,
         group,
-        cols,
         inside,
+        later,
         k,
         v,
         gc,

time: 249 us -> 225 us (0.904)
  blocking collectives: 122 us -> 49.5 us
  waiting for transfers between devices: 33.5 us -> 73.9 us
  starting transfers between devices: 34.4 us -> 40.7 us
    all_gather x2 -> x0, blocking collectives: 72.9 us -> none  [the longest x1 60.6 us: on_device(): lax.all_gather(lax.all_gather(totals, 'x'), 'z').reshape(spans, 8, 128)]
    all_to_all x1, waiting for transfers between devices: 0.01 us -> 27.6 us  [on_device(): own = lax.all_to_all(sent, SP, 0, 0, tiled=True).reshape(spans * 40, part)]
    ppermute x1 -> x5, starting transfers between devices: 1.92 us -> 13.5 us  [the longest x1 5.38 us: on_device(): high = lax.ppermute(own[rows_all // 2:], 'y', down)]
    ppermute x1 -> x5, waiting for transfers between devices: 0.01 us -> 11.2 us  [the longest x1 5.86 us: on_device(): high = lax.ppermute(own[rows_all // 2:], 'y', down)]
    all_to_all x1, starting transfers between devices: 12 us -> 6.77 us  [on_device(): lax.all_to_all(terms.reshape(nz * ny, nx * 20, 128), ('z', 'y'), 0, 0, ti...]
  transfers between devices with their start and end apart: 5 -> 9, of which waited for: 2 -> 5; matrix products, arithmetic and copies ran while one was open for 0% -> 0% of each run, Pallas kernels for 9% -> 11%
where the time goes in v3:
time: 225 us; the launch traced here: 223 us
  waiting for transfers between devices  73.9 us (33%)
  Pallas kernels  52.3 us (23%)
  blocking collectives  49.5 us (22%)
  starting transfers between devices  40.7 us (18%)
  local copies, waits for them, and re-layouts  4.27 us (2%)
    pallas_call x13, Pallas kernels, call(): pl.pallas_call(body, name=name, out_shape=outs, grid_spec=pltpu.PrefetchS...  52.3 us
    all_to_all x1, waiting for transfers between devices, on_device(): lax.all_to_all(terms.reshape(nz * ny, nx * 20, 128), ('z', 'y'), 0, 0, ti...  28.7 us
    all_to_all x1, waiting for transfers between devices, on_device(): own = lax.all_to_all(sent, SP, 0, 0, tiled=True).reshape(spans * 40, part)  27.6 us
    all_gather x1, blocking collectives, on_device(): total_grad = lax.all_gather(slice_grad, TP, axis=0)  19 us
    all_to_all x1, blocking collectives, on_device(): group = lax.all_to_all(group, 'z', 0, 0, tiled=True)  16.2 us
    all_to_all x1, starting transfers between devices, on_device(): own = lax.all_to_all(sent, SP, 0, 0, tiled=True).reshape(spans * 40, part)  13.6 us
    all_to_all x1, blocking collectives, on_device(): lax.all_to_all(summed.reshape(nx, nz * 24, 128), 'x', 0, 0, tiled=True)  10.3 us
    all_to_all x1, starting transfers between devices, on_device(): lax.all_to_all(terms.reshape(nz * ny, nx * 20, 128), ('z', 'y'), 0, 0, ti...  6.77 us
  transfers between devices with their start and end apart: 9, of which 5 were waited for; matrix products, arithmetic and copies ran while one was open for 0% of the time, Pallas kernels for 11%

profile of v3, /device:TPU:2, one launch (start us, length us, event | category | flops | bytes accessed | tf_op | source)
XLA Modules:
  0.0 223.1 jit_solution(7938870117613337476)
XLA Ops:
  0.6 1.4 and_select_fusion.at
  2.1 3.4 %dispatch.1.refs_5_ = bf16[32,40,512]{2,1,0:T(8,128)(2,1)} custom-call(s32[7]{0:T(128)} %and_select_fusion.at, s32[2,128]{1,0:T(2,128)} %bitcast.55, f32[2,128]{1,0:T(2,128)} %bitcast.57, bf16[128,2048]{1,0:T(8,128)(2,1)} %refs_2_.6, bf16[128,2048]{1,0:T(8,128)(2,1)} %refs_2_.11), custom_call_target="tpu_custom_call" | custom-call | tf_op jit(solution)/shard_map/dispatch/pallas_call | solution.py:69
  5.5 13.6 %all-to-all-start = ((bf16[32,40,512]{2,1,0:T(8,128)(2,1)}), bf16[32,40,512]{2,1,0:T(8,128)(2,1)S(1)}, u32[]{:S(2)}, u32[]{:S(2)}) async-start(bf16[32,40,512]{2,1,0:T(8,128)(2,1)} %dispatch.1.refs_5_), calls=%async_computation | async-start | bytes 2621440 | tf_op jit(solution)/shard_map/all_to_all | solution.py:511
  19.1 0.1 pad_maximum_fusion
  19.2 0.1 dynamic-slice_bitcast_fusion
  19.3 1.9 collective-permute-start
  21.2 3.1 %forward.1 = (bf16[128,128]{1,0:T(8,128)(2,1)}, bf16[128,128]{1,0:T(8,128)(2,1)}, f32[64,128]{1,0:T(8,128)}, f32[64,128]{1,0:T(8,128)}, bf16[8,128]{1,0:T(8,128)(2,1)}) custom-call(s32[7]{0:T(128)} %and_select_fusion.at, bf16[64,128]{1,0:T(8,128)(2,1)} %bitcast.48, bf16[64,128]{1,0:T(8,128)(2,1)} %bitcast.51, bf16[128,128]{1,0:T(8,128)(2,1)} %bitcast.45, ...), custom_call_target="tpu_custom_call" | custom-call | tf_op jit(solution)/shard_map/forward/pallas_call | solution.py:69
  24.3 0.0 collective-permute-done.refs_3_
  24.3 27.6 %all-to-all-done = bf16[32,40,512]{2,1,0:T(8,128)(2,1)S(1)} async-done(((bf16[32,40,512]{2,1,0:T(8,128)(2,1)}), bf16[32,40,512]{2,1,0:T(8,128)(2,1)S(1)}, u32[]{:S(2)}, u32[]{:S(2)}) %all-to-all-start) | async-done | bytes 1310752 | tf_op jit(solution)/shard_map/all_to_all | solution.py:511
  52.0 1.9 collective-permute-start.3
  53.9 0.1 fusion
  54.0 0.0 copy-done.10
  54.0 0.0 copy-done
  54.0 5.4 %collective-permute-start.2 = (bf16[640,512]{1,0:T(8,128)(2,1)S(1)}, bf16[640,512]{1,0:T(8,128)(2,1)S(1)}, u32[]{:S(2)}, u32[]{:S(2)}) collective-permute-start(bf16[640,512]{1,0:T(8,128)(2,1)S(1)} %get-tuple-element.76), channel_id=1, source_target_pairs={{0,14},{2,0},{4,2},{6,4},{8,6},{10,8},{12,10},{14,12},{1,15},{3,1}... | collective-permute-start | bytes 1966088 | tf_op jit(solution)/shard_map/ppermute | solution.py:541
  59.4 1.9 collective-permute-start.1
  61.3 0.0 collective-permute-done.3.refs_1_.refs_2_
  61.4 1.1 copy-done.4
  62.4 5.8 %first.1 = (f32[1280,256]{1,0:T(8,128)}, f32[1280,128]{1,0:T(8,128)}) custom-call(s32[7]{0:T(128)} %and_select_fusion.at, bf16[1280,512]{1,0:T(8,128)(2,1)} %bitcast.36, bf16[1280,512]{1,0:T(8,128)(2,1)} %copy-done.4, bf16[1,2048,128]{2,1,0:T(8,128)(2,1)} %refs_1_.2, bf16[1,2048,128]{2,1,0:T(8,128)(2,1)} %refs_2_.10, bf16[1,128,2048]{2,1,0:T(8,128)(2,1)} %refs_4_.7, ...), custom_call_target="tpu_custom_call" | custom-call | tf_op jit(solution)/shard_map/first/pallas_call | solution.py:69
  68.2 5.9 %collective-permute-done.2.refs_1_.refs_4_ = bf16[640,512]{1,0:T(8,128)(2,1)S(1)} collective-permute-done((bf16[640,512]{1,0:T(8,128)(2,1)S(1)}, bf16[640,512]{1,0:T(8,128)(2,1)S(1)}, u32[]{:S(2)}, u32[]{:S(2)}) %collective-permute-start.2) | collective-permute-done | bytes 655392 | tf_op jit(solution)/shard_map/ppermute | solution.py:541
  74.0 5.3 %collective-permute-done.1.refs_0_.refs_3_ = bf16[640,512]{1,0:T(8,128)(2,1)S(1)} collective-permute-done((bf16[640,512]{1,0:T(8,128)(2,1)S(1)}, bf16[640,512]{1,0:T(8,128)(2,1)S(1)}, u32[]{:S(2)}, u32[]{:S(2)}) %collective-permute-start.1) | collective-permute-done | bytes 655392 | tf_op jit(solution)/shard_map/ppermute | solution.py:540
  79.4 1.9 collective-permute-start.4
  81.3 2.4 %collective-permute-start.5 = (bf16[640,512]{1,0:T(8,128)(2,1)S(1)}, bf16[640,512]{1,0:T(8,128)(2,1)S(1)}, u32[]{:S(2)}, u32[]{:S(2)}) collective-permute-start(bf16[640,512]{1,0:T(8,128)(2,1)S(1)} %collective-permute-done.2.refs_1_.refs_4_), channel_id=1, source_target_pairs={{0,1},{1,0},{2,3},{3,2},{4,5},{5,4},{6,7},{7,6},{8,9},{9,8},{10,11... | collective-permute-start | bytes 1966088 | tf_op jit(solution)/shard_map/ppermute | solution.py:580
  83.7 0.0 copy-done.5
  83.7 0.0 copy-done.6
  83.7 5.5 %second.1 = (f32[1280,256]{1,0:T(8,128)}, f32[1280,128]{1,0:T(8,128)}) custom-call(s32[7]{0:T(128)} %and_select_fusion.at, bf16[640,512]{1,0:T(8,128)(2,1)} %copy-done.6, bf16[640,512]{1,0:T(8,128)(2,1)} %copy-done.5, bf16[1,2048,128]{2,1,0:T(8,128)(2,1)} %refs_1_.2, bf16[1,2048,128]{2,1,0:T(8,128)(2,1)} %refs_2_.10, bf16[1,128,2048]{2,1,0:T(8,128)(2,1)} %refs_4_.7, ...), custom_call_target="tpu_custom_call" | custom-call | tf_op jit(solution)/shard_map/second/pallas_call | solution.py:69
  89.2 0.0 collective-permute-done.4.refs_0_.refs_5_
  89.2 0.0 collective-permute-done.5.refs_1_.refs_6_
  89.2 0.8 copy-done.7
  90.1 0.2 copy-done.8
  90.3 5.3 %deltas.1 = (bf16[1280,384]{1,0:T(8,128)(2,1)}, bf16[640,256]{1,0:T(8,128)(2,1)}) custom-call(s32[7]{0:T(128)} %and_select_fusion.at, bf16[640,512]{1,0:T(8,128)(2,1)} %copy-done.7, bf16[640,512]{1,0:T(8,128)(2,1)} %copy-done.8, bf16[1,2048,128]{2,1,0:T(8,128)(2,1)} %refs_1_.2, bf16[1,2048,128]{2,1,0:T(8,128)(2,1)} %refs_2_.10, ...), custom_call_target="tpu_custom_call" | custom-call | tf_op jit(solution)/shard_map/deltas/pallas_call | solution.py:69
  95.7 4.0 %all-gather = bf16[1280,256]{1,0:T(8,128)(2,1)} all-gather(bf16[640,256]{1,0:T(8,128)(2,1)} %get-tuple-element.53), channel_id=2, replica_groups=mesh['z'=8,'x'=4,'y'=8,'c'=2] {'c'}, dimensions={0}, use_global_device_ids=true | all-gather | bytes 983040 | tf_op jit(solution)/shard_map/all_gather | solution.py:624
  99.6 4.2 %partials.1.refs_7_ = bf16[8,8,80,128]{3,2,1,0:T(8,128)(2,1)} custom-call(s32[7]{0:T(128)} %and_select_fusion.at, bf16[2,640,256]{2,1,0:T(8,128)(2,1)} %bitcast.40, bf16[1,2048,128]{2,1,0:T(8,128)(2,1)} %refs_1_.2, bf16[1,2048,128]{2,1,0:T(8,128)(2,1)} %refs_2_.10, bf16[2,8,128,128]{3,2,1,0:T(8,128)(2,1)} %copy-done.10), custom_call_target="tpu_custom_call" | custom-call | tf_op jit(solution)/shard_map/partials/pallas_call | solution.py:69
  103.8 6.8 %all-to-all-start.1 = ((bf16[64,80,128]{2,1,0:T(8,128)(2,1)}), bf16[64,80,128]{2,1,0:T(8,128)(2,1)S(1)}, u32[]{:S(2)}, u32[]{:S(2)}) async-start(bf16[64,80,128]{2,1,0:T(8,128)(2,1)} %bitcast.38), calls=%async_computation.1 | async-start | bytes 2621440 | tf_op jit(solution)/shard_map/all_to_all | solution.py:635
  110.5 7.1 %weights.1 = (bf16[1,2048,128]{2,1,0:T(8,128)(2,1)}, bf16[1,2048,128]{2,1,0:T(8,128)(2,1)}, bf16[1,128,2048]{2,1,0:T(8,128)(2,1)}) custom-call(s32[7]{0:T(128)} %and_select_fusion.at, bf16[1280,384]{1,0:T(8,128)(2,1)} %get-tuple-element.52.refs_0_, bf16[1280,512]{1,0:T(8,128)(2,1)} %bitcast.37, bf16[1280,512]{1,0:T(8,128)(2,1)} %copy-done.4, ...), custom_call_target="tpu_custom_call" | custom-call | tf_op jit(solution)/shard_map/weights/pallas_call | solution.py:69
  117.6 28.7 %all-to-all-done.1 = bf16[64,80,128]{2,1,0:T(8,128)(2,1)S(1)} async-done(((bf16[64,80,128]{2,1,0:T(8,128)(2,1)}), bf16[64,80,128]{2,1,0:T(8,128)(2,1)S(1)}, u32[]{:S(2)}, u32[]{:S(2)}) %all-to-all-start.1) | async-done | bytes 1310752 | tf_op jit(solution)/shard_map/all_to_all | solution.py:635
  146.4 1.1 copy-done.3
  147.5 2.8 %sums.1 = bf16[4,8,24,128]{3,2,1,0:T(8,128)(2,1)} custom-call(s32[7]{0:T(128)} %and_select_fusion.at, bf16[8,8,80,128]{3,2,1,0:T(8,128)(2,1)} %bitcast.39, bf16[1,128,2048]{2,1,0:T(8,128)(2,1)} %get-tuple-element.36.refs_1_), custom_call_target="tpu_custom_call" | custom-call | tf_op jit(solution)/shard_map/sums/pallas_call | solution.py:69
  150.3 10.3 %all_to_all.25 = bf16[4,192,128]{2,1,0:T(8,128)(2,1)} all-to-all(bf16[4,192,128]{2,1,0:T(8,128)(2,1)} %bitcast.43), channel_id=1, replica_groups=mesh['z'=8,'x'=4,'y'=8,'c'=2] {'x'}, dimensions={0} | all-to-all | bytes 393216 | tf_op jit(solution)/shard_map/all_to_all | solution.py:660
  160.6 2.8 %collect.1 = bf16[128,128]{1,0:T(8,128)(2,1)} custom-call(s32[7]{0:T(128)} %and_select_fusion.at, s32[2,128]{1,0:T(2,128)} %bitcast.56, bf16[4,8,24,128]{3,2,1,0:T(8,128)(2,1)} %bitcast.44, bf16[128,2048]{1,0:T(8,128)(2,1)} %refs_2_.11), custom_call_target="tpu_custom_call" | custom-call | tf_op jit(solution)/shard_map/collect/pallas_call | solution.py:69
  163.4 19.0 %all-gather.1 = bf16[2048,128]{1,0:T(8,128)(2,1)} all-gather(bf16[128,128]{1,0:T(8,128)(2,1)} %collect.1), channel_id=3, replica_groups=mesh['z'=8,'x'=4,'y'=8,'c'=2] {'y','c'}, dimensions={0}, use_global_device_ids=true | all-gather | bytes 557056 | tf_op jit(solution)/shard_map/all_gather | solution.py:671
  182.4 3.3 %head.1 = (bf16[128,128]{1,0:T(8,128)(2,1)}, bf16[4,584,128]{2,1,0:T(8,128)(2,1)}) custom-call(s32[7]{0:T(128)} %and_select_fusion.at, bf16[16,128,128]{2,1,0:T(8,128)(2,1)} %bitcast.42, bf16[2048,128]{1,0:T(8,128)(2,1)} %refs_1_.3, bf16[64,128]{1,0:T(8,128)(2,1)} %bitcast.49, f32[64,128]{1,0:T(8,128)} %get-tuple-element.58.refs_3_.refs_4_.refs_5_, ...), custom_call_target="tpu_custom_call" | custom-call | tf_op jit(solution)/shard_map/head/pallas_call | solution.py:69
  185.7 4.9 %all-to-all-start.3 = ((bf16[4,584,128]{2,1,0:T(8,128)(2,1)}), bf16[4,584,128]{2,1,0:T(8,128)(2,1)S(1)}, u32[]{:S(2)}, u32[]{:S(2)}) async-start(bf16[4,584,128]{2,1,0:T(8,128)(2,1)} %get-tuple-element.61.refs_7_), calls=%async_computation.3 | async-start | bytes 1196032 | tf_op jit(solution)/shard_map/all_to_all | solution.py:685
  190.6 3.2 %local.1 = (bf16[64,128]{1,0:T(8,128)(2,1)}, f32[64,128]{1,0:T(8,128)}, f32[64,128]{1,0:T(8,128)}, f32[128,128]{1,0:T(8,128)}) custom-call(s32[7]{0:T(128)} %and_select_fusion.at, bf16[128,128]{1,0:T(8,128)(2,1)} %get-tuple-element.62.refs_0_, bf16[64,128]{1,0:T(8,128)(2,1)} %bitcast.50, bf16[64,128]{1,0:T(8,128)(2,1)} %bitcast.52, ...), custom_call_target="tpu_custom_call" | custom-call | tf_op jit(solution)/shard_map/local/pallas_call | solution.py:69
  193.9 6.4 %all-to-all-done.3.refs_0_ = bf16[4,584,128]{2,1,0:T(8,128)(2,1)S(1)} async-done(((bf16[4,584,128]{2,1,0:T(8,128)(2,1)}), bf16[4,584,128]{2,1,0:T(8,128)(2,1)S(1)}, u32[]{:S(2)}, u32[]{:S(2)}) %all-to-all-start.3) | async-done | bytes 598048 | tf_op jit(solution)/shard_map/all_to_all | solution.py:685
  200.2 0.9 copy-done.9
  201.1 2.7 %group.1 = (f32[64,128]{1,0:T(8,128)}, f32[8,128]{1,0:T(8,128)}, bf16[8,136,128]{2,1,0:T(8,128)(2,1)}) custom-call(s32[7]{0:T(128)} %and_select_fusion.at, bf16[4,584,128]{2,1,0:T(8,128)(2,1)} %copy-done.9, f32[64,128]{1,0:T(8,128)} %get-tuple-element.64.refs_1_.refs_7_), custom_call_target="tpu_custom_call" | custom-call | tf_op jit(solution)/shard_map/group/pallas_call | solution.py:69
  203.8 16.2 %all_to_all.26.refs_0_ = bf16[8,136,128]{2,1,0:T(8,128)(2,1)} all-to-all(bf16[8,136,128]{2,1,0:T(8,128)(2,1)} %get-tuple-element.65), channel_id=1, replica_groups=mesh['z'=8,'x'=4,'y'=8,'c'=2] {'z'}, dimensions={0} | all-to-all | bytes 557056 | tf_op jit(solution)/shard_map/all_to_all | solution.py:717
  220.0 3.1 %last.1 = (f32[64,128]{1,0:T(8,128)}, bf16[64,128]{1,0:T(8,128)(2,1)}, bf16[128,128]{1,0:T(8,128)(2,1)}, f32[64,128]{1,0:T(8,128)}) custom-call(s32[7]{0:T(128)} %and_select_fusion.at, bf16[8,136,128]{2,1,0:T(8,128)(2,1)} %all_to_all.26.refs_0_, f32[64,128]{1,0:T(8,128)} %get-tuple-element.66.refs_1_, f32[8,128]{1,0:T(8,128)} %get-tuple-element.67.refs_2_, ...), custom_call_target="tpu_custom_call" | custom-call | tf_op jit(solution)/shard_map/last/pallas_call | solution.py:69
  (13 shorter events, 0.0 us)
Async XLA Ops:
  5.5 13.6 %copy-start.1 = (bf16[1,2048,128]{2,1,0:T(8,128)(2,1)S(1)}, bf16[1,2048,128]{2,1,0:T(8,128)(2,1)}, u32[]{:S(2)}) copy-start(bf16[1,2048,128]{2,1,0:T(8,128)(2,1)} %refs_1_.2) | copy-start | bytes 1572868
  5.5 13.6 %copy-start.2 = (bf16[1,2048,128]{2,1,0:T(8,128)(2,1)S(1)}, bf16[1,2048,128]{2,1,0:T(8,128)(2,1)}, u32[]{:S(2)}) copy-start(bf16[1,2048,128]{2,1,0:T(8,128)(2,1)} %refs_2_.10) | copy-start | bytes 1572868
  5.5 46.5 %all-to-all-start = ((bf16[32,40,512]{2,1,0:T(8,128)(2,1)}), bf16[32,40,512]{2,1,0:T(8,128)(2,1)S(1)}, u32[]{:S(2)}, u32[]{:S(2)}) async-start(bf16[32,40,512]{2,1,0:T(8,128)(2,1)} %dispatch.1.refs_5_), calls=%async_computation | async-start | bytes 2621440 | tf_op jit(solution)/shard_map/all_to_all | solution.py:511
  19.3 5.1 %collective-permute-start = (bf16[2,8,128,128]{3,2,1,0:T(8,128)(2,1)S(1)}, bf16[2,8,128,128]{3,2,1,0:T(8,128)(2,1)S(1)}, u32[]{:S(2)}, u32[]{:S(2)}) collective-permute-start(bf16[2,8,128,128]{3,2,1,0:T(8,128)(2,1)S(1)} %dynamic-slice_bitcast_fusion), channel_id=1, source_target_pairs={{0,1},{1,0},{2,3},{3,2},{4,5},{5,4},{6,7},{7,6},{8,9},{9,8},{10,11... | collective-permute-start | bytes 1572872 | tf_op jit(solution)/shard_map/ppermute | solution.py:515
  24.3 29.7 %copy-start.10 = (bf16[2,8,128,128]{3,2,1,0:T(8,128)(2,1)}, bf16[2,8,128,128]{3,2,1,0:T(8,128)(2,1)S(1)}, u32[]{:S(2)}) copy-start(bf16[2,8,128,128]{3,2,1,0:T(8,128)(2,1)S(1)} %collective-permute-done.refs_3_) | copy-start | bytes 1572868
  52.0 2.0 copy-start
  52.0 9.3 %collective-permute-start.3 = (bf16[1280,512]{1,0:T(8,128)(2,1)S(1)}, bf16[1280,512]{1,0:T(8,128)(2,1)S(1)}, u32[]{:S(2)}, u32[]{:S(2)}) collective-permute-start(bf16[1280,512]{1,0:T(8,128)(2,1)S(1)} %bitcast.34), channel_id=1, source_target_pairs={{0,1},{1,0},{2,3},{3,2},{4,5},{5,4},{6,7},{7,6},{8,9},{9,8},{10,11... | collective-permute-start | bytes 3932168 | tf_op jit(solution)/shard_map/ppermute | solution.py:542
  54.0 20.0 %collective-permute-start.2 = (bf16[640,512]{1,0:T(8,128)(2,1)S(1)}, bf16[640,512]{1,0:T(8,128)(2,1)S(1)}, u32[]{:S(2)}, u32[]{:S(2)}) collective-permute-start(bf16[640,512]{1,0:T(8,128)(2,1)S(1)} %get-tuple-element.76), channel_id=1, source_target_pairs={{0,14},{2,0},{4,2},{6,4},{8,6},{10,8},{12,10},{14,12},{1,15},{3,1}... | collective-permute-start | bytes 1966088 | tf_op jit(solution)/shard_map/ppermute | solution.py:541
  59.4 20.0 %collective-permute-start.1 = (bf16[640,512]{1,0:T(8,128)(2,1)S(1)}, bf16[640,512]{1,0:T(8,128)(2,1)S(1)}, u32[]{:S(2)}, u32[]{:S(2)}) collective-permute-start(bf16[640,512]{1,0:T(8,128)(2,1)S(1)} %get-tuple-element.77), channel_id=1, source_target_pairs={{0,2},{2,4},{4,6},{6,8},{8,10},{10,12},{12,14},{14,0},{1,3},{3,5},... | collective-permute-start | bytes 1966088 | tf_op jit(solution)/shard_map/ppermute | solution.py:540
  61.4 1.1 copy-start.4
  74.0 9.7 %copy-start.5 = (bf16[640,512]{1,0:T(8,128)(2,1)}, bf16[640,512]{1,0:T(8,128)(2,1)S(1)}, u32[]{:S(2)}) copy-start(bf16[640,512]{1,0:T(8,128)(2,1)S(1)} %collective-permute-done.2.refs_1_.refs_4_) | copy-start | bytes 1966084
  79.4 4.3 %copy-start.6 = (bf16[640,512]{1,0:T(8,128)(2,1)}, bf16[640,512]{1,0:T(8,128)(2,1)S(1)}, u32[]{:S(2)}) copy-start(bf16[640,512]{1,0:T(8,128)(2,1)S(1)} %collective-permute-done.1.refs_0_.refs_3_) | copy-start | bytes 1966084
  79.4 9.8 %collective-permute-start.4 = (bf16[640,512]{1,0:T(8,128)(2,1)S(1)}, bf16[640,512]{1,0:T(8,128)(2,1)S(1)}, u32[]{:S(2)}, u32[]{:S(2)}) collective-permute-start(bf16[640,512]{1,0:T(8,128)(2,1)S(1)} %collective-permute-done.1.refs_0_.refs_3_), channel_id=1, source_target_pairs={{0,1},{1,0},{2,3},{3,2},{4,5},{5,4},{6,7},{7,6},{8,9},{9,8},{10,11... | collective-permute-start | bytes 1966088 | tf_op jit(solution)/shard_map/ppermute | solution.py:579
  81.3 7.9 %collective-permute-start.5 = (bf16[640,512]{1,0:T(8,128)(2,1)S(1)}, bf16[640,512]{1,0:T(8,128)(2,1)S(1)}, u32[]{:S(2)}, u32[]{:S(2)}) collective-permute-start(bf16[640,512]{1,0:T(8,128)(2,1)S(1)} %collective-permute-done.2.refs_1_.refs_4_), channel_id=1, source_target_pairs={{0,1},{1,0},{2,3},{3,2},{4,5},{5,4},{6,7},{7,6},{8,9},{9,8},{10,11... | collective-permute-start | bytes 1966088 | tf_op jit(solution)/shard_map/ppermute | solution.py:580
  89.2 0.9 copy-start.7
  89.2 1.1 copy-start.8
  103.8 42.6 %all-to-all-start.1 = ((bf16[64,80,128]{2,1,0:T(8,128)(2,1)}), bf16[64,80,128]{2,1,0:T(8,128)(2,1)S(1)}, u32[]{:S(2)}, u32[]{:S(2)}) async-start(bf16[64,80,128]{2,1,0:T(8,128)(2,1)} %bitcast.38), calls=%async_computation.1 | async-start | bytes 2621440 | tf_op jit(solution)/shard_map/all_to_all | solution.py:635
  146.4 1.1 copy-start.3
  185.7 14.5 %all-to-all-start.3 = ((bf16[4,584,128]{2,1,0:T(8,128)(2,1)}), bf16[4,584,128]{2,1,0:T(8,128)(2,1)S(1)}, u32[]{:S(2)}, u32[]{:S(2)}) async-start(bf16[4,584,128]{2,1,0:T(8,128)(2,1)} %get-tuple-element.61.refs_7_), calls=%async_computation.3 | async-start | bytes 1196032 | tf_op jit(solution)/shard_map/all_to_all | solution.py:685
  200.2 0.9 copy-start.9

commit v4 on v3

--- a/solution.py
+++ b/solution.py
@@ -15,6 +15,9 @@
 HI = lax.Precision.HIGHEST
 BLOCK = 32
 LIMIT = 56 * 1024 * 1024
+SMALL = 20 * 1024 * 1024
+LEAN = ('first', 'deltas', 'partials', 'sums', 'collect', 'head', 'local', 'group', 'last')
+TILES = 2
 
 
 def dot(a, b, precision=None):
@@ -37,10 +40,6 @@
 
 def iota(shape, dim):
     return lax.broadcasted_iota(jnp.int32, shape, dim)
-
-
-def params(**kw):
-    return pltpu.CompilerParams(vmem_limit_bytes=LIMIT, **kw)
 
 
 def call(
@@ -77,7 +76,9 @@
             out_specs=out_specs,
             scratch_shapes=list(scratch),
         ),
-        compiler_params=params(),
+        compiler_params=pltpu.CompilerParams(
+            vmem_limit_bytes=(SMALL if name in LEAN else LIMIT)
+        ),
     )(scalars, *args, *after)
 
 
@@ -149,37 +150,36 @@
     return jnp.concatenate([a[4:8], a[0:4]], axis=0)
 
 
-def products(g, wg_ref, wu_ref, wd_ref):
-    return dot(g, jnp.concatenate([wg_ref[0], wu_ref[0]], axis=1)), dot_nt(g, wd_ref[0])
-
-
-def first_kernel(at, a_ref, b_ref, *refs):
-    gu0, yh0 = products(a_ref[...], *refs[0:3])
-    gu1, yh1 = products(b_ref[...], *refs[3:6])
-    refs[6][...] = gu0 + gu1
-    refs[7][...] = yh0 + yh1
-
-
-def chosen(low_ref, high_ref):
-    upper = pl.program_id(0) >= pl.num_programs(0) // 2
-    return jnp.where(upper, high_ref[...], low_ref[...])
-
-
-def second_kernel(at, low_ref, high_ref, wg_ref, wu_ref, wd_ref, gu_ref, yh_ref, gu_out, yh_out):
-    gu, yh = products(chosen(low_ref, high_ref), wg_ref, wu_ref, wd_ref)
-    gu_out[...] = gu + gu_ref[...]
-    yh_out[...] = yh + yh_ref[...]
-
-
-def delta_kernel(at, low_ref, high_ref, wg_ref, wu_ref, wd_ref, gu_ref, yh_ref, delta_ref, pack_ref):
-    gu, yh = products(chosen(low_ref, high_ref), wg_ref, wu_ref, wd_ref)
-    gu = gu + gu_ref[...]
-    yh = yh + yh_ref[...]
+def layout_kernel(at, wg_ref, wu_ref, wd_ref, woth_ref, side_ref, back_ref):
+    side_ref[:, 0:128] = wg_ref[0]
+    side_ref[:, 128:256] = wu_ref[0]
+    for t in range(0, side_ref.shape[0], 128):
+        side_ref[t : t + 128, 256:384] = wd_ref[0, :, t : t + 128].astype(F32).T.astype(BF)
+    for y in range(back_ref.shape[1] // 128):
+        first = pl.multiple_of((2 * y + at[1]) * 128, 128)
+        for n, w in enumerate(
+            (
+                wg_ref[0, pl.ds(first, 128), :],
+                wu_ref[0, pl.ds(first, 128), :],
+                woth_ref[0, y],
+                woth_ref[1, y],
+            )
+        ):
+            back_ref[128 * n : 128 * n + 128, 128 * y : 128 * y + 128] = w.astype(F32).T.astype(BF)
+
+
+def first_kernel(at, g_ref, w_ref, out_ref):
+    out_ref[...] = dot(g_ref[...], w_ref[...])
+
+
+def delta_kernel(at, g_ref, w_ref, acc_ref, delta_ref, pack_ref):
+    sums = dot(g_ref[...], w_ref[...]) + acc_ref[...]
+    gu, yh = sums[:, 0:256], sums[:, 256:384]
     low = iota((8, 128), 0) < 4
     zero8 = jnp.zeros((8, 128), F32)
     dgs, dus, dhs, pgs, pus = [], [], [], [], []
     mixed = []
-    spans = low_ref.shape[0] // 40
+    spans = g_ref.shape[0] // 40
     for d in range(spans):
         b = 40 * d
         pg, pu = gu[b : b + 24, 0:128], gu[b : b + 24, 128:256]
@@ -208,52 +208,29 @@
     pack_ref[:, 128:256] = jnp.concatenate(pus, axis=0).astype(BF)
 
 
-def partial_kernel(at, pack_ref, wg_ref, wu_ref, woth_ref, out_ref):
+def partial_kernel(at, pack_ref, back_ref, out_ref):
     core = at[1]
+    nz, ny, rows, _ = out_ref.shape
     lhs = jnp.concatenate([pack_ref[core], pack_ref[1 - core]], axis=1)
-    nz, ny, rows, _ = out_ref.shape
     for y in range(0, ny, 2):
-        sides = []
-        for v in (y, y + 1):
-            first = pl.multiple_of((2 * v + core) * 128, 128)
-            sides.append(
-                jnp.concatenate(
-                    [
-                        wg_ref[0, pl.ds(first, 128), :],
-                        wu_ref[0, pl.ds(first, 128), :],
-                        woth_ref[0, v],
-                        woth_ref[1, v],
-                    ],
-                    axis=1,
-                )
-            )
-        o = dot_nt(lhs, jnp.concatenate(sides, axis=0)).astype(BF)
+        o = dot(lhs, back_ref[:, 128 * y : 128 * y + 256]).astype(BF)
         for z in range(nz):
             out_ref[z, y] = o[z * rows : (z + 1) * rows, 0:128]
             out_ref[z, y + 1] = o[z * rows : (z + 1) * rows, 128:256]
 
 
-def weight_kernel(at, delta_ref, a_ref, b_ref, c0_ref, c1_ref, d0_ref, d1_ref, gate_ref, up_ref, down_ref, dt_ref):
-    rows, part = a_ref.shape
+def weight_kernel(at, delta_ref, own_ref, other_ref, gate_ref, up_ref, down_ref, token_ref, dt_ref):
+    token_ref[...] = jnp.zeros(token_ref.shape, F32)
+    rows, half = own_ref.shape
     for r in range(0, rows, 128):
         dt_ref[:, r : r + 128] = delta_ref[r : r + 128, :].astype(F32).T.astype(BF)
-    core, side = at[1], at[6]
-    for refs, quarter in (
-        ((a_ref,), 2 * side + core),
-        ((b_ref,), 2 * side + 1 - core),
-        ((c0_ref, c1_ref), 2 * (1 - side) + core),
-        ((d0_ref, d1_ref), 2 * (1 - side) + 1 - core),
-    ):
-        size = rows // len(refs)
-        for p in range(0, part, 256):
-            o = dot(dt_ref[:, 0:size], refs[0][:, p : p + 256])
-            for n in range(1, len(refs)):
-                o = o + dot(dt_ref[:, n * size : (n + 1) * size], refs[n][:, p : p + 256])
-            at_row = pl.multiple_of(quarter * part + p, 128)
-            wide = min(256, part - p)
-            gate_ref[0, pl.ds(at_row, wide), :] = o[0:128].T.astype(BF)
-            up_ref[0, pl.ds(at_row, wide), :] = o[128:256].T.astype(BF)
-            down_ref[0, :, pl.ds(at_row, wide)] = o[256:384].astype(BF)
+    for g_ref, core in ((own_ref, at[1]), (other_ref, 1 - at[1])):
+        for p in range(0, half, 256):
+            o = dot(dt_ref[...], g_ref[:, p : p + 256])
+            first = pl.multiple_of(core * half + p, 256)
+            gate_ref[0, pl.ds(first, 256), :] = o[0:128].T.astype(BF)
+            up_ref[0, pl.ds(first, 256), :] = o[128:256].T.astype(BF)
+            down_ref[0, :, pl.ds(first, 256)] = o[256:384].astype(BF)
 
 
 def sum_kernel(at, got_ref, out_ref):
@@ -494,21 +471,21 @@
     v = value_rows.reshape(tokens, 128)
     g = log_decay.reshape(tokens, width).T
     slice_block = ((tokens, 128), lambda i, s: (0, s[0]))
-    part = slices * 32
-    part_block = ((tokens, part), lambda i, s: (0, 2 * s[6] + s[1]))
+    half = slices * 64
+    half_block = ((tokens, half), lambda i, s: (0, s[1]))
 
     (sent,) = call(
         dispatch_kernel,
         "dispatch",
-        (sds((spans, 40, part), BF),),
+        (sds((spans, 40, half), BF),),
         at,
         routes,
         route_weight,
         expert_input,
         cotangent,
-        blocks={2: part_block, 3: part_block},
-    )
-    own = lax.all_to_all(sent, SP, 0, 0, tiled=True).reshape(spans * 40, part)
+        blocks={2: half_block, 3: half_block},
+    )
+    own = lax.all_to_all(sent, SP, 0, 0, tiled=True).reshape(spans * 40, half)
 
     weights = jnp.stack([gate_weight[0], up_weight[0]]).reshape(2, ny, 2, 128, 128)
     weights = lax.dynamic_index_in_dim(weights, 1 - core, 2, keepdims=False)
@@ -531,95 +508,50 @@
         start_state,
         after=(sent,),
     )
-    own, mixed, weights = lax.optimization_barrier((own, mixed, weights))
-
-    swap = [(0, 1), (1, 0)]
+    side, back = call(
+        layout_kernel,
+        "layout",
+        (sds((slices * 128, 384), BF), sds((512, half), BF)),
+        at,
+        gate_weight,
+        up_weight,
+        down_weight,
+        weights,
+        after=(mixed,),
+    )
+    own, mixed, side = lax.optimization_barrier((own, mixed, side))
+
+    other = lax.ppermute(own, "c", [(0, 1), (1, 0)])
     rows_all = spans * 40
-    up = [(i, (i + 1) % ny) for i in range(ny)]
-    down = [(i, (i - 1) % ny) for i in range(ny)]
-    low = lax.ppermute(own[: rows_all // 2], "y", up)
-    high = lax.ppermute(own[rows_all // 2 :], "y", down)
-    beside = lax.ppermute(own, "c", swap)
-
-    tiles = spans // 8
-    last_low = tiles // 2 - 1
-    rows_block = ((320, part), lambda i, s: (i, 0))
-    low_block = ((320, part), lambda i, s: (jnp.minimum(i, last_low), 0))
-    high_block = ((320, part), lambda i, s: (jnp.maximum(i - last_low - 1, 0), 0))
-    acc_blocks = (((320, 256), lambda i, s: (i, 0)), ((320, 128), lambda i, s: (i, 0)))
-    acc = (sds((rows_all, 256), F32), sds((rows_all, 128), F32))
-
-    def weight_blocks(first, quarter):
-        return {
-            first: ((1, part, 128), lambda i, s: (0, quarter(s), 0)),
-            first + 1: ((1, part, 128), lambda i, s: (0, quarter(s), 0)),
-            first + 2: ((1, 128, part), lambda i, s: (0, 0, quarter(s))),
-        }
-
-    experts = (gate_weight, up_weight, down_weight)
-    gu, yh = call(
+    tile = rows_all // TILES
+    rows_block = ((tile, half), lambda i, s: (i, 0))
+    acc_block = ((tile, 384), lambda i, s: (i, 0))
+    (acc,) = call(
         first_kernel,
         "first",
-        acc,
+        (sds((rows_all, 384), F32),),
         at,
         own,
-        beside,
-        *experts,
-        *experts,
-        blocks={
-            0: rows_block,
-            1: rows_block,
-            **weight_blocks(2, lambda s: 2 * s[6] + s[1]),
-            **weight_blocks(5, lambda s: 2 * s[6] + 1 - s[1]),
-        },
-        out_blocks={0: acc_blocks[0], 1: acc_blocks[1]},
-        grid=tiles,
-    )
-    low, high, gu, yh = lax.optimization_barrier((low, high, gu, yh))
-    low_beside = lax.ppermute(low, "c", swap)
-    high_beside = lax.ppermute(high, "c", swap)
-    gu, yh = call(
-        second_kernel,
-        "second",
-        acc,
-        at,
-        low,
-        high,
-        *experts,
-        gu,
-        yh,
-        blocks={
-            0: low_block,
-            1: high_block,
-            **weight_blocks(2, lambda s: 2 * (1 - s[6]) + s[1]),
-            5: acc_blocks[0],
-            6: acc_blocks[1],
-        },
-        out_blocks={0: acc_blocks[0], 1: acc_blocks[1]},
-        grid=tiles,
+        side,
+        blocks={0: rows_block, 1: ((half, 384), lambda i, s: (s[1], 0))},
+        out_blocks={0: acc_block},
+        grid=TILES,
     )
     delta, pack = call(
         delta_kernel,
         "deltas",
         (sds((rows_all, 384), BF), sds((rows_all // 2, 256), BF)),
         at,
-        low_beside,
-        high_beside,
-        *experts,
-        gu,
-        yh,
+        other,
+        side,
+        acc,
         blocks={
-            0: low_block,
-            1: high_block,
-            **weight_blocks(2, lambda s: 2 * (1 - s[6]) + 1 - s[1]),
-            5: acc_blocks[0],
-            6: acc_blocks[1],
+            0: rows_block,
+            1: ((half, 384), lambda i, s: (1 - s[1], 0)),
+            2: acc_block,
         },
-        out_blocks={
-            0: ((320, 384), lambda i, s: (i, 0)),
-            1: ((160, 256), lambda i, s: (i, 0)),
-        },
-        grid=tiles,
+        out_blocks={0: acc_block, 1: ((tile // 2, 256), lambda i, s: (i, 0))},
+        grid=TILES,
     )
     packs = lax.all_gather(pack, "c", axis=0)
     (terms,) = call(
@@ -628,34 +560,29 @@
         (sds((nz, ny, nx * 20, 128), BF),),
         at,
         packs,
-        gate_weight,
-        up_weight,
-        weights,
+        back,
     )
     got = lax.all_to_all(
         terms.reshape(nz * ny, nx * 20, 128), ("z", "y"), 0, 0, tiled=True
     ).reshape(nz, ny, nx * 20, 128)
-    gate_grad, up_grad, down_grad = call(
+    gate_grad, up_grad, down_grad, token = call(
         weight_kernel,
         "weights",
         (
             sds((1, slices * 128, 128), BF),
             sds((1, slices * 128, 128), BF),
             sds((1, 128, slices * 128), BF),
+            sds((8, 128), F32),
         ),
         at,
         delta,
         own,
-        beside,
-        low,
-        high,
-        low_beside,
-        high_beside,
+        other,
         scratch=[pltpu.VMEM((384, spans * 40), BF)],
         after=(terms,),
     )
     (summed,) = call(
-        sum_kernel, "sums", (sds((nx, nz, 24, 128), BF),), at, got, after=(down_grad,)
+        sum_kernel, "sums", (sds((nx, nz, 24, 128), BF),), at, got, after=(token,)
     )
     returned = lax.all_to_all(summed.reshape(nx, nz * 24, 128), "x", 0, 0, tiled=True)
     (slice_grad,) = call(

time: 225 us -> 205 us (0.911)
  Pallas kernels: 52.3 us -> 34.6 us
  waiting for transfers between devices: 73.9 us -> 85.8 us
  starting transfers between devices: 40.7 us -> 33.1 us
  blocking collectives: 49.5 us -> 44.4 us
    all_to_all x1, waiting for transfers between devices: 27.6 us -> 48.6 us  [on_device(): own = lax.all_to_all(sent, SP, 0, 0, tiled=True).reshape(spans * 40, half)]
    pallas_call x13, Pallas kernels: 52.3 us -> 34.6 us  [call(): pl.pallas_call(body, name=name, out_shape=outs, grid_spec=pltpu.PrefetchS...]
    ppermute x5 -> x1, starting transfers between devices: 13.5 us -> 1.91 us  [on_device(): other = lax.ppermute(own, 'c', [(0, 1), (1, 0)])]
    ppermute x5 -> x1, waiting for transfers between devices: 11.2 us -> 1.16 us  [on_device(): other = lax.ppermute(own, 'c', [(0, 1), (1, 0)])]
    all_to_all x1, starting transfers between devices: 6.77 us -> 10.7 us  [on_device(): lax.all_to_all(terms.reshape(nz * ny, nx * 20, 128), ('z', 'y'), 0, 0, ti...]
  transfers between devices with their start and end apart: 9 -> 5, of which waited for: 5 -> 4; matrix products, arithmetic and copies ran while one was open for 0% -> 1% of each run, Pallas kernels for 11% -> 9%
where the time goes in v4:
time: 205 us; the launch traced here: 204 us
  waiting for transfers between devices  85.8 us (42%)
  blocking collectives  44.4 us (22%)
  Pallas kernels  34.6 us (17%)
  starting transfers between devices  33.1 us (16%)
  local copies, waits for them, and re-layouts  3.02 us (1%)
  other arithmetic  2.59 us (1%)
    all_to_all x1, waiting for transfers between devices, on_device(): own = lax.all_to_all(sent, SP, 0, 0, tiled=True).reshape(spans * 40, half)  48.6 us
    pallas_call x13, Pallas kernels, call(): pl.pallas_call(body, name=name, out_shape=outs, grid_spec=pltpu.PrefetchS...  34.6 us
    all_to_all x1, waiting for transfers between devices, on_device(): lax.all_to_all(terms.reshape(nz * ny, nx * 20, 128), ('z', 'y'), 0, 0, ti...  28.7 us
    all_gather x1, blocking collectives, on_device(): total_grad = lax.all_gather(slice_grad, TP, axis=0)  17.1 us
    all_to_all x1, blocking collectives, on_device(): group = lax.all_to_all(group, 'z', 0, 0, tiled=True)  15.7 us
    all_to_all x1, starting transfers between devices, on_device(): own = lax.all_to_all(sent, SP, 0, 0, tiled=True).reshape(spans * 40, half)  13.6 us
    all_to_all x1, starting transfers between devices, on_device(): lax.all_to_all(terms.reshape(nz * ny, nx * 20, 128), ('z', 'y'), 0, 0, ti...  10.7 us
    all_to_all x1, blocking collectives, on_device(): lax.all_to_all(summed.reshape(nx, nz * 24, 128), 'x', 0, 0, tiled=True)  9.3 us
  transfers between devices with their start and end apart: 5, of which 4 were waited for; matrix products, arithmetic and copies ran while one was open for 1% of the time, Pallas kernels for 9%

profile of v4, /device:TPU:2, one launch (start us, length us, event | category | flops | bytes accessed | tf_op | source)
XLA Modules:
  0.0 204.4 jit_solution(8927506857735844876)
XLA Ops:
  0.6 1.4 and_select_fusion.at
  2.1 4.2 %dispatch.1.refs_5_ = bf16[32,40,1024]{2,1,0:T(8,128)(2,1)} custom-call(s32[7]{0:T(128)} %and_select_fusion.at, s32[2,128]{1,0:T(2,128)} %bitcast.51, f32[2,128]{1,0:T(2,128)} %bitcast.55, bf16[128,2048]{1,0:T(8,128)(2,1)} %refs_2_.3, bf16[128,2048]{1,0:T(8,128)(2,1)} %refs_2_.5), custom_call_target="tpu_custom_call" | custom-call | tf_op jit(solution)/shard_map/dispatch/pallas_call | solution.py:68
  6.3 13.6 %all-to-all-start = ((bf16[32,40,1024]{2,1,0:T(8,128)(2,1)}), bf16[32,40,1024]{2,1,0:T(8,128)(2,1)S(1)}, u32[]{:S(2)}, u32[]{:S(2)}) async-start(bf16[32,40,1024]{2,1,0:T(8,128)(2,1)} %dispatch.1.refs_5_), calls=%async_computation | async-start | bytes 5242880 | tf_op jit(solution)/shard_map/all_to_all | solution.py:488
  19.9 1.1 pad_maximum_fusion
  21.1 1.9 collective-permute-start
  23.1 3.2 %forward.1 = (bf16[128,128]{1,0:T(8,128)(2,1)}, bf16[128,128]{1,0:T(8,128)(2,1)}, f32[64,128]{1,0:T(8,128)}, f32[64,128]{1,0:T(8,128)}, bf16[8,128]{1,0:T(8,128)(2,1)}) custom-call(s32[7]{0:T(128)} %and_select_fusion.at, bf16[64,128]{1,0:T(8,128)(2,1)} %bitcast.45, bf16[64,128]{1,0:T(8,128)(2,1)} %bitcast.48, bf16[128,128]{1,0:T(8,128)(2,1)} %bitcast.42, ...), custom_call_target="tpu_custom_call" | custom-call | tf_op jit(solution)/shard_map/forward/pallas_call | solution.py:68
  26.3 0.0 collective-permute-done.refs_3_
  26.3 0.8 copy-done.21
  27.1 4.3 %layout.1 = (bf16[2048,384]{1,0:T(8,128)(2,1)}, bf16[512,1024]{1,0:T(8,128)(2,1)}) custom-call(s32[7]{0:T(128)} %and_select_fusion.at, bf16[1,2048,128]{2,1,0:T(8,128)(2,1)} %refs_0_.1, bf16[1,2048,128]{2,1,0:T(8,128)(2,1)} %refs_1_.2, bf16[1,128,2048]{2,1,0:T(8,128)(2,1)} %refs_2_.4, bf16[2,8,128,128]{3,2,1,0:T(8,128)(2,1)} %copy-done.21, ...), custom_call_target="tpu_custom_call" | custom-call | tf_op jit(solution)/shard_map/layout/pallas_call | solution.py:68
  31.4 48.6 %all-to-all-done = bf16[32,40,1024]{2,1,0:T(8,128)(2,1)S(1)} async-done(((bf16[32,40,1024]{2,1,0:T(8,128)(2,1)}), bf16[32,40,1024]{2,1,0:T(8,128)(2,1)S(1)}, u32[]{:S(2)}, u32[]{:S(2)}) %all-to-all-start) | async-done | bytes 2621472 | tf_op jit(solution)/shard_map/all_to_all | solution.py:488
  80.0 1.9 collective-permute-start.1
  81.9 1.4 copy-done.2
  83.3 2.3 %first.1.refs_2_ = f32[1280,384]{1,0:T(8,128)S(1)} custom-call(s32[7]{0:T(128)S(1)} %copy-done.13, bf16[1280,1024]{1,0:T(8,128)(2,1)S(1)} %bitcast.35, bf16[2048,384]{1,0:T(8,128)(2,1)S(1)} %copy-done.2), custom_call_target="tpu_custom_call" | custom-call | tf_op jit(solution)/shard_map/first/pallas_call | solution.py:68
  85.6 1.2 collective-permute-done.1.refs_0_.refs_2_
  86.8 2.3 %deltas.1 = (bf16[1280,384]{1,0:T(8,128)(2,1)S(1)}, bf16[640,256]{1,0:T(8,128)(2,1)S(1)}) custom-call(s32[7]{0:T(128)S(1)} %copy-done.13, bf16[1280,1024]{1,0:T(8,128)(2,1)S(1)} %collective-permute-done.1.refs_0_.refs_2_, bf16[2048,384]{1,0:T(8,128)(2,1)S(1)} %copy-done.2, f32[1280,384]{1,0:T(8,128)S(1)} %first.1.refs_2_), custom_call_target="tpu_custom_call" | custom-call | tf_op jit(solution)/shard_map/deltas/pallas_call | solution.py:68
  89.1 2.3 %all-gather = bf16[1280,256]{1,0:T(8,128)(2,1)S(1)} all-gather(bf16[640,256]{1,0:T(8,128)(2,1)S(1)} %get-tuple-element.42), channel_id=2, replica_groups=mesh['z'=8,'x'=4,'y'=8,'c'=2] {'c'}, dimensions={0}, use_global_device_ids=true | all-gather | bytes 983040 | tf_op jit(solution)/shard_map/all_gather | solution.py:556
  91.4 2.5 %partials.1.refs_3_ = bf16[8,8,80,128]{3,2,1,0:T(8,128)(2,1)} custom-call(s32[7]{0:T(128)S(1)} %copy-done.13, bf16[2,640,256]{2,1,0:T(8,128)(2,1)S(1)} %bitcast.38, bf16[512,1024]{1,0:T(8,128)(2,1)S(1)} %copy-done.4), custom_call_target="tpu_custom_call" | custom-call | tf_op jit(solution)/shard_map/partials/pallas_call | solution.py:68
  93.9 10.7 %all-to-all-start.1 = ((bf16[64,80,128]{2,1,0:T(8,128)(2,1)}), bf16[64,80,128]{2,1,0:T(8,128)(2,1)S(1)}, u32[]{:S(2)}, u32[]{:S(2)}) async-start(bf16[64,80,128]{2,1,0:T(8,128)(2,1)} %bitcast.13), calls=%async_computation.1 | async-start | bytes 2621440 | tf_op jit(solution)/shard_map/all_to_all | solution.py:565
  104.6 0.0 copy-start.14
  104.6 0.0 copy-start.18
  104.6 0.0 copy-start.19
  104.6 7.1 %weights.1 = (bf16[1,2048,128]{2,1,0:T(8,128)(2,1)}, bf16[1,2048,128]{2,1,0:T(8,128)(2,1)}, bf16[1,128,2048]{2,1,0:T(8,128)(2,1)}, f32[8,128]{1,0:T(8,128)}) custom-call(s32[7]{0:T(128)} %and_select_fusion.at, bf16[1280,384]{1,0:T(8,128)(2,1)} %copy-done.5, bf16[1280,1024]{1,0:T(8,128)(2,1)} %bitcast.36, bf16[1280,1024]{1,0:T(8,128)(2,1)} %copy-done.1, ...), custom_call_target="tpu_custom_call" | custom-call | tf_op jit(solution)/shard_map/weights/pallas_call | solution.py:68
  111.7 0.0 copy-start.9
  111.7 0.0 copy-start.12
  111.8 28.7 %all-to-all-done.1 = bf16[64,80,128]{2,1,0:T(8,128)(2,1)S(1)} async-done(((bf16[64,80,128]{2,1,0:T(8,128)(2,1)}), bf16[64,80,128]{2,1,0:T(8,128)(2,1)S(1)}, u32[]{:S(2)}, u32[]{:S(2)}) %all-to-all-start.1) | async-done | bytes 1310752 | tf_op jit(solution)/shard_map/all_to_all | solution.py:565
  140.5 0.0 copy-done.14
  140.5 0.7 copy-done.17
  141.2 0.7 sums.1
  141.9 0.0 copy-start.7
  141.9 0.0 copy-start.10
  141.9 0.0 copy-start.11
  141.9 0.0 copy-start.16
  141.9 9.3 %all_to_all.25 = bf16[4,192,128]{2,1,0:T(8,128)(2,1)S(1)} all-to-all(bf16[4,192,128]{2,1,0:T(8,128)(2,1)S(1)} %bitcast.41), channel_id=1, replica_groups=mesh['z'=8,'x'=4,'y'=8,'c'=2] {'x'}, dimensions={0} | all-to-all | bytes 393216 | tf_op jit(solution)/shard_map/all_to_all | solution.py:587
  151.2 0.0 copy-done.18
  151.2 1.1 collect.1
  152.4 17.1 %all-gather.1 = bf16[2048,128]{1,0:T(8,128)(2,1)S(1)} all-gather(bf16[128,128]{1,0:T(8,128)(2,1)S(1)} %collect.1), channel_id=3, replica_groups=mesh['z'=8,'x'=4,'y'=8,'c'=2] {'y','c'}, dimensions={0}, use_global_device_ids=true | all-gather | bytes 557056 | tf_op jit(solution)/shard_map/all_gather | solution.py:598
  169.5 0.0 copy-done.19
  169.5 0.0 copy-done.8
  169.5 0.0 copy-start.15
  169.5 2.0 head.1
  171.5 4.9 %all-to-all-start.3 = ((bf16[4,584,128]{2,1,0:T(8,128)(2,1)}), bf16[4,584,128]{2,1,0:T(8,128)(2,1)S(1)}, u32[]{:S(2)}, u32[]{:S(2)}) async-start(bf16[4,584,128]{2,1,0:T(8,128)(2,1)} %get-tuple-element.51.refs_7_), calls=%async_computation.3 | async-start | bytes 1196032 | tf_op jit(solution)/shard_map/all_to_all | solution.py:612
  176.4 0.0 copy-done.7
  176.4 2.3 %local.1 = (bf16[64,128]{1,0:T(8,128)(2,1)}, f32[64,128]{1,0:T(8,128)S(1)}, f32[64,128]{1,0:T(8,128)S(1)}, f32[128,128]{1,0:T(8,128)S(1)}) custom-call(s32[7]{0:T(128)S(1)} %copy-done.14, bf16[128,128]{1,0:T(8,128)(2,1)S(1)} %get-tuple-element.52.refs_0_, bf16[64,128]{1,0:T(8,128)(2,1)S(1)} %bitcast.47, bf16[64,128]{1,0:T(8,128)(2,1)S(1)} %bitcast.49, ...), custom_call_target="tpu_custom_call" | custom-call | tf_op jit(solution)/shard_map/local/pallas_call | solution.py:68
  178.7 7.3 %all-to-all-done.3.refs_0_ = bf16[4,584,128]{2,1,0:T(8,128)(2,1)S(1)} async-done(((bf16[4,584,128]{2,1,0:T(8,128)(2,1)}), bf16[4,584,128]{2,1,0:T(8,128)(2,1)S(1)}, u32[]{:S(2)}, u32[]{:S(2)}) %all-to-all-start.3) | async-done | bytes 598048 | tf_op jit(solution)/shard_map/all_to_all | solution.py:612
  186.0 0.8 group.1
  186.8 15.7 %all_to_all.26.refs_0_ = bf16[8,136,128]{2,1,0:T(8,128)(2,1)S(1)} all-to-all(bf16[8,136,128]{2,1,0:T(8,128)(2,1)S(1)} %get-tuple-element.55), channel_id=1, replica_groups=mesh['z'=8,'x'=4,'y'=8,'c'=2] {'z'}, dimensions={0} | all-to-all | bytes 557056 | tf_op jit(solution)/shard_map/all_to_all | solution.py:644
  202.5 0.0 copy-done.15
  202.5 1.9 last.1
  (26 shorter events, 0.1 us)
Async XLA Ops:
  6.3 13.6 %copy-start.20 = (bf16[1,2048,128]{2,1,0:T(8,128)(2,1)S(1)}, bf16[1,2048,128]{2,1,0:T(8,128)(2,1)}, u32[]{:S(2)}) copy-start(bf16[1,2048,128]{2,1,0:T(8,128)(2,1)} %refs_0_.1) | copy-start | bytes 1572868
  6.3 73.7 %all-to-all-start = ((bf16[32,40,1024]{2,1,0:T(8,128)(2,1)}), bf16[32,40,1024]{2,1,0:T(8,128)(2,1)S(1)}, u32[]{:S(2)}, u32[]{:S(2)}) async-start(bf16[32,40,1024]{2,1,0:T(8,128)(2,1)} %dispatch.1.refs_5_), calls=%async_computation | async-start | bytes 5242880 | tf_op jit(solution)/shard_map/all_to_all | solution.py:488
  21.1 5.1 %collective-permute-start = (bf16[2,8,128,128]{3,2,1,0:T(8,128)(2,1)S(1)}, bf16[2,8,128,128]{3,2,1,0:T(8,128)(2,1)S(1)}, u32[]{:S(2)}, u32[]{:S(2)}) collective-permute-start(bf16[2,8,128,128]{3,2,1,0:T(8,128)(2,1)S(1)} %dynamic-slice_bitcast_fusion), channel_id=1, source_target_pairs={{0,1},{1,0},{2,3},{3,2},{4,5},{5,4},{6,7},{7,6},{8,9},{9,8},{10,11... | collective-permute-start | bytes 1572872 | tf_op jit(solution)/shard_map/ppermute | solution.py:492
  23.1 58.8 %copy-start.13 = (s32[7]{0:T(128)S(1)}, s32[7]{0:T(128)}, u32[]{:S(2)}) copy-start(s32[7]{0:T(128)} %and_select_fusion.at) | copy-start | bytes 88
  26.3 0.8 copy-start.21
  80.0 5.6 %copy-start = (bf16[32,40,1024]{2,1,0:T(8,128)(2,1)}, bf16[32,40,1024]{2,1,0:T(8,128)(2,1)S(1)}, u32[]{:S(2)}) copy-start(bf16[32,40,1024]{2,1,0:T(8,128)(2,1)S(1)} %all-to-all-done) | copy-start | bytes 7864324
  80.0 6.8 %collective-permute-start.1 = (bf16[1280,1024]{1,0:T(8,128)(2,1)S(1)}, bf16[1280,1024]{1,0:T(8,128)(2,1)S(1)}, u32[]{:S(2)}, u32[]{:S(2)}) collective-permute-start(bf16[1280,1024]{1,0:T(8,128)(2,1)S(1)} %bitcast.34), channel_id=1, source_target_pairs={{0,1},{1,0},{2,3},{3,2},{4,5},{5,4},{6,7},{7,6},{8,9},{9,8},{10,11... | collective-permute-start | bytes 7864328 | tf_op jit(solution)/shard_map/ppermute | solution.py:524
  81.9 1.4 copy-start.2
  85.6 5.8 %copy-start.4 = (bf16[512,1024]{1,0:T(8,128)(2,1)S(1)}, bf16[512,1024]{1,0:T(8,128)(2,1)}, u32[]{:S(2)}) copy-start(bf16[512,1024]{1,0:T(8,128)(2,1)} %get-tuple-element.43.refs_1_) | copy-start | bytes 3145732
  86.8 2.3 %copy-start.1 = (bf16[1280,1024]{1,0:T(8,128)(2,1)}, bf16[1280,1024]{1,0:T(8,128)(2,1)S(1)}, u32[]{:S(2)}) copy-start(bf16[1280,1024]{1,0:T(8,128)(2,1)S(1)} %collective-permute-done.1.refs_0_.refs_2_) | copy-start | bytes 7864324
  89.1 4.8 %copy-start.5 = (bf16[1280,384]{1,0:T(8,128)(2,1)}, bf16[1280,384]{1,0:T(8,128)(2,1)S(1)}, u32[]{:S(2)}) copy-start(bf16[1280,384]{1,0:T(8,128)(2,1)S(1)} %get-tuple-element.41.refs_0_) | copy-start | bytes 2949124
  93.9 46.6 %all-to-all-start.1 = ((bf16[64,80,128]{2,1,0:T(8,128)(2,1)}), bf16[64,80,128]{2,1,0:T(8,128)(2,1)S(1)}, u32[]{:S(2)}, u32[]{:S(2)}) async-start(bf16[64,80,128]{2,1,0:T(8,128)(2,1)} %bitcast.13), calls=%async_computation.1 | async-start | bytes 2621440 | tf_op jit(solution)/shard_map/all_to_all | solution.py:565
  104.6 35.9 %copy-start.14 = (s32[7]{0:T(128)S(1)}, s32[7]{0:T(128)}, u32[]{:S(2)}) copy-start(s32[7]{0:T(128)} %and_select_fusion.at) | copy-start | bytes 88
  104.6 46.6 %copy-start.18 = (s32[128,2]{0,1:T(2,128)S(1)}, s32[128,2]{0,1:T(2,128)}, u32[]{:S(2)}) copy-start(s32[128,2]{0,1:T(2,128)} %param.17) | copy-start | bytes 3076
  104.6 64.9 %copy-start.19 = (bf16[8,128]{1,0:T(8,128)(2,1)S(1)}, bf16[8,128]{1,0:T(8,128)(2,1)}, u32[]{:S(2)}) copy-start(bf16[8,128]{1,0:T(8,128)(2,1)} %get-tuple-element.50.refs_5_) | copy-start | bytes 6148
  111.7 39.5 %copy-start.3 = (bf16[128,2048]{1,0:T(8,128)(2,1)S(1)}, bf16[128,2048]{1,0:T(8,128)(2,1)}, u32[]{:S(2)}) copy-start(bf16[128,2048]{1,0:T(8,128)(2,1)} %refs_2_.5) | copy-start | bytes 1572868
  111.7 57.8 %copy-start.6 = (bf16[2048,128]{1,0:T(8,128)(2,1)S(1)}, bf16[2048,128]{1,0:T(8,128)(2,1)}, u32[]{:S(2)}) copy-start(bf16[2048,128]{1,0:T(8,128)(2,1)} %refs_1_.3) | copy-start | bytes 1572868
  111.7 57.8 %copy-start.8 = (f32[64,128]{1,0:T(8,128)S(1)}, f32[64,128]{1,0:T(8,128)}, u32[]{:S(2)}) copy-start(f32[64,128]{1,0:T(8,128)} %get-tuple-element.48.refs_3_.refs_4_.refs_5_) | copy-start | bytes 98308
  111.7 57.8 %copy-start.9 = (bf16[128,1,64]{0,2,1:T(8,128)(2,1)S(1)}, bf16[128,1,64]{0,2,1:T(8,128)(2,1)}, u32[]{:S(2)}) copy-start(bf16[128,1,64]{0,2,1:T(8,128)(2,1)} %param.23) | copy-start | bytes 49156
  111.7 57.8 %copy-start.12 = (bf16[128,128]{1,0:T(8,128)(2,1)S(1)}, bf16[128,128]{1,0:T(8,128)(2,1)}, u32[]{:S(2)}) copy-start(bf16[128,128]{1,0:T(8,128)(2,1)} %get-tuple-element.49.refs_4_) | copy-start | bytes 98308
  140.5 0.7 copy-start.17
  141.9 34.5 %copy-start.7 = (bf16[128,1,128]{2,0,1:T(8,128)(2,1)S(1)}, bf16[128,1,128]{2,0,1:T(8,128)(2,1)}, u32[]{:S(2)}) copy-start(bf16[128,1,128]{2,0,1:T(8,128)(2,1)} %param.25) | copy-start | bytes 98308
  141.9 34.5 %copy-start.10 = (bf16[128,1,64]{0,2,1:T(8,128)(2,1)S(1)}, bf16[128,1,64]{0,2,1:T(8,128)(2,1)}, u32[]{:S(2)}) copy-start(bf16[128,1,64]{0,2,1:T(8,128)(2,1)} %param.24) | copy-start | bytes 49156
  141.9 34.5 %copy-start.11 = (f32[1,1,64,128]{3,2,1,0:T(8,128)S(1)}, f32[1,1,64,128]{3,2,1,0:T(8,128)}, u32[]{:S(2)}) copy-start(f32[1,1,64,128]{3,2,1,0:T(8,128)} %refs_5_.1) | copy-start | bytes 98308
  141.9 34.5 %copy-start.16 = (bf16[128,128]{1,0:T(8,128)(2,1)S(1)}, bf16[128,128]{1,0:T(8,128)(2,1)}, u32[]{:S(2)}) copy-start(bf16[128,128]{1,0:T(8,128)(2,1)} %get-tuple-element.53.refs_6_) | copy-start | bytes 98308
  169.5 33.0 %copy-start.15 = (f32[64,128]{1,0:T(8,128)S(1)}, f32[64,128]{1,0:T(8,128)}, u32[]{:S(2)}) copy-start(f32[64,128]{1,0:T(8,128)} %get-tuple-element.58.refs_6_) | copy-start | bytes 98308
  171.5 14.5 %all-to-all-start.3 = ((bf16[4,584,128]{2,1,0:T(8,128)(2,1)}), bf16[4,584,128]{2,1,0:T(8,128)(2,1)S(1)}, u32[]{:S(2)}, u32[]{:S(2)}) async-start(bf16[4,584,128]{2,1,0:T(8,128)(2,1)} %get-tuple-element.51.refs_7_), calls=%async_computation.3 | async-start | bytes 1196032 | tf_op jit(solution)/shard_map/all_to_all | solution.py:612

commit v5 on v4

--- a/solution.py
+++ b/solution.py
@@ -103,21 +103,15 @@
     return jnp.broadcast_to(row, (row.shape[1], row.shape[1])).T
 
 
-def dispatch_kernel(at, routes_ref, weight_ref, x_ref, y_ref, out_ref):
+def dispatch_kernel(at, routes_ref, weight_ref, *refs):
+    out_ref = refs[-1]
+    blocks = (len(refs) - 1) // 2
     tokens = routes_ref.shape[1]
     r0, r1, s0, s1 = slots_of(routes_ref[...])
     key0 = r0 * 32.0 + s0
     key1 = r1 * 32.0 + s1
-    y = y_ref[...].astype(F32)
     w = weight_ref[...]
-    table = jnp.concatenate(
-        [
-            x_ref[...],
-            (column(w[0:1])[:, 0:1] * y).astype(BF),
-            (column(w[1:2])[:, 0:1] * y).astype(BF),
-        ],
-        axis=0,
-    )
+    w0, w1 = column(w[0:1])[:, 0:1], column(w[1:2])[:, 0:1]
     q = iota((40, tokens), 0)
     is_input = q < 20
     slot = jnp.where(is_input, q, jnp.where(q < 24, q - 4, q - 24)).astype(F32)
@@ -137,9 +131,11 @@
             )
         )
     pick = jnp.concatenate(picks, axis=0).astype(BF)
-    for f in range(0, out_ref.shape[2], 256):
-        wide = slice(f, min(f + 256, out_ref.shape[2]))
-        rows = dot(pick, table[:, wide])
+    for n in range(blocks):
+        y = refs[blocks + n][...].astype(F32)
+        table = jnp.concatenate([refs[n][...], (w0 * y).astype(BF), (w1 * y).astype(BF)], axis=0)
+        rows = dot(pick, table)
+        wide = slice(n * rows.shape[1], (n + 1) * rows.shape[1])
         for e in range(experts):
             block = rows[40 * e : 40 * e + 40].astype(BF)
             out_ref[2 * e, :, wide] = block
@@ -151,10 +147,14 @@
 
 
 def layout_kernel(at, wg_ref, wu_ref, wd_ref, woth_ref, side_ref, back_ref):
-    side_ref[:, 0:128] = wg_ref[0]
-    side_ref[:, 128:256] = wu_ref[0]
-    for t in range(0, side_ref.shape[0], 128):
-        side_ref[t : t + 128, 256:384] = wd_ref[0, :, t : t + 128].astype(F32).T.astype(BF)
+    quarter = side_ref.shape[0] // 8
+    for n in range(8):
+        core = at[1] if n < 4 else 1 - at[1]
+        first = pl.multiple_of((core * 4 + quarter_at(n % 4, at[5])) * quarter, 128)
+        to = slice(n * quarter, (n + 1) * quarter)
+        side_ref[to, 0:128] = wg_ref[0, pl.ds(first, quarter), :]
+        side_ref[to, 128:256] = wu_ref[0, pl.ds(first, quarter), :]
+        side_ref[to, 256:384] = wd_ref[0, :, pl.ds(first, quarter)].astype(F32).T.astype(BF)
     for y in range(back_ref.shape[1] // 128):
         first = pl.multiple_of((2 * y + at[1]) * 128, 128)
         for n, w in enumerate(
@@ -168,18 +168,31 @@
             back_ref[128 * n : 128 * n + 128, 128 * y : 128 * y + 128] = w.astype(F32).T.astype(BF)
 
 
-def first_kernel(at, g_ref, w_ref, out_ref):
-    out_ref[...] = dot(g_ref[...], w_ref[...])
-
-
-def delta_kernel(at, g_ref, w_ref, acc_ref, delta_ref, pack_ref):
-    sums = dot(g_ref[...], w_ref[...]) + acc_ref[...]
+def quarter_at(n, side):
+    if n == 0:
+        return 3 - 3 * side
+    return 3 * side if n == 3 else n
+
+
+def first_kernel(at, own_ref, other_ref, w_ref, out_ref):
+    most = own_ref.shape[1]
+    half = w_ref.shape[0] // 2
+    out_ref[...] = dot(own_ref[...], w_ref[0:most, :]) + dot(
+        other_ref[...], w_ref[half : half + most, :]
+    )
+
+
+def delta_kernel(at, rest_ref, beside_ref, w_ref, acc_ref, delta_ref, pack_ref):
+    half = w_ref.shape[0] // 2
+    most = half - rest_ref.shape[1]
+    sums = acc_ref[...] + dot(rest_ref[...], w_ref[most:half, :])
+    sums = sums + dot(beside_ref[...], w_ref[half + most :, :])
     gu, yh = sums[:, 0:256], sums[:, 256:384]
     low = iota((8, 128), 0) < 4
     zero8 = jnp.zeros((8, 128), F32)
     dgs, dus, dhs, pgs, pus = [], [], [], [], []
     mixed = []
-    spans = g_ref.shape[0] // 40
+    spans = rest_ref.shape[0] // 40
     for d in range(spans):
         b = 40 * d
         pg, pu = gu[b : b + 24, 0:128], gu[b : b + 24, 128:256]
@@ -219,18 +232,19 @@
             out_ref[z, y + 1] = o[z * rows : (z + 1) * rows, 128:256]
 
 
-def weight_kernel(at, delta_ref, own_ref, other_ref, gate_ref, up_ref, down_ref, token_ref, dt_ref):
+def weight_kernel(at, delta_ref, own_ref, other_ref, rest_ref, beside_ref, gate_ref, up_ref, down_ref, token_ref, dt_ref):
     token_ref[...] = jnp.zeros(token_ref.shape, F32)
-    rows, half = own_ref.shape
+    rows, quarter = rest_ref.shape
     for r in range(0, rows, 128):
         dt_ref[:, r : r + 128] = delta_ref[r : r + 128, :].astype(F32).T.astype(BF)
-    for g_ref, core in ((own_ref, at[1]), (other_ref, 1 - at[1])):
-        for p in range(0, half, 256):
-            o = dot(dt_ref[...], g_ref[:, p : p + 256])
-            first = pl.multiple_of(core * half + p, 256)
-            gate_ref[0, pl.ds(first, 256), :] = o[0:128].T.astype(BF)
-            up_ref[0, pl.ds(first, 256), :] = o[128:256].T.astype(BF)
-            down_ref[0, :, pl.ds(first, 256)] = o[256:384].astype(BF)
+    for most_ref, last_ref, core in ((own_ref, rest_ref, at[1]), (other_ref, beside_ref, 1 - at[1])):
+        for n in range(4):
+            g = last_ref[...] if n == 3 else most_ref[:, n * quarter : (n + 1) * quarter]
+            o = dot(dt_ref[...], g)
+            first = pl.multiple_of((core * 4 + quarter_at(n, at[5])) * quarter, 128)
+            gate_ref[0, pl.ds(first, quarter), :] = o[0:128].T.astype(BF)
+            up_ref[0, pl.ds(first, quarter), :] = o[128:256].T.astype(BF)
+            down_ref[0, :, pl.ds(first, quarter)] = o[256:384].astype(BF)
 
 
 def sum_kernel(at, got_ref, out_ref):
@@ -459,9 +473,10 @@
     slices = ny * 2
     core = lax.axis_index("c")
     place = lax.axis_index(("z", "x", "y", "c"))
-    divide = jnp.array([1, 1, slices, slices * nx, slices, 1, 2], jnp.int32)
-    wrap = jnp.array([slices, 2, spans, nz, nx, 1, 2], jnp.int32)
-    at = (place // divide) % wrap
+    sizes = ((1, slices), (1, 2), (slices, spans), (slices * nx, nz), (slices, nx), (2, 2))
+    shifts = jnp.array([(d).bit_length() - 1 for d, _ in sizes], jnp.int32)
+    masks = jnp.array([n - 1 for _, n in sizes], jnp.int32)
+    at = lax.shift_right_logical(jnp.broadcast_to(place, shifts.shape), shifts) & masks
     width = queries.shape[2]
     piece_rows = slices * 128 // spans
     routes = routes.T
@@ -472,20 +487,25 @@
     g = log_decay.reshape(tokens, width).T
     slice_block = ((tokens, 128), lambda i, s: (0, s[0]))
     half = slices * 64
-    half_block = ((tokens, half), lambda i, s: (0, s[1]))
+    quarter = half // 4
+    most = half - quarter
+
+    def features(n):
+        return ((tokens, quarter), lambda i, s: (0, s[1] * 4 + quarter_at(n, s[5])))
+
 
     (sent,) = call(
         dispatch_kernel,
         "dispatch",
-        (sds((spans, 40, half), BF),),
+        (sds((spans, 40, most), BF),),
         at,
         routes,
         route_weight,
-        expert_input,
-        cotangent,
-        blocks={2: half_block, 3: half_block},
-    )
-    own = lax.all_to_all(sent, SP, 0, 0, tiled=True).reshape(spans * 40, half)
+        *[expert_input] * 3,
+        *[cotangent] * 3,
+        blocks={2 + n: features(n % 3) for n in range(6)},
+    )
+    own = lax.all_to_all(sent, SP, 0, 0, tiled=True).reshape(spans * 40, most)
 
     weights = jnp.stack([gate_weight[0], up_weight[0]]).reshape(2, ny, 2, 128, 128)
     weights = lax.dynamic_index_in_dim(weights, 1 - core, 2, keepdims=False)
@@ -521,10 +541,16 @@
     )
     own, mixed, side = lax.optimization_barrier((own, mixed, side))
 
-    other = lax.ppermute(own, "c", [(0, 1), (1, 0)])
     rows_all = spans * 40
+    swap = [(0, 1), (1, 0)]
+    up = [(i, (i + 1) % ny) for i in range(ny)]
+    down = [(i, (i - 1) % ny) for i in range(ny)]
+    low = lax.ppermute(own[: rows_all // 2, :quarter], "y", up)
+    high = lax.ppermute(own[rows_all // 2 :, :quarter], "y", down)
+    other = lax.ppermute(own, "c", swap)
     tile = rows_all // TILES
-    rows_block = ((tile, half), lambda i, s: (i, 0))
+    most_block = ((tile, most), lambda i, s: (i, 0))
+    rest_block = ((tile, quarter), lambda i, s: (i, 0))
     acc_block = ((tile, 384), lambda i, s: (i, 0))
     (acc,) = call(
         first_kernel,
@@ -532,24 +558,25 @@
         (sds((rows_all, 384), F32),),
         at,
         own,
+        other,
         side,
-        blocks={0: rows_block, 1: ((half, 384), lambda i, s: (s[1], 0))},
+        blocks={0: most_block, 1: most_block},
         out_blocks={0: acc_block},
         grid=TILES,
     )
+    low, high, acc = lax.optimization_barrier((low, high, acc))
+    rest = jnp.concatenate([low, high], axis=0)
+    beside = lax.ppermute(rest, "c", swap)
     delta, pack = call(
         delta_kernel,
         "deltas",
         (sds((rows_all, 384), BF), sds((rows_all // 2, 256), BF)),
         at,
-        other,
+        rest,
+        beside,
         side,
         acc,
-        blocks={
-            0: rows_block,
-            1: ((half, 384), lambda i, s: (1 - s[1], 0)),
-            2: acc_block,
-        },
+        blocks={0: rest_block, 1: rest_block, 3: acc_block},
         out_blocks={0: acc_block, 1: ((tile // 2, 256), lambda i, s: (i, 0))},
         grid=TILES,
     )
@@ -578,12 +605,13 @@
         delta,
         own,
         other,
+        rest,
+        beside,
         scratch=[pltpu.VMEM((384, spans * 40), BF)],
         after=(terms,),
     )
-    (summed,) = call(
-        sum_kernel, "sums", (sds((nx, nz, 24, 128), BF),), at, got, after=(token,)
-    )
+    got, token = lax.optimization_barrier((got, token))
+    (summed,) = call(sum_kernel, "sums", (sds((nx, nz, 24, 128), BF),), at, got)
     returned = lax.all_to_all(summed.reshape(nx, nz * 24, 128), "x", 0, 0, tiled=True)
     (slice_grad,) = call(
         collect_kernel,

time: 205 us -> 204 us (level)
  waiting for transfers between devices: 85.8 us -> 57 us
  blocking collectives: 44.4 us -> 71.7 us
  starting transfers between devices: 33.1 us -> 35.7 us
    all_to_all x2, waiting for transfers between devices: 77.3 us -> 41 us  [the longest x1 36.1 us: on_device(): own = lax.all_to_all(sent, SP, 0, 0, tiled=True).reshape(spans * 40, most)]
    all_to_all x1, blocking collectives: 15.7 us -> 43 us  [on_device(): lax.all_to_all(terms.reshape(nz * ny, nx * 20, 128), ('z', 'y'), 0, 0, ti...]
    ppermute x1 -> x4, starting transfers between devices: 1.91 us -> 11.3 us  [the longest x1 5.38 us: on_device(): high = lax.ppermute(own[rows_all // 2:, :quarter], 'y', down)]
    ppermute x1 -> x4, waiting for transfers between devices: 1.16 us -> 8.7 us  [the longest x1 5.33 us: on_device(): low = lax.ppermute(own[:rows_all // 2, :quarter], 'y', up)]
    all_to_all x2, starting transfers between devices: 24.3 us -> 17.6 us  [the longest x1 13.6 us: on_device(): own = lax.all_to_all(sent, SP, 0, 0, tiled=True).reshape(spans * 40, most)]
  transfers between devices with their start and end apart: 5 -> 8, of which waited for: 4 -> 6; matrix products, arithmetic and copies ran while one was open for 1% -> 0% of each run, Pallas kernels for 9% -> 10%
where the time goes in v5:
time: 204 us; the launch traced here: 203 us
  blocking collectives  71.7 us (35%)
  waiting for transfers between devices  57 us (28%)
  starting transfers between devices  35.7 us (18%)
  Pallas kernels  33.8 us (17%)
  local copies, waits for them, and re-layouts  2.43 us (1%)
    all_to_all x1, blocking collectives, on_device(): lax.all_to_all(terms.reshape(nz * ny, nx * 20, 128), ('z', 'y'), 0, 0, ti...  43 us
    all_to_all x1, waiting for transfers between devices, on_device(): own = lax.all_to_all(sent, SP, 0, 0, tiled=True).reshape(spans * 40, most)  36.1 us
    pallas_call x13, Pallas kernels, call(): pl.pallas_call(body, name=name, out_shape=outs, grid_spec=pltpu.PrefetchS...  33.8 us
    all_gather x1, blocking collectives, on_device(): total_grad = lax.all_gather(slice_grad, TP, axis=0)  17.1 us
    all_to_all x1, starting transfers between devices, on_device(): own = lax.all_to_all(sent, SP, 0, 0, tiled=True).reshape(spans * 40, most)  13.6 us
    all_to_all x1, blocking collectives, on_device(): lax.all_to_all(summed.reshape(nx, nz * 24, 128), 'x', 0, 0, tiled=True)  9.31 us
    all_to_all x1, waiting for transfers between devices, on_device(): crossing = lax.all_to_all(leaving, 'x', 0, 0, tiled=True)  7.34 us
    ppermute x1, starting transfers between devices, on_device(): high = lax.ppermute(own[rows_all // 2:, :quarter], 'y', down)  5.38 us
  transfers between devices with their start and end apart: 8, of which 6 were waited for; matrix products, arithmetic and copies ran while one was open for 0% of the time, Pallas kernels for 10%

profile of v5, /device:TPU:2, one launch (start us, length us, event | category | flops | bytes accessed | tf_op | source)
XLA Modules:
  0.0 203.0 jit_solution(6273762107009977713)
XLA Ops:
  0.6 1.3 shift-right-logical_and_fusion.at
  1.9 3.8 %dispatch.1.refs_5_ = bf16[32,40,768]{2,1,0:T(8,128)(2,1)} custom-call(s32[6]{0:T(128)} %shift-right-logical_and_fusion.at, s32[2,128]{1,0:T(2,128)} %bitcast.53, f32[2,128]{1,0:T(2,128)} %bitcast.57, bf16[128,2048]{1,0:T(8,128)(2,1)} %refs_4_.2, bf16[128,2048]{1,0:T(8,128)(2,1)} %refs_4_.2, bf16[128,2048]{1,0:T(8,128)(2,1)} %refs_4_.2, ...), custom_call_target="tpu_custom_call" | custom-call | tf_op jit(solution)/shard_map/dispatch/pallas_call | solution.py:68
  5.8 13.6 %all-to-all-start = ((bf16[32,40,768]{2,1,0:T(8,128)(2,1)}), bf16[32,40,768]{2,1,0:T(8,128)(2,1)S(1)}, u32[]{:S(2)}, u32[]{:S(2)}) async-start(bf16[32,40,768]{2,1,0:T(8,128)(2,1)} %dispatch.1.refs_5_), calls=%async_computation | async-start | bytes 3932160 | tf_op jit(solution)/shard_map/all_to_all | solution.py:508
  19.4 0.1 pad_maximum_fusion
  19.5 1.9 collective-permute-start
  21.5 3.1 %forward.1 = (bf16[128,128]{1,0:T(8,128)(2,1)}, bf16[128,128]{1,0:T(8,128)(2,1)}, f32[64,128]{1,0:T(8,128)}, f32[64,128]{1,0:T(8,128)}, bf16[8,128]{1,0:T(8,128)(2,1)}) custom-call(s32[6]{0:T(128)} %shift-right-logical_and_fusion.at, bf16[64,128]{1,0:T(8,128)(2,1)} %bitcast.47, bf16[64,128]{1,0:T(8,128)(2,1)} %bitcast.50, bf16[128,128]{1,0:T(8,128)(2,1)} %bitcast.44, ...), custom_call_target="tpu_custom_call" | custom-call | tf_op jit(solution)/shard_map/forward/pallas_call | solution.py:68
  24.6 0.0 collective-permute-done.refs_3_
  24.6 0.0 copy-start.24
  24.6 0.8 copy-done.24
  25.4 4.3 %layout.1 = (bf16[2048,384]{1,0:T(8,128)(2,1)}, bf16[512,1024]{1,0:T(8,128)(2,1)}) custom-call(s32[6]{0:T(128)} %shift-right-logical_and_fusion.at, bf16[1,2048,128]{2,1,0:T(8,128)(2,1)} %refs_0_.1, bf16[1,2048,128]{2,1,0:T(8,128)(2,1)} %refs_1_.2, bf16[1,128,2048]{2,1,0:T(8,128)(2,1)} %refs_2_.4, bf16[2,8,128,128]{3,2,1,0:T(8,128)(2,1)} %copy-done.24, ...), custom_call_target="tpu_custom_call" | custom-call | tf_op jit(solution)/shard_map/layout/pallas_call | solution.py:68
  29.7 36.1 %all-to-all-done = bf16[32,40,768]{2,1,0:T(8,128)(2,1)S(1)} async-done(((bf16[32,40,768]{2,1,0:T(8,128)(2,1)}), bf16[32,40,768]{2,1,0:T(8,128)(2,1)S(1)}, u32[]{:S(2)}, u32[]{:S(2)}) %all-to-all-start) | async-done | bytes 1966112 | tf_op jit(solution)/shard_map/all_to_all | solution.py:508
  65.9 1.9 collective-permute-start.3
  67.8 5.4 %collective-permute-start.2 = (bf16[640,256]{1,0:T(8,128)(2,1)S(1)}, bf16[640,256]{1,0:T(8,128)(2,1)S(1)}, u32[]{:S(2)}, u32[]{:S(2)}) collective-permute-start(bf16[640,256]{1,0:T(8,128)(2,1)S(1)} %get-tuple-element.70), channel_id=1, source_target_pairs={{0,14},{2,0},{4,2},{6,4},{8,6},{10,8},{12,10},{14,12},{1,15},{3,1}... | collective-permute-start | bytes 983048 | tf_op jit(solution)/shard_map/ppermute | solution.py:549
  73.2 1.9 collective-permute-start.1
  75.2 0.0 collective-permute-done.3.refs_1_.refs_2_
  75.2 1.4 copy-done.4
  76.6 2.9 %first.1.refs_3_ = f32[1280,384]{1,0:T(8,128)S(1)} custom-call(s32[6]{0:T(128)S(1)} %copy-done.16, bf16[1280,768]{1,0:T(8,128)(2,1)S(1)} %bitcast.36, bf16[1280,768]{1,0:T(8,128)(2,1)S(1)} %collective-permute-done.3.refs_1_.refs_2_, bf16[2048,384]{1,0:T(8,128)(2,1)S(1)} %copy-done.4), custom_call_target="tpu_custom_call" | custom-call | tf_op jit(solution)/shard_map/first/pallas_call | solution.py:68
  79.5 1.3 collective-permute-done.2
  80.8 5.3 %collective-permute-done.1 = bf16[640,256]{1,0:T(8,128)(2,1)S(1)} collective-permute-done((bf16[640,256]{1,0:T(8,128)(2,1)S(1)}, bf16[640,256]{1,0:T(8,128)(2,1)S(1)}, u32[]{:S(2)}, u32[]{:S(2)}) %collective-permute-start.1) | collective-permute-done | bytes 327712 | tf_op jit(solution)/shard_map/ppermute | solution.py:548
  86.2 2.1 %collective-permute-start.4 = (bf16[1280,256]{1,0:T(8,128)(2,1)S(1)}, bf16[1280,256]{1,0:T(8,128)(2,1)S(1)}, u32[]{:S(2)}, u32[]{:S(2)}) collective-permute-start(bf16[1280,256]{1,0:T(8,128)(2,1)S(1)} %constant_dynamic-update-slice_fusion.refs_0_.refs_3_), channel_id=1, source_target_pairs={{0,1},{1,0},{2,3},{3,2},{4,5},{5,4},{6,7},{7,6},{8,9},{9,8},{10,11... | collective-permute-start | bytes 1966088 | tf_op jit(solution)/shard_map/ppermute | solution.py:569
  88.3 2.1 %collective-permute-done.4.refs_1_.refs_4_ = bf16[1280,256]{1,0:T(8,128)(2,1)S(1)} collective-permute-done((bf16[1280,256]{1,0:T(8,128)(2,1)S(1)}, bf16[1280,256]{1,0:T(8,128)(2,1)S(1)}, u32[]{:S(2)}, u32[]{:S(2)}) %collective-permute-start.4) | collective-permute-done | bytes 655392 | tf_op jit(solution)/shard_map/ppermute | solution.py:569
  90.4 1.6 deltas.1
  92.0 2.3 %all-gather = bf16[1280,256]{1,0:T(8,128)(2,1)S(1)} all-gather(bf16[640,256]{1,0:T(8,128)(2,1)S(1)} %get-tuple-element.47), channel_id=2, replica_groups=mesh['z'=8,'x'=4,'y'=8,'c'=2] {'c'}, dimensions={0}, use_global_device_ids=true | all-gather | bytes 983040 | tf_op jit(solution)/shard_map/all_gather | solution.py:583
  94.3 1.4 partials.1.refs_5_
  95.7 0.0 copy-start.2
  95.7 0.0 copy-start.20
  95.7 43.0 %all_to_all.25 = bf16[64,80,128]{2,1,0:T(8,128)(2,1)S(1)} all-to-all(bf16[64,80,128]{2,1,0:T(8,128)(2,1)S(1)} %bitcast.38), channel_id=1, replica_groups=mesh['z'=8,'x'=4,'y'=8,'c'=2] {'z','y'}, dimensions={0} | all-to-all | bytes 2621440 | tf_op jit(solution)/shard_map/all_to_all | solution.py:592
  138.8 0.0 copy-start.21
  138.8 0.7 sums.1
  139.5 0.0 copy-start.10
  139.5 0.0 copy-start.13
  139.5 0.0 copy-start.14
  139.5 0.0 copy-start.19
  139.6 9.3 %all_to_all.26 = bf16[4,192,128]{2,1,0:T(8,128)(2,1)S(1)} all-to-all(bf16[4,192,128]{2,1,0:T(8,128)(2,1)S(1)} %bitcast.43), channel_id=1, replica_groups=mesh['z'=8,'x'=4,'y'=8,'c'=2] {'x'}, dimensions={0} | all-to-all | bytes 393216 | tf_op jit(solution)/shard_map/all_to_all | solution.py:615
  148.9 1.1 collect.1
  150.0 17.1 %all-gather.1 = bf16[2048,128]{1,0:T(8,128)(2,1)S(1)} all-gather(bf16[128,128]{1,0:T(8,128)(2,1)S(1)} %collect.1), channel_id=3, replica_groups=mesh['z'=8,'x'=4,'y'=8,'c'=2] {'y','c'}, dimensions={0}, use_global_device_ids=true | all-gather | bytes 557056 | tf_op jit(solution)/shard_map/all_gather | solution.py:626
  167.1 0.0 copy-done.11
  167.1 2.0 head.1
  169.2 4.9 %all-to-all-start.3 = ((bf16[4,584,128]{2,1,0:T(8,128)(2,1)}), bf16[4,584,128]{2,1,0:T(8,128)(2,1)S(1)}, u32[]{:S(2)}, u32[]{:S(2)}) async-start(bf16[4,584,128]{2,1,0:T(8,128)(2,1)} %get-tuple-element.55.refs_7_), calls=%async_computation.3 | async-start | bytes 1196032 | tf_op jit(solution)/shard_map/all_to_all | solution.py:640
  174.1 0.0 copy-done.10
  174.1 2.3 %local.1 = (bf16[64,128]{1,0:T(8,128)(2,1)}, f32[64,128]{1,0:T(8,128)S(1)}, f32[64,128]{1,0:T(8,128)S(1)}, f32[128,128]{1,0:T(8,128)S(1)}) custom-call(s32[6]{0:T(128)S(1)} %copy-done.16, bf16[128,128]{1,0:T(8,128)(2,1)S(1)} %get-tuple-element.56.refs_0_, bf16[64,128]{1,0:T(8,128)(2,1)S(1)} %bitcast.49, bf16[64,128]{1,0:T(8,128)(2,1)S(1)} %bitcast.51, ...), custom_call_target="tpu_custom_call" | custom-call | tf_op jit(solution)/shard_map/local/pallas_call | solution.py:68
  176.3 7.3 %all-to-all-done.3.refs_0_ = bf16[4,584,128]{2,1,0:T(8,128)(2,1)S(1)} async-done(((bf16[4,584,128]{2,1,0:T(8,128)(2,1)}), bf16[4,584,128]{2,1,0:T(8,128)(2,1)S(1)}, u32[]{:S(2)}, u32[]{:S(2)}) %all-to-all-start.3) | async-done | bytes 598048 | tf_op jit(solution)/shard_map/all_to_all | solution.py:640
  183.7 1.6 group.1
  185.2 4.0 %all-to-all-start.4 = ((bf16[8,136,128]{2,1,0:T(8,128)(2,1)}), bf16[8,136,128]{2,1,0:T(8,128)(2,1)S(1)}, u32[]{:S(2)}, u32[]{:S(2)}) async-start(bf16[8,136,128]{2,1,0:T(8,128)(2,1)} %get-tuple-element.59), calls=%async_computation.4 | async-start | bytes 557056 | tf_op jit(solution)/shard_map/all_to_all | solution.py:672
  189.2 0.0 copy-start.18
  189.3 7.0 %weights.1 = (bf16[1,2048,128]{2,1,0:T(8,128)(2,1)}, bf16[1,2048,128]{2,1,0:T(8,128)(2,1)}, bf16[1,128,2048]{2,1,0:T(8,128)(2,1)}, f32[8,128]{1,0:T(8,128)}) custom-call(s32[6]{0:T(128)} %shift-right-logical_and_fusion.at, bf16[1280,384]{1,0:T(8,128)(2,1)} %copy-done.8, bf16[1280,768]{1,0:T(8,128)(2,1)} %bitcast.37, bf16[1280,768]{1,0:T(8,128)(2,1)} %copy-done.3, ...), custom_call_target="tpu_custom_call" | custom-call | tf_op jit(solution)/shard_map/weights/pallas_call | solution.py:68
  196.3 4.8 %all-to-all-done.4.refs_0_ = bf16[8,136,128]{2,1,0:T(8,128)(2,1)S(1)} async-done(((bf16[8,136,128]{2,1,0:T(8,128)(2,1)}), bf16[8,136,128]{2,1,0:T(8,128)(2,1)S(1)}, u32[]{:S(2)}, u32[]{:S(2)}) %all-to-all-start.4) | async-done | bytes 278560 | tf_op jit(solution)/shard_map/all_to_all | solution.py:672
  201.1 1.9 last.1
  (41 shorter events, 0.2 us)
Async XLA Ops:
  5.7 13.6 %copy-start.22 = (bf16[1,2048,128]{2,1,0:T(8,128)(2,1)S(1)}, bf16[1,2048,128]{2,1,0:T(8,128)(2,1)}, u32[]{:S(2)}) copy-start(bf16[1,2048,128]{2,1,0:T(8,128)(2,1)} %refs_0_.1) | copy-start | bytes 1572868
  5.8 13.6 %copy-start.23 = (bf16[1,2048,128]{2,1,0:T(8,128)(2,1)S(1)}, bf16[1,2048,128]{2,1,0:T(8,128)(2,1)}, u32[]{:S(2)}) copy-start(bf16[1,2048,128]{2,1,0:T(8,128)(2,1)} %refs_1_.2) | copy-start | bytes 1572868
  5.8 60.1 %all-to-all-start = ((bf16[32,40,768]{2,1,0:T(8,128)(2,1)}), bf16[32,40,768]{2,1,0:T(8,128)(2,1)S(1)}, u32[]{:S(2)}, u32[]{:S(2)}) async-start(bf16[32,40,768]{2,1,0:T(8,128)(2,1)} %dispatch.1.refs_5_), calls=%async_computation | async-start | bytes 3932160 | tf_op jit(solution)/shard_map/all_to_all | solution.py:508
  19.5 5.1 %collective-permute-start = (bf16[2,8,128,128]{3,2,1,0:T(8,128)(2,1)S(1)}, bf16[2,8,128,128]{3,2,1,0:T(8,128)(2,1)S(1)}, u32[]{:S(2)}, u32[]{:S(2)}) collective-permute-start(bf16[2,8,128,128]{3,2,1,0:T(8,128)(2,1)S(1)} %dynamic-slice_bitcast_fusion), channel_id=1, source_target_pairs={{0,1},{1,0},{2,3},{3,2},{4,5},{5,4},{6,7},{7,6},{8,9},{9,8},{10,11... | collective-permute-start | bytes 1572872 | tf_op jit(solution)/shard_map/ppermute | solution.py:512
  24.6 50.6 %copy-start.16 = (s32[6]{0:T(128)S(1)}, s32[6]{0:T(128)}, u32[]{:S(2)}) copy-start(s32[6]{0:T(128)} %shift-right-logical_and_fusion.at) | copy-start | bytes 76
  24.6 0.8 copy-start.24
  65.9 13.6 %copy-start = (bf16[32,40,768]{2,1,0:T(8,128)(2,1)}, bf16[32,40,768]{2,1,0:T(8,128)(2,1)S(1)}, u32[]{:S(2)}) copy-start(bf16[32,40,768]{2,1,0:T(8,128)(2,1)S(1)} %all-to-all-done) | copy-start | bytes 5898244
  65.9 9.3 %collective-permute-start.3 = (bf16[1280,768]{1,0:T(8,128)(2,1)S(1)}, bf16[1280,768]{1,0:T(8,128)(2,1)S(1)}, u32[]{:S(2)}, u32[]{:S(2)}) collective-permute-start(bf16[1280,768]{1,0:T(8,128)(2,1)S(1)} %bitcast.34), channel_id=1, source_target_pairs={{0,1},{1,0},{2,3},{3,2},{4,5},{5,4},{6,7},{7,6},{8,9},{9,8},{10,11... | collective-permute-start | bytes 5898248 | tf_op jit(solution)/shard_map/ppermute | solution.py:550
  67.8 13.0 %collective-permute-start.2 = (bf16[640,256]{1,0:T(8,128)(2,1)S(1)}, bf16[640,256]{1,0:T(8,128)(2,1)S(1)}, u32[]{:S(2)}, u32[]{:S(2)}) collective-permute-start(bf16[640,256]{1,0:T(8,128)(2,1)S(1)} %get-tuple-element.70), channel_id=1, source_target_pairs={{0,14},{2,0},{4,2},{6,4},{8,6},{10,8},{12,10},{14,12},{1,15},{3,1}... | collective-permute-start | bytes 983048 | tf_op jit(solution)/shard_map/ppermute | solution.py:549
  73.2 12.9 %collective-permute-start.1 = (bf16[640,256]{1,0:T(8,128)(2,1)S(1)}, bf16[640,256]{1,0:T(8,128)(2,1)S(1)}, u32[]{:S(2)}, u32[]{:S(2)}) collective-permute-start(bf16[640,256]{1,0:T(8,128)(2,1)S(1)} %get-tuple-element.71), channel_id=1, source_target_pairs={{0,2},{2,4},{4,6},{6,8},{8,10},{10,12},{12,14},{14,0},{1,3},{3,5},... | collective-permute-start | bytes 983048 | tf_op jit(solution)/shard_map/ppermute | solution.py:548
  75.2 1.4 copy-start.4
  76.6 2.9 %copy-start.3 = (bf16[1280,768]{1,0:T(8,128)(2,1)}, bf16[1280,768]{1,0:T(8,128)(2,1)S(1)}, u32[]{:S(2)}) copy-start(bf16[1280,768]{1,0:T(8,128)(2,1)S(1)} %collective-permute-done.3.refs_1_.refs_2_) | copy-start | bytes 5898244
  86.2 5.8 %copy-start.5 = (bf16[1280,256]{1,0:T(8,128)(2,1)}, bf16[1280,256]{1,0:T(8,128)(2,1)S(1)}, u32[]{:S(2)}) copy-start(bf16[1280,256]{1,0:T(8,128)(2,1)S(1)} %constant_dynamic-update-slice_fusion.refs_0_.refs_3_) | copy-start | bytes 1966084
  86.2 8.1 %copy-start.7 = (bf16[512,1024]{1,0:T(8,128)(2,1)S(1)}, bf16[512,1024]{1,0:T(8,128)(2,1)}, u32[]{:S(2)}) copy-start(bf16[512,1024]{1,0:T(8,128)(2,1)} %get-tuple-element.48.refs_1_) | copy-start | bytes 3145732
  86.2 4.1 %collective-permute-start.4 = (bf16[1280,256]{1,0:T(8,128)(2,1)S(1)}, bf16[1280,256]{1,0:T(8,128)(2,1)S(1)}, u32[]{:S(2)}, u32[]{:S(2)}) collective-permute-start(bf16[1280,256]{1,0:T(8,128)(2,1)S(1)} %constant_dynamic-update-slice_fusion.refs_0_.refs_3_), channel_id=1, source_target_pairs={{0,1},{1,0},{2,3},{3,2},{4,5},{5,4},{6,7},{7,6},{8,9},{9,8},{10,11... | collective-permute-start | bytes 1966088 | tf_op jit(solution)/shard_map/ppermute | solution.py:569
  90.4 1.6 copy-start.6
  92.0 3.7 %copy-start.8 = (bf16[1280,384]{1,0:T(8,128)(2,1)}, bf16[1280,384]{1,0:T(8,128)(2,1)S(1)}, u32[]{:S(2)}) copy-start(bf16[1280,384]{1,0:T(8,128)(2,1)S(1)} %get-tuple-element.46.refs_0_) | copy-start | bytes 2949124
  95.7 43.8 %copy-start.1 = (bf16[8,8,80,128]{3,2,1,0:T(8,128)(2,1)}, bf16[8,8,80,128]{3,2,1,0:T(8,128)(2,1)S(1)}, u32[]{:S(2)}) copy-start(bf16[8,8,80,128]{3,2,1,0:T(8,128)(2,1)S(1)} %partials.1.refs_5_) | copy-start | bytes 3932164
  95.7 53.1 %copy-start.2 = (bf16[128,2048]{1,0:T(8,128)(2,1)S(1)}, bf16[128,2048]{1,0:T(8,128)(2,1)}, u32[]{:S(2)}) copy-start(bf16[128,2048]{1,0:T(8,128)(2,1)} %refs_2_.5) | copy-start | bytes 1572868
  95.7 53.1 %copy-start.20 = (s32[128,2]{0,1:T(2,128)S(1)}, s32[128,2]{0,1:T(2,128)}, u32[]{:S(2)}) copy-start(s32[128,2]{0,1:T(2,128)} %param.17) | copy-start | bytes 3076
  138.8 28.4 %copy-start.9 = (bf16[2048,128]{1,0:T(8,128)(2,1)S(1)}, bf16[2048,128]{1,0:T(8,128)(2,1)}, u32[]{:S(2)}) copy-start(bf16[2048,128]{1,0:T(8,128)(2,1)} %refs_1_.3) | copy-start | bytes 1572868
  138.8 28.4 %copy-start.11 = (f32[64,128]{1,0:T(8,128)S(1)}, f32[64,128]{1,0:T(8,128)}, u32[]{:S(2)}) copy-start(f32[64,128]{1,0:T(8,128)} %get-tuple-element.52.refs_3_.refs_4_.refs_5_) | copy-start | bytes 98308
  138.8 28.4 %copy-start.12 = (bf16[128,1,64]{0,2,1:T(8,128)(2,1)S(1)}, bf16[128,1,64]{0,2,1:T(8,128)(2,1)}, u32[]{:S(2)}) copy-start(bf16[128,1,64]{0,2,1:T(8,128)(2,1)} %param.23) | copy-start | bytes 49156
  138.8 28.4 %copy-start.15 = (bf16[128,128]{1,0:T(8,128)(2,1)S(1)}, bf16[128,128]{1,0:T(8,128)(2,1)}, u32[]{:S(2)}) copy-start(bf16[128,128]{1,0:T(8,128)(2,1)} %get-tuple-element.53.refs_4_) | copy-start | bytes 98308
  138.8 28.4 %copy-start.21 = (bf16[8,128]{1,0:T(8,128)(2,1)S(1)}, bf16[8,128]{1,0:T(8,128)(2,1)}, u32[]{:S(2)}) copy-start(bf16[8,128]{1,0:T(8,128)(2,1)} %get-tuple-element.54.refs_5_) | copy-start | bytes 6148
  139.5 34.6 %copy-start.10 = (bf16[128,1,128]{2,0,1:T(8,128)(2,1)S(1)}, bf16[128,1,128]{2,0,1:T(8,128)(2,1)}, u32[]{:S(2)}) copy-start(bf16[128,1,128]{2,0,1:T(8,128)(2,1)} %param.25) | copy-start | bytes 98308
  139.5 34.5 %copy-start.13 = (bf16[128,1,64]{0,2,1:T(8,128)(2,1)S(1)}, bf16[128,1,64]{0,2,1:T(8,128)(2,1)}, u32[]{:S(2)}) copy-start(bf16[128,1,64]{0,2,1:T(8,128)(2,1)} %param.24) | copy-start | bytes 49156
  139.5 34.5 %copy-start.14 = (f32[1,1,64,128]{3,2,1,0:T(8,128)S(1)}, f32[1,1,64,128]{3,2,1,0:T(8,128)}, u32[]{:S(2)}) copy-start(f32[1,1,64,128]{3,2,1,0:T(8,128)} %refs_5_.3) | copy-start | bytes 98308
  139.5 34.5 %copy-start.19 = (bf16[128,128]{1,0:T(8,128)(2,1)S(1)}, bf16[128,128]{1,0:T(8,128)(2,1)}, u32[]{:S(2)}) copy-start(bf16[128,128]{1,0:T(8,128)(2,1)} %get-tuple-element.57.refs_6_) | copy-start | bytes 98308
  169.2 14.5 %all-to-all-start.3 = ((bf16[4,584,128]{2,1,0:T(8,128)(2,1)}), bf16[4,584,128]{2,1,0:T(8,128)(2,1)S(1)}, u32[]{:S(2)}, u32[]{:S(2)}) async-start(bf16[4,584,128]{2,1,0:T(8,128)(2,1)} %get-tuple-element.55.refs_7_), calls=%async_computation.3 | async-start | bytes 1196032 | tf_op jit(solution)/shard_map/all_to_all | solution.py:640
  185.2 15.9 %all-to-all-start.4 = ((bf16[8,136,128]{2,1,0:T(8,128)(2,1)}), bf16[8,136,128]{2,1,0:T(8,128)(2,1)S(1)}, u32[]{:S(2)}, u32[]{:S(2)}) async-start(bf16[8,136,128]{2,1,0:T(8,128)(2,1)} %get-tuple-element.59), calls=%async_computation.4 | async-start | bytes 557056 | tf_op jit(solution)/shard_map/all_to_all | solution.py:672
  189.2 11.9 %copy-start.17 = (s32[6]{0:T(128)S(1)}, s32[6]{0:T(128)}, u32[]{:S(2)}) copy-start(s32[6]{0:T(128)} %shift-right-logical_and_fusion.at) | copy-start | bytes 76
  189.2 11.9 %copy-start.18 = (f32[64,128]{1,0:T(8,128)S(1)}, f32[64,128]{1,0:T(8,128)}, u32[]{:S(2)}) copy-start(f32[64,128]{1,0:T(8,128)} %get-tuple-element.62.refs_6_) | copy-start | bytes 98308

commit v6 on v4

--- a/solution.py
+++ b/solution.py
@@ -42,6 +42,15 @@
     return lax.broadcasted_iota(jnp.int32, shape, dim)
 
 
+class Place:
+    def __init__(self, number, sizes):
+        self.number, self.sizes = number, sizes
+
+    def __getitem__(self, k):
+        step, count = self.sizes[k]
+        return lax.shift_right_logical(self.number[0], step.bit_length() - 1) & (count - 1)
+
+
 def call(
     kernel, name, outs, scalars, *args, blocks=None, out_blocks=None, scratch=(), after=(), grid=1
 ):
@@ -50,17 +59,20 @@
     specs = []
     used, waits = len(args), len(after)
 
-    def body(at, *refs):
-        kernel(at, *refs[:used], *refs[used + waits :])
+    def body(number, *refs):
+        kernel(Place(number, scalars.sizes), *refs[:used], *refs[used + waits :])
+
+    def placed(index):
+        return lambda i, s: index(i, Place(s, scalars.sizes))
 
     for n, a in enumerate(args):
         if n in blocks:
-            specs.append(pl.BlockSpec(*blocks[n]))
+            specs.append(pl.BlockSpec(blocks[n][0], placed(blocks[n][1])))
         else:
             specs.append(pl.BlockSpec(a.shape, lambda i, s, nd=a.ndim: (0,) * nd))
     specs += [pl.BlockSpec(memory_space=pl.ANY)] * waits
     out_specs = tuple(
-        pl.BlockSpec(*out_blocks[n])
+        pl.BlockSpec(out_blocks[n][0], placed(out_blocks[n][1]))
         if n in out_blocks
         else pl.BlockSpec(o.shape, lambda i, s, nd=len(o.shape): (0,) * nd)
         for n, o in enumerate(outs)
@@ -79,7 +91,7 @@
         compiler_params=pltpu.CompilerParams(
             vmem_limit_bytes=(SMALL if name in LEAN else LIMIT)
         ),
-    )(scalars, *args, *after)
+    )(scalars.number, *args, *after)
 
 
 def sds(shape, dtype):
@@ -108,16 +120,8 @@
     r0, r1, s0, s1 = slots_of(routes_ref[...])
     key0 = r0 * 32.0 + s0
     key1 = r1 * 32.0 + s1
-    y = y_ref[...].astype(F32)
     w = weight_ref[...]
-    table = jnp.concatenate(
-        [
-            x_ref[...],
-            (column(w[0:1])[:, 0:1] * y).astype(BF),
-            (column(w[1:2])[:, 0:1] * y).astype(BF),
-        ],
-        axis=0,
-    )
+    w0, w1 = column(w[0:1])[:, 0:1], column(w[1:2])[:, 0:1]
     q = iota((40, tokens), 0)
     is_input = q < 20
     slot = jnp.where(is_input, q, jnp.where(q < 24, q - 4, q - 24)).astype(F32)
@@ -139,7 +143,9 @@
     pick = jnp.concatenate(picks, axis=0).astype(BF)
     for f in range(0, out_ref.shape[2], 256):
         wide = slice(f, min(f + 256, out_ref.shape[2]))
-        rows = dot(pick, table[:, wide])
+        y = y_ref[:, wide].astype(F32)
+        table = jnp.concatenate([x_ref[:, wide], (w0 * y).astype(BF), (w1 * y).astype(BF)], axis=0)
+        rows = dot(pick, table)
         for e in range(experts):
             block = rows[40 * e : 40 * e + 40].astype(BF)
             out_ref[2 * e, :, wide] = block
@@ -219,8 +225,7 @@
             out_ref[z, y + 1] = o[z * rows : (z + 1) * rows, 128:256]
 
 
-def weight_kernel(at, delta_ref, own_ref, other_ref, gate_ref, up_ref, down_ref, token_ref, dt_ref):
-    token_ref[...] = jnp.zeros(token_ref.shape, F32)
+def weight_kernel(at, delta_ref, own_ref, other_ref, gate_ref, up_ref, down_ref, dt_ref):
     rows, half = own_ref.shape
     for r in range(0, rows, 128):
         dt_ref[:, r : r + 128] = delta_ref[r : r + 128, :].astype(F32).T.astype(BF)
@@ -372,7 +377,8 @@
     vl_ref[...] = dot_tn(p_ref[...], rows)
 
 
-def group_kernel(at, got_ref, inside_ref, after_ref, send_ref):
+def group_kernel(at, got_ref, inside_ref, after_ref, send_ref, token_ref):
+    token_ref[...] = jnp.zeros(token_ref.shape, F32)
     nx, rows, _ = got_ref.shape
     nz = send_ref.shape[0]
     width = inside_ref.shape[0]
@@ -458,10 +464,9 @@
     spans = nz * nx
     slices = ny * 2
     core = lax.axis_index("c")
-    place = lax.axis_index(("z", "x", "y", "c"))
-    divide = jnp.array([1, 1, slices, slices * nx, slices, 1, 2], jnp.int32)
-    wrap = jnp.array([slices, 2, spans, nz, nx, 1, 2], jnp.int32)
-    at = (place // divide) % wrap
+    place = lax.axis_index(("z", "x", "y", "c")).astype(jnp.int32)
+    sizes = ((1, slices), (1, 2), (slices, spans), (slices * nx, nz), (slices, nx))
+    at = Place(place.reshape(1), sizes)
     width = queries.shape[2]
     piece_rows = slices * 128 // spans
     routes = routes.T
@@ -565,51 +570,61 @@
     got = lax.all_to_all(
         terms.reshape(nz * ny, nx * 20, 128), ("z", "y"), 0, 0, tiled=True
     ).reshape(nz, ny, nx * 20, 128)
-    gate_grad, up_grad, down_grad, token = call(
+    (summed,) = call(sum_kernel, "sums", (sds((nx, nz, 24, 128), BF),), at, got)
+    returned = lax.all_to_all(summed.reshape(nx, nz * 24, 128), "x", 0, 0, tiled=True)
+    (slice_grad,) = call(
+        collect_kernel,
+        "collect",
+        (sds((tokens, 128), BF),),
+        at,
+        routes,
+        returned.reshape(nx, nz, 24, 128),
+        cotangent,
+        blocks={2: slice_block},
+    )
+    total_grad = lax.all_gather(slice_grad, TP, axis=0)
+
+    rows, leaving = call(
+        partial(head_kernel, piece_rows),
+        "head",
+        (sds((tokens, 128), BF), sds((nx, nz * piece_rows + width + 8, 128), BF)),
+        at,
+        total_grad,
+        out_weight,
+        q,
+        gc,
+        mixed,
+        totals,
+    )
+    crossing = lax.all_to_all(leaving, "x", 0, 0, tiled=True)
+    inside, later, group, token = call(
+        group_kernel,
+        "group",
+        (
+            sds((width, 128), F32),
+            sds((8, 128), F32),
+            sds((nz, piece_rows + width + 8, 128), BF),
+            sds((8, 128), F32),
+        ),
+        at,
+        crossing,
+    )
+    group = lax.all_to_all(group, "z", 0, 0, tiled=True)
+    gate_grad, up_grad, down_grad = call(
         weight_kernel,
         "weights",
         (
             sds((1, slices * 128, 128), BF),
             sds((1, slices * 128, 128), BF),
             sds((1, 128, slices * 128), BF),
-            sds((8, 128), F32),
         ),
         at,
         delta,
         own,
         other,
         scratch=[pltpu.VMEM((384, spans * 40), BF)],
-        after=(terms,),
-    )
-    (summed,) = call(
-        sum_kernel, "sums", (sds((nx, nz, 24, 128), BF),), at, got, after=(token,)
-    )
-    returned = lax.all_to_all(summed.reshape(nx, nz * 24, 128), "x", 0, 0, tiled=True)
-    (slice_grad,) = call(
-        collect_kernel,
-        "collect",
-        (sds((tokens, 128), BF),),
-        at,
-        routes,
-        returned.reshape(nx, nz, 24, 128),
-        cotangent,
-        blocks={2: slice_block},
-    )
-    total_grad = lax.all_gather(slice_grad, TP, axis=0)
-
-    rows, leaving = call(
-        partial(head_kernel, piece_rows),
-        "head",
-        (sds((tokens, 128), BF), sds((nx, nz * piece_rows + width + 8, 128), BF)),
-        at,
-        total_grad,
-        out_weight,
-        q,
-        gc,
-        mixed,
-        totals,
-    )
-    crossing = lax.all_to_all(leaving, "x", 0, 0, tiled=True)
+        after=(token,),
+    )
     qraw, qq, key_local, value_local = call(
         local_kernel,
         "local",
@@ -627,21 +642,8 @@
         gc,
         start_state,
         p,
-        after=(leaving,),
-    )
-    inside, later, group = call(
-        group_kernel,
-        "group",
-        (
-            sds((width, 128), F32),
-            sds((8, 128), F32),
-            sds((nz, piece_rows + width + 8, 128), BF),
-        ),
-        at,
-        crossing,
-        after=(qq,),
-    )
-    group = lax.all_to_all(group, "z", 0, 0, tiled=True)
+        after=(token,),
+    )
     out_grad, key, value, decay = call(
         last_kernel,
         "last",

time: 205 us -> 197 us (0.961)
  blocking collectives: 44.4 us -> 88.7 us
  waiting for transfers between devices: 85.8 us -> 55.6 us
  starting transfers between devices: 33.1 us -> 21.4 us
  Pallas kernels: 34.6 us -> 25.7 us
    all_to_all x1 -> x2, blocking collectives: 15.7 us -> 60 us  [the longest x1 46.5 us: on_device(): lax.all_to_all(terms.reshape(nz * ny, nx * 20, 128), ('z', 'y'), 0, 0, ti...]
    all_to_all x2 -> x1, waiting for transfers between devices: 36.1 us -> 3.86 us  [on_device(): group = lax.all_to_all(group, 'z', 0, 0, tiled=True)]
    all_to_all x2 -> x1, starting transfers between devices: 15.6 us -> 4.01 us  [on_device(): group = lax.all_to_all(group, 'z', 0, 0, tiled=True)]
    pallas_call x13, Pallas kernels: 34.6 us -> 25.7 us  [call(): pl.pallas_call(body, name=name, out_shape=outs, grid_spec=pltpu.PrefetchS...]
  transfers between devices with their start and end apart: 5 -> 4, of which waited for: 4 -> 3; matrix products, arithmetic and copies ran while one was open for 1% -> 1% of each run, Pallas kernels for 9% -> 8%
where the time goes in v6:
time: 197 us; the launch traced here: 196 us
  blocking collectives  88.7 us (45%)
  waiting for transfers between devices  55.6 us (28%)
  Pallas kernels  25.7 us (13%)
  starting transfers between devices  21.4 us (11%)
  local copies, waits for them, and re-layouts  2.32 us (1%)
    all_to_all x1, waiting for transfers between devices, on_device(): own = lax.all_to_all(sent, SP, 0, 0, tiled=True).reshape(spans * 40, half)  50 us
    all_to_all x1, blocking collectives, on_device(): lax.all_to_all(terms.reshape(nz * ny, nx * 20, 128), ('z', 'y'), 0, 0, ti...  46.5 us
    pallas_call x13, Pallas kernels, call(): pl.pallas_call(body, name=name, out_shape=outs, grid_spec=pltpu.PrefetchS...  25.7 us
    all_gather x1, blocking collectives, on_device(): total_grad = lax.all_gather(slice_grad, TP, axis=0)  17.1 us
    all_to_all x1, starting transfers between devices, on_device(): own = lax.all_to_all(sent, SP, 0, 0, tiled=True).reshape(spans * 40, half)  13.6 us
    all_to_all x1, blocking collectives, on_device(): crossing = lax.all_to_all(leaving, 'x', 0, 0, tiled=True)  13.5 us
    all_to_all x1, blocking collectives, on_device(): lax.all_to_all(summed.reshape(nx, nz * 24, 128), 'x', 0, 0, tiled=True)  9.3 us
    all_to_all x1, starting transfers between devices, on_device(): group = lax.all_to_all(group, 'z', 0, 0, tiled=True)  4.01 us
  transfers between devices with their start and end apart: 4, of which 3 were waited for; matrix products, arithmetic and copies ran while one was open for 1% of the time, Pallas kernels for 8%

profile of v6, /device:TPU:2, one launch (start us, length us, event | category | flops | bytes accessed | tf_op | source)
XLA Modules:
  0.0 195.8 jit_solution(4115978494828005410)
XLA Ops:
  0.6 3.6 %dispatch.1.refs_5_ = bf16[32,40,1024]{2,1,0:T(8,128)(2,1)} custom-call(s32[1]{0:T(128)} %bitcast.number, s32[2,128]{1,0:T(2,128)} %bitcast.53, f32[2,128]{1,0:T(2,128)} %bitcast.57, bf16[128,2048]{1,0:T(8,128)(2,1)} %refs_2_.3, bf16[128,2048]{1,0:T(8,128)(2,1)} %refs_2_.5), custom_call_target="tpu_custom_call" | custom-call | tf_op jit(solution)/shard_map/dispatch/pallas_call | solution.py:80
  4.2 13.6 %all-to-all-start = ((bf16[32,40,1024]{2,1,0:T(8,128)(2,1)}), bf16[32,40,1024]{2,1,0:T(8,128)(2,1)S(1)}, u32[]{:S(2)}, u32[]{:S(2)}) async-start(bf16[32,40,1024]{2,1,0:T(8,128)(2,1)} %dispatch.1.refs_5_), calls=%async_computation | async-start | bytes 5242880 | tf_op jit(solution)/shard_map/all_to_all | solution.py:493
  17.8 0.0 copy-done.18
  17.8 1.1 pad_maximum_fusion
  19.0 1.9 collective-permute-start
  21.0 2.5 %forward.1 = (bf16[128,128]{1,0:T(8,128)(2,1)}, bf16[128,128]{1,0:T(8,128)(2,1)}, f32[64,128]{1,0:T(8,128)}, f32[64,128]{1,0:T(8,128)}, bf16[8,128]{1,0:T(8,128)(2,1)}) custom-call(s32[1]{0:T(128)} %bitcast.number, bf16[64,128]{1,0:T(8,128)(2,1)} %bitcast.47, bf16[64,128]{1,0:T(8,128)(2,1)} %bitcast.50, bf16[128,128]{1,0:T(8,128)(2,1)} %bitcast.44, ...), custom_call_target="tpu_custom_call" | custom-call | tf_op jit(solution)/shard_map/forward/pallas_call | solution.py:80
  23.5 0.0 collective-permute-done.refs_3_
  23.5 0.8 copy-done.19
  24.3 3.6 %layout.1 = (bf16[2048,384]{1,0:T(8,128)(2,1)}, bf16[512,1024]{1,0:T(8,128)(2,1)}) custom-call(s32[1]{0:T(128)} %bitcast.number, bf16[1,2048,128]{2,1,0:T(8,128)(2,1)} %refs_0_.1, bf16[1,2048,128]{2,1,0:T(8,128)(2,1)} %refs_1_.2, bf16[1,128,2048]{2,1,0:T(8,128)(2,1)} %refs_2_.4, bf16[2,8,128,128]{3,2,1,0:T(8,128)(2,1)} %copy-done.19, ...), custom_call_target="tpu_custom_call" | custom-call | tf_op jit(solution)/shard_map/layout/pallas_call | solution.py:80
  27.9 50.0 %all-to-all-done = bf16[32,40,1024]{2,1,0:T(8,128)(2,1)S(1)} async-done(((bf16[32,40,1024]{2,1,0:T(8,128)(2,1)}), bf16[32,40,1024]{2,1,0:T(8,128)(2,1)S(1)}, u32[]{:S(2)}, u32[]{:S(2)}) %all-to-all-start) | async-done | bytes 2621472 | tf_op jit(solution)/shard_map/all_to_all | solution.py:493
  77.9 1.9 collective-permute-start.1
  79.8 0.0 copy-start.2
  79.8 1.4 copy-done.2
  81.2 1.7 first.1.refs_2_
  82.9 0.0 copy-done
  82.9 0.0 copy-start.4
  82.9 1.7 collective-permute-done.1.refs_0_.refs_2_
  84.7 1.8 deltas.1
  86.5 0.0 copy-done.1
  86.5 0.0 copy-start.5
  86.5 2.3 %all-gather = bf16[1280,256]{1,0:T(8,128)(2,1)S(1)} all-gather(bf16[640,256]{1,0:T(8,128)(2,1)S(1)} %get-tuple-element.42), channel_id=2, replica_groups=mesh['z'=8,'x'=4,'y'=8,'c'=2] {'c'}, dimensions={0}, use_global_device_ids=true | all-gather | bytes 983040 | tf_op jit(solution)/shard_map/all_gather | solution.py:561
  88.8 0.0 copy-done.4
  88.8 0.8 partials.1
  89.6 0.0 copy-done.5
  89.6 0.0 copy-start.3
  89.6 0.0 copy-start.16
  89.7 46.5 %all_to_all.25 = bf16[64,80,128]{2,1,0:T(8,128)(2,1)S(1)} all-to-all(bf16[64,80,128]{2,1,0:T(8,128)(2,1)S(1)} %bitcast.38), channel_id=1, replica_groups=mesh['z'=8,'x'=4,'y'=8,'c'=2] {'z','y'}, dimensions={0} | all-to-all | bytes 2621440 | tf_op jit(solution)/shard_map/all_to_all | solution.py:570
  136.2 0.0 copy-start.17
  136.2 0.2 sums.1
  136.4 9.3 %all_to_all.26 = bf16[4,192,128]{2,1,0:T(8,128)(2,1)S(1)} all-to-all(bf16[4,192,128]{2,1,0:T(8,128)(2,1)S(1)} %bitcast.43), channel_id=1, replica_groups=mesh['z'=8,'x'=4,'y'=8,'c'=2] {'x'}, dimensions={0} | all-to-all | bytes 393216 | tf_op jit(solution)/shard_map/all_to_all | solution.py:574
  145.7 0.0 copy-done.3
  145.7 0.0 copy-done.16
  145.7 0.6 collect.1
  146.3 0.0 copy-start.7
  146.3 0.0 copy-start.10
  146.3 0.0 copy-start.11
  146.3 0.0 copy-start.14
  146.3 17.1 %all-gather.1 = bf16[2048,128]{1,0:T(8,128)(2,1)S(1)} all-gather(bf16[128,128]{1,0:T(8,128)(2,1)S(1)} %collect.1), channel_id=3, replica_groups=mesh['z'=8,'x'=4,'y'=8,'c'=2] {'y','c'}, dimensions={0}, use_global_device_ids=true | all-gather | bytes 557056 | tf_op jit(solution)/shard_map/all_gather | solution.py:585
  163.5 0.0 copy-done.6
  163.5 0.0 copy-done.8
  163.5 0.6 head.1
  164.1 13.5 %all_to_all.27.refs_0_ = bf16[4,584,128]{2,1,0:T(8,128)(2,1)S(1)} all-to-all(bf16[4,584,128]{2,1,0:T(8,128)(2,1)S(1)} %get-tuple-element.47), channel_id=1, replica_groups=mesh['z'=8,'x'=4,'y'=8,'c'=2] {'x'}, dimensions={0} | all-to-all | bytes 1196032 | tf_op jit(solution)/shard_map/all_to_all | solution.py:599
  177.5 1.0 group.1
  178.5 4.0 %all-to-all-start.4 = ((bf16[8,136,128]{2,1,0:T(8,128)(2,1)}), bf16[8,136,128]{2,1,0:T(8,128)(2,1)S(1)}, u32[]{:S(2)}, u32[]{:S(2)}) async-start(bf16[8,136,128]{2,1,0:T(8,128)(2,1)} %get-tuple-element.52), calls=%async_computation.4 | async-start | bytes 557056 | tf_op jit(solution)/shard_map/all_to_all | solution.py:612
  182.5 1.7 local.1
  184.3 6.3 %weights.1 = (bf16[1,2048,128]{2,1,0:T(8,128)(2,1)}, bf16[1,2048,128]{2,1,0:T(8,128)(2,1)}, bf16[1,128,2048]{2,1,0:T(8,128)(2,1)}) custom-call(s32[1]{0:T(128)} %bitcast.number, bf16[1280,384]{1,0:T(8,128)(2,1)} %copy-done.5, bf16[1280,1024]{1,0:T(8,128)(2,1)} %bitcast.37, bf16[1280,1024]{1,0:T(8,128)(2,1)} %copy-done.1, f32[8,128]{1,0:T(8,128)} %copy-done.15), custom_call_target="tpu_custom_call" | custom-call | tf_op jit(solution)/shard_map/weights/pallas_call | solution.py:80
  190.5 3.9 %all-to-all-done.4.refs_0_ = bf16[8,136,128]{2,1,0:T(8,128)(2,1)S(1)} async-done(((bf16[8,136,128]{2,1,0:T(8,128)(2,1)}), bf16[8,136,128]{2,1,0:T(8,128)(2,1)S(1)}, u32[]{:S(2)}, u32[]{:S(2)}) %all-to-all-start.4) | async-done | bytes 278560 | tf_op jit(solution)/shard_map/all_to_all | solution.py:612
  194.4 1.4 last.1
  (20 shorter events, 0.1 us)
Async XLA Ops:
  4.2 13.6 %copy-start.18 = (bf16[1,2048,128]{2,1,0:T(8,128)(2,1)S(1)}, bf16[1,2048,128]{2,1,0:T(8,128)(2,1)}, u32[]{:S(2)}) copy-start(bf16[1,2048,128]{2,1,0:T(8,128)(2,1)} %refs_0_.1) | copy-start | bytes 1572868
  4.2 73.7 %all-to-all-start = ((bf16[32,40,1024]{2,1,0:T(8,128)(2,1)}), bf16[32,40,1024]{2,1,0:T(8,128)(2,1)S(1)}, u32[]{:S(2)}, u32[]{:S(2)}) async-start(bf16[32,40,1024]{2,1,0:T(8,128)(2,1)} %dispatch.1.refs_5_), calls=%async_computation | async-start | bytes 5242880 | tf_op jit(solution)/shard_map/all_to_all | solution.py:493
  19.0 4.4 %collective-permute-start = (bf16[2,8,128,128]{3,2,1,0:T(8,128)(2,1)S(1)}, bf16[2,8,128,128]{3,2,1,0:T(8,128)(2,1)S(1)}, u32[]{:S(2)}, u32[]{:S(2)}) collective-permute-start(bf16[2,8,128,128]{3,2,1,0:T(8,128)(2,1)S(1)} %dynamic-slice_bitcast_fusion), channel_id=1, source_target_pairs={{0,1},{1,0},{2,3},{3,2},{4,5},{5,4},{6,7},{7,6},{8,9},{9,8},{10,11... | collective-permute-start | bytes 1572872 | tf_op jit(solution)/shard_map/ppermute | solution.py:497
  23.5 0.8 copy-start.19
  77.9 5.0 %copy-start = (bf16[32,40,1024]{2,1,0:T(8,128)(2,1)}, bf16[32,40,1024]{2,1,0:T(8,128)(2,1)S(1)}, u32[]{:S(2)}) copy-start(bf16[32,40,1024]{2,1,0:T(8,128)(2,1)S(1)} %all-to-all-done) | copy-start | bytes 7864324
  77.9 6.8 %collective-permute-start.1 = (bf16[1280,1024]{1,0:T(8,128)(2,1)S(1)}, bf16[1280,1024]{1,0:T(8,128)(2,1)S(1)}, u32[]{:S(2)}, u32[]{:S(2)}) collective-permute-start(bf16[1280,1024]{1,0:T(8,128)(2,1)S(1)} %bitcast.35), channel_id=1, source_target_pairs={{0,1},{1,0},{2,3},{3,2},{4,5},{5,4},{6,7},{7,6},{8,9},{9,8},{10,11... | collective-permute-start | bytes 7864328 | tf_op jit(solution)/shard_map/ppermute | solution.py:529
  79.8 1.4 copy-start.2
  82.9 5.8 %copy-start.4 = (bf16[512,1024]{1,0:T(8,128)(2,1)S(1)}, bf16[512,1024]{1,0:T(8,128)(2,1)}, u32[]{:S(2)}) copy-start(bf16[512,1024]{1,0:T(8,128)(2,1)} %get-tuple-element.43.refs_1_) | copy-start | bytes 3145732
  84.7 1.8 copy-start.1
  86.5 3.1 %copy-start.5 = (bf16[1280,384]{1,0:T(8,128)(2,1)}, bf16[1280,384]{1,0:T(8,128)(2,1)S(1)}, u32[]{:S(2)}) copy-start(bf16[1280,384]{1,0:T(8,128)(2,1)S(1)} %get-tuple-element.41.refs_0_) | copy-start | bytes 2949124
  89.6 56.1 %copy-start.3 = (bf16[128,2048]{1,0:T(8,128)(2,1)S(1)}, bf16[128,2048]{1,0:T(8,128)(2,1)}, u32[]{:S(2)}) copy-start(bf16[128,2048]{1,0:T(8,128)(2,1)} %refs_2_.5) | copy-start | bytes 1572868
  89.6 56.1 %copy-start.16 = (s32[128,2]{0,1:T(2,128)S(1)}, s32[128,2]{0,1:T(2,128)}, u32[]{:S(2)}) copy-start(s32[128,2]{0,1:T(2,128)} %param.15) | copy-start | bytes 3076
  136.2 27.3 %copy-start.6 = (bf16[2048,128]{1,0:T(8,128)(2,1)S(1)}, bf16[2048,128]{1,0:T(8,128)(2,1)}, u32[]{:S(2)}) copy-start(bf16[2048,128]{1,0:T(8,128)(2,1)} %refs_1_.3) | copy-start | bytes 1572868
  136.2 27.3 %copy-start.8 = (f32[64,128]{1,0:T(8,128)S(1)}, f32[64,128]{1,0:T(8,128)}, u32[]{:S(2)}) copy-start(f32[64,128]{1,0:T(8,128)} %get-tuple-element.44.refs_3_.refs_4_.refs_5_) | copy-start | bytes 98308
  136.2 27.3 %copy-start.9 = (bf16[128,1,64]{0,2,1:T(8,128)(2,1)S(1)}, bf16[128,1,64]{0,2,1:T(8,128)(2,1)}, u32[]{:S(2)}) copy-start(bf16[128,1,64]{0,2,1:T(8,128)(2,1)} %param.21) | copy-start | bytes 49156
  136.2 27.3 %copy-start.12 = (bf16[128,128]{1,0:T(8,128)(2,1)S(1)}, bf16[128,128]{1,0:T(8,128)(2,1)}, u32[]{:S(2)}) copy-start(bf16[128,128]{1,0:T(8,128)(2,1)} %get-tuple-element.45.refs_4_) | copy-start | bytes 98308
  136.2 27.3 %copy-start.17 = (bf16[8,128]{1,0:T(8,128)(2,1)S(1)}, bf16[8,128]{1,0:T(8,128)(2,1)}, u32[]{:S(2)}) copy-start(bf16[8,128]{1,0:T(8,128)(2,1)} %get-tuple-element.46.refs_5_) | copy-start | bytes 6148
  146.3 36.2 %copy-start.7 = (bf16[128,1,128]{2,0,1:T(8,128)(2,1)S(1)}, bf16[128,1,128]{2,0,1:T(8,128)(2,1)}, u32[]{:S(2)}) copy-start(bf16[128,1,128]{2,0,1:T(8,128)(2,1)} %param.23) | copy-start | bytes 98308
  146.3 36.2 %copy-start.10 = (bf16[128,1,64]{0,2,1:T(8,128)(2,1)S(1)}, bf16[128,1,64]{0,2,1:T(8,128)(2,1)}, u32[]{:S(2)}) copy-start(bf16[128,1,64]{0,2,1:T(8,128)(2,1)} %param.22) | copy-start | bytes 49156
  146.3 36.2 %copy-start.11 = (f32[1,1,64,128]{3,2,1,0:T(8,128)S(1)}, f32[1,1,64,128]{3,2,1,0:T(8,128)}, u32[]{:S(2)}) copy-start(f32[1,1,64,128]{3,2,1,0:T(8,128)} %refs_5_.1) | copy-start | bytes 98308
  146.3 36.2 %copy-start.14 = (bf16[128,128]{1,0:T(8,128)(2,1)S(1)}, bf16[128,128]{1,0:T(8,128)(2,1)}, u32[]{:S(2)}) copy-start(bf16[128,128]{1,0:T(8,128)(2,1)} %get-tuple-element.57.refs_6_) | copy-start | bytes 98308
  178.5 5.8 %copy-start.15 = (f32[8,128]{1,0:T(8,128)}, f32[8,128]{1,0:T(8,128)S(1)}, u32[]{:S(2)}) copy-start(f32[8,128]{1,0:T(8,128)S(1)} %get-tuple-element.48.refs_3_.refs_7_) | copy-start | bytes 12292
  178.5 15.9 %all-to-all-start.4 = ((bf16[8,136,128]{2,1,0:T(8,128)(2,1)}), bf16[8,136,128]{2,1,0:T(8,128)(2,1)S(1)}, u32[]{:S(2)}, u32[]{:S(2)}) async-start(bf16[8,136,128]{2,1,0:T(8,128)(2,1)} %get-tuple-element.52), calls=%async_computation.4 | async-start | bytes 557056 | tf_op jit(solution)/shard_map/all_to_all | solution.py:612
  184.3 10.1 %copy-start.13 = (f32[64,128]{1,0:T(8,128)S(1)}, f32[64,128]{1,0:T(8,128)}, u32[]{:S(2)}) copy-start(f32[64,128]{1,0:T(8,128)} %get-tuple-element.55.refs_6_) | copy-start | bytes 98308

commit v7 on v6

--- a/solution.py
+++ b/solution.py
@@ -156,11 +156,19 @@
     return jnp.concatenate([a[4:8], a[0:4]], axis=0)
 
 
+def part_at(at, n):
+    core = at[1] if n < 2 else 1 - at[1]
+    return 2 * core + (at[5] if n % 2 == 0 else 1 - at[5])
+
+
 def layout_kernel(at, wg_ref, wu_ref, wd_ref, woth_ref, side_ref, back_ref):
-    side_ref[:, 0:128] = wg_ref[0]
-    side_ref[:, 128:256] = wu_ref[0]
-    for t in range(0, side_ref.shape[0], 128):
-        side_ref[t : t + 128, 256:384] = wd_ref[0, :, t : t + 128].astype(F32).T.astype(BF)
+    part = side_ref.shape[0] // 4
+    for n in range(4):
+        first = pl.multiple_of(part_at(at, n) * part, 128)
+        to = slice(n * part, (n + 1) * part)
+        side_ref[to, 0:128] = wg_ref[0, pl.ds(first, part), :]
+        side_ref[to, 128:256] = wu_ref[0, pl.ds(first, part), :]
+        side_ref[to, 256:384] = wd_ref[0, :, pl.ds(first, part)].astype(F32).T.astype(BF)
     for y in range(back_ref.shape[1] // 128):
         first = pl.multiple_of((2 * y + at[1]) * 128, 128)
         for n, w in enumerate(
@@ -178,14 +186,17 @@
     out_ref[...] = dot(g_ref[...], w_ref[...])
 
 
-def delta_kernel(at, g_ref, w_ref, acc_ref, delta_ref, pack_ref):
-    sums = dot(g_ref[...], w_ref[...]) + acc_ref[...]
+def delta_kernel(at, other_ref, rest_ref, beside_ref, w_ref, acc_ref, delta_ref, pack_ref):
+    part = rest_ref.shape[1]
+    sums = acc_ref[...] + dot(rest_ref[...], w_ref[part : 2 * part, :])
+    sums = sums + dot(other_ref[...], w_ref[2 * part : 3 * part, :])
+    sums = sums + dot(beside_ref[...], w_ref[3 * part : 4 * part, :])
     gu, yh = sums[:, 0:256], sums[:, 256:384]
     low = iota((8, 128), 0) < 4
     zero8 = jnp.zeros((8, 128), F32)
     dgs, dus, dhs, pgs, pus = [], [], [], [], []
     mixed = []
-    spans = g_ref.shape[0] // 40
+    spans = rest_ref.shape[0] // 40
     for d in range(spans):
         b = 40 * d
         pg, pu = gu[b : b + 24, 0:128], gu[b : b + 24, 128:256]
@@ -225,17 +236,18 @@
             out_ref[z, y + 1] = o[z * rows : (z + 1) * rows, 128:256]
 
 
-def weight_kernel(at, delta_ref, own_ref, other_ref, gate_ref, up_ref, down_ref, dt_ref):
-    rows, half = own_ref.shape
+def weight_kernel(at, delta_ref, a_ref, b_ref, c_ref, d_ref, gate_ref, up_ref, down_ref, dt_ref):
+    rows, part = a_ref.shape
     for r in range(0, rows, 128):
         dt_ref[:, r : r + 128] = delta_ref[r : r + 128, :].astype(F32).T.astype(BF)
-    for g_ref, core in ((own_ref, at[1]), (other_ref, 1 - at[1])):
-        for p in range(0, half, 256):
-            o = dot(dt_ref[...], g_ref[:, p : p + 256])
-            first = pl.multiple_of(core * half + p, 256)
-            gate_ref[0, pl.ds(first, 256), :] = o[0:128].T.astype(BF)
-            up_ref[0, pl.ds(first, 256), :] = o[128:256].T.astype(BF)
-            down_ref[0, :, pl.ds(first, 256)] = o[256:384].astype(BF)
+    for n, g_ref in enumerate((a_ref, b_ref, c_ref, d_ref)):
+        wide = min(256, part)
+        for p in range(0, part, wide):
+            o = dot(dt_ref[...], g_ref[:, p : p + wide])
+            first = pl.multiple_of(part_at(at, n) * part + p, 128)
+            gate_ref[0, pl.ds(first, wide), :] = o[0:128].T.astype(BF)
+            up_ref[0, pl.ds(first, wide), :] = o[128:256].T.astype(BF)
+            down_ref[0, :, pl.ds(first, wide)] = o[256:384].astype(BF)
 
 
 def sum_kernel(at, got_ref, out_ref):
@@ -465,7 +477,7 @@
     slices = ny * 2
     core = lax.axis_index("c")
     place = lax.axis_index(("z", "x", "y", "c")).astype(jnp.int32)
-    sizes = ((1, slices), (1, 2), (slices, spans), (slices * nx, nz), (slices, nx))
+    sizes = ((1, slices), (1, 2), (slices, spans), (slices * nx, nz), (slices, nx), (2, 2))
     at = Place(place.reshape(1), sizes)
     width = queries.shape[2]
     piece_rows = slices * 128 // spans
@@ -477,20 +489,21 @@
     g = log_decay.reshape(tokens, width).T
     slice_block = ((tokens, 128), lambda i, s: (0, s[0]))
     half = slices * 64
-    half_block = ((tokens, half), lambda i, s: (0, s[1]))
+    part = half // 2
+    part_block = ((tokens, part), lambda i, s: (0, part_at(s, 0)))
 
     (sent,) = call(
         dispatch_kernel,
         "dispatch",
-        (sds((spans, 40, half), BF),),
+        (sds((spans, 40, part), BF),),
         at,
         routes,
         route_weight,
         expert_input,
         cotangent,
-        blocks={2: half_block, 3: half_block},
-    )
-    own = lax.all_to_all(sent, SP, 0, 0, tiled=True).reshape(spans * 40, half)
+        blocks={2: part_block, 3: part_block},
+    )
+    own = lax.all_to_all(sent, SP, 0, 0, tiled=True).reshape(spans * 40, part)
 
     weights = jnp.stack([gate_weight[0], up_weight[0]]).reshape(2, ny, 2, 128, 128)
     weights = lax.dynamic_index_in_dim(weights, 1 - core, 2, keepdims=False)
@@ -526,10 +539,15 @@
     )
     own, mixed, side = lax.optimization_barrier((own, mixed, side))
 
-    other = lax.ppermute(own, "c", [(0, 1), (1, 0)])
     rows_all = spans * 40
+    swap = [(0, 1), (1, 0)]
+    up = [(i, (i + 1) % ny) for i in range(ny)]
+    down = [(i, (i - 1) % ny) for i in range(ny)]
+    low = lax.ppermute(own[: rows_all // 2], "y", up)
+    high = lax.ppermute(own[rows_all // 2 :], "y", down)
+    other = lax.ppermute(own, "c", swap)
     tile = rows_all // TILES
-    rows_block = ((tile, half), lambda i, s: (i, 0))
+    part_rows = ((tile, part), lambda i, s: (i, 0))
     acc_block = ((tile, 384), lambda i, s: (i, 0))
     (acc,) = call(
         first_kernel,
@@ -538,23 +556,24 @@
         at,
         own,
         side,
-        blocks={0: rows_block, 1: ((half, 384), lambda i, s: (s[1], 0))},
+        blocks={0: part_rows, 1: ((part, 384), lambda i, s: (0, 0))},
         out_blocks={0: acc_block},
         grid=TILES,
     )
+    low, high, acc, other = lax.optimization_barrier((low, high, acc, other))
+    rest = jnp.concatenate([low, high], axis=0)
+    beside = lax.ppermute(rest, "c", swap)
     delta, pack = call(
         delta_kernel,
         "deltas",
         (sds((rows_all, 384), BF), sds((rows_all // 2, 256), BF)),
         at,
         other,
+        rest,
+        beside,
         side,
         acc,
-        blocks={
-            0: rows_block,
-            1: ((half, 384), lambda i, s: (1 - s[1], 0)),
-            2: acc_block,
-        },
+        blocks={0: part_rows, 1: part_rows, 2: part_rows, 4: acc_block},
         out_blocks={0: acc_block, 1: ((tile // 2, 256), lambda i, s: (i, 0))},
         grid=TILES,
     )
@@ -621,7 +640,9 @@
         at,
         delta,
         own,
+        rest,
         other,
+        beside,
         scratch=[pltpu.VMEM((384, spans * 40), BF)],
         after=(token,),
     )

time: 197 us -> 191 us (0.970)
  starting transfers between devices: 21.4 us -> 30.9 us
  waiting for transfers between devices: 55.6 us -> 47.8 us
  blocking collectives: 88.7 us -> 84.7 us
    all_to_all x1, waiting for transfers between devices: 50 us -> 23.9 us  [on_device(): own = lax.all_to_all(sent, SP, 0, 0, tiled=True).reshape(spans * 40, part)]
    ppermute x1 -> x4, waiting for transfers between devices: 1.74 us -> 20 us  [the longest x1 11.6 us: on_device(): high = lax.ppermute(own[rows_all // 2:], 'y', down)]
    ppermute x1 -> x4, starting transfers between devices: 1.91 us -> 11.4 us  [the longest x1 5.37 us: on_device(): high = lax.ppermute(own[rows_all // 2:], 'y', down)]
    all_to_all x1, blocking collectives: 46.5 us -> 42.5 us  [on_device(): lax.all_to_all(terms.reshape(nz * ny, nx * 20, 128), ('z', 'y'), 0, 0, ti...]
  transfers between devices with their start and end apart: 4 -> 7, of which waited for: 3 -> 5; matrix products, arithmetic and copies ran while one was open for 1% -> 0% of each run, Pallas kernels for 8% -> 8%
where the time goes in v7:
time: 191 us; the launch traced here: 190 us
  blocking collectives  84.7 us (44%)
  waiting for transfers between devices  47.8 us (25%)
  starting transfers between devices  30.9 us (16%)
  Pallas kernels  24.8 us (13%)
    all_to_all x1, blocking collectives, on_device(): lax.all_to_all(terms.reshape(nz * ny, nx * 20, 128), ('z', 'y'), 0, 0, ti...  42.5 us
    pallas_call x13, Pallas kernels, call(): pl.pallas_call(body, name=name, out_shape=outs, grid_spec=pltpu.PrefetchS...  24.8 us
    all_to_all x1, waiting for transfers between devices, on_device(): own = lax.all_to_all(sent, SP, 0, 0, tiled=True).reshape(spans * 40, part)  23.9 us
    all_gather x1, blocking collectives, on_device(): total_grad = lax.all_gather(slice_grad, TP, axis=0)  17.1 us
    all_to_all x1, starting transfers between devices, on_device(): own = lax.all_to_all(sent, SP, 0, 0, tiled=True).reshape(spans * 40, part)  13.6 us
    all_to_all x1, blocking collectives, on_device(): crossing = lax.all_to_all(leaving, 'x', 0, 0, tiled=True)  13.6 us
    ppermute x1, waiting for transfers between devices, on_device(): high = lax.ppermute(own[rows_all // 2:], 'y', down)  11.6 us
    all_to_all x1, blocking collectives, on_device(): lax.all_to_all(summed.reshape(nx, nz * 24, 128), 'x', 0, 0, tiled=True)  9.3 us
  transfers between devices with their start and end apart: 7, of which 5 were waited for; matrix products, arithmetic and copies ran while one was open for 0% of the time, Pallas kernels for 8%

profile of v7, /device:TPU:2, one launch (start us, length us, event | category | flops | bytes accessed | tf_op | source)
XLA Modules:
  0.0 190.4 jit_solution(6069014447992461386)
XLA Ops:
  0.6 2.8 %dispatch.1.refs_5_ = bf16[32,40,512]{2,1,0:T(8,128)(2,1)} custom-call(s32[1]{0:T(128)} %bitcast.number, s32[2,128]{1,0:T(2,128)} %bitcast.54, f32[2,128]{1,0:T(2,128)} %bitcast.58, bf16[128,2048]{1,0:T(8,128)(2,1)} %refs_2_.3, bf16[128,2048]{1,0:T(8,128)(2,1)} %refs_2_.5), custom_call_target="tpu_custom_call" | custom-call | tf_op jit(solution)/shard_map/dispatch/pallas_call | solution.py:80
  3.4 13.6 %all-to-all-start = ((bf16[32,40,512]{2,1,0:T(8,128)(2,1)}), bf16[32,40,512]{2,1,0:T(8,128)(2,1)S(1)}, u32[]{:S(2)}, u32[]{:S(2)}) async-start(bf16[32,40,512]{2,1,0:T(8,128)(2,1)} %dispatch.1.refs_5_), calls=%async_computation | async-start | bytes 2621440 | tf_op jit(solution)/shard_map/all_to_all | solution.py:506
  17.0 0.1 pad_maximum_fusion
  17.2 1.9 %collective-permute-start = (bf16[2,8,128,128]{3,2,1,0:T(8,128)(2,1)S(1)}, bf16[2,8,128,128]{3,2,1,0:T(8,128)(2,1)S(1)}, u32[]{:S(2)}, u32[]{:S(2)}) collective-permute-start(bf16[2,8,128,128]{3,2,1,0:T(8,128)(2,1)S(1)} %dynamic-slice_bitcast_fusion), channel_id=1, source_target_pairs={{0,1},{1,0},{2,3},{3,2},{4,5},{5,4},{6,7},{7,6},{8,9},{9,8},{10,11... | collective-permute-start | bytes 1572872 | tf_op jit(solution)/shard_map/ppermute | solution.py:510
  19.1 2.5 %forward.1 = (bf16[128,128]{1,0:T(8,128)(2,1)}, bf16[128,128]{1,0:T(8,128)(2,1)}, f32[64,128]{1,0:T(8,128)}, f32[64,128]{1,0:T(8,128)}, bf16[8,128]{1,0:T(8,128)(2,1)}) custom-call(s32[1]{0:T(128)} %bitcast.number, bf16[64,128]{1,0:T(8,128)(2,1)} %bitcast.48, bf16[64,128]{1,0:T(8,128)(2,1)} %bitcast.51, bf16[128,128]{1,0:T(8,128)(2,1)} %bitcast.45, ...), custom_call_target="tpu_custom_call" | custom-call | tf_op jit(solution)/shard_map/forward/pallas_call | solution.py:80
  21.6 0.0 collective-permute-done.refs_3_
  21.6 0.8 copy-done.22
  22.4 3.6 %layout.1 = (bf16[2048,384]{1,0:T(8,128)(2,1)}, bf16[512,1024]{1,0:T(8,128)(2,1)}) custom-call(s32[1]{0:T(128)} %bitcast.number, bf16[1,2048,128]{2,1,0:T(8,128)(2,1)} %refs_0_.1, bf16[1,2048,128]{2,1,0:T(8,128)(2,1)} %refs_1_.2, bf16[1,128,2048]{2,1,0:T(8,128)(2,1)} %refs_2_.4, bf16[2,8,128,128]{3,2,1,0:T(8,128)(2,1)} %copy-done.22, ...), custom_call_target="tpu_custom_call" | custom-call | tf_op jit(solution)/shard_map/layout/pallas_call | solution.py:80
  26.0 23.9 %all-to-all-done = bf16[32,40,512]{2,1,0:T(8,128)(2,1)S(1)} async-done(((bf16[32,40,512]{2,1,0:T(8,128)(2,1)}), bf16[32,40,512]{2,1,0:T(8,128)(2,1)S(1)}, u32[]{:S(2)}, u32[]{:S(2)}) %all-to-all-start) | async-done | bytes 1310752 | tf_op jit(solution)/shard_map/all_to_all | solution.py:506
  49.9 2.2 %collective-permute-start.3 = (bf16[1280,512]{1,0:T(8,128)(2,1)S(1)}, bf16[1280,512]{1,0:T(8,128)(2,1)S(1)}, u32[]{:S(2)}, u32[]{:S(2)}) collective-permute-start(bf16[1280,512]{1,0:T(8,128)(2,1)S(1)} %bitcast.35), channel_id=1, source_target_pairs={{0,1},{1,0},{2,3},{3,2},{4,5},{5,4},{6,7},{7,6},{8,9},{9,8},{10,11... | collective-permute-start | bytes 3932168 | tf_op jit(solution)/shard_map/ppermute | solution.py:548
  52.1 0.1 fusion
  52.2 5.4 %collective-permute-start.2 = (bf16[640,512]{1,0:T(8,128)(2,1)S(1)}, bf16[640,512]{1,0:T(8,128)(2,1)S(1)}, u32[]{:S(2)}, u32[]{:S(2)}) collective-permute-start(bf16[640,512]{1,0:T(8,128)(2,1)S(1)} %get-tuple-element.74), channel_id=1, source_target_pairs={{0,14},{2,0},{4,2},{6,4},{8,6},{10,8},{12,10},{14,12},{1,15},{3,1}... | collective-permute-start | bytes 1966088 | tf_op jit(solution)/shard_map/ppermute | solution.py:547
  57.6 1.9 %collective-permute-start.1 = (bf16[640,512]{1,0:T(8,128)(2,1)S(1)}, bf16[640,512]{1,0:T(8,128)(2,1)S(1)}, u32[]{:S(2)}, u32[]{:S(2)}) collective-permute-start(bf16[640,512]{1,0:T(8,128)(2,1)S(1)} %get-tuple-element.75), channel_id=1, source_target_pairs={{0,2},{2,4},{4,6},{6,8},{8,10},{10,12},{12,14},{14,0},{1,3},{3,5},... | collective-permute-start | bytes 1966088 | tf_op jit(solution)/shard_map/ppermute | solution.py:546
  59.5 0.0 copy-done
  59.5 0.0 copy-done.2
  59.5 1.0 first.1.refs_4_
  60.6 11.6 %collective-permute-done.2 = bf16[640,512]{1,0:T(8,128)(2,1)S(1)} collective-permute-done((bf16[640,512]{1,0:T(8,128)(2,1)S(1)}, bf16[640,512]{1,0:T(8,128)(2,1)S(1)}, u32[]{:S(2)}, u32[]{:S(2)}) %collective-permute-start.2) | collective-permute-done | bytes 655392 | tf_op jit(solution)/shard_map/ppermute | solution.py:547
  72.2 5.3 %collective-permute-done.1 = bf16[640,512]{1,0:T(8,128)(2,1)S(1)} collective-permute-done((bf16[640,512]{1,0:T(8,128)(2,1)S(1)}, bf16[640,512]{1,0:T(8,128)(2,1)S(1)}, u32[]{:S(2)}, u32[]{:S(2)}) %collective-permute-start.1) | collective-permute-done | bytes 655392 | tf_op jit(solution)/shard_map/ppermute | solution.py:546
  77.5 0.0 collective-permute-done.3.refs_0_.refs_3_
  77.7 1.9 %collective-permute-start.4 = (bf16[1280,512]{1,0:T(8,128)(2,1)S(1)}, bf16[1280,512]{1,0:T(8,128)(2,1)S(1)}, u32[]{:S(2)}, u32[]{:S(2)}) collective-permute-start(bf16[1280,512]{1,0:T(8,128)(2,1)S(1)} %constant_dynamic-update-slice_fusion.refs_1_.refs_2_), channel_id=1, source_target_pairs={{0,1},{1,0},{2,3},{3,2},{4,5},{5,4},{6,7},{7,6},{8,9},{9,8},{10,11... | collective-permute-start | bytes 3932168 | tf_op jit(solution)/shard_map/ppermute | solution.py:565
  79.6 3.0 %collective-permute-done.4.refs_2_.refs_4_ = bf16[1280,512]{1,0:T(8,128)(2,1)S(1)} collective-permute-done((bf16[1280,512]{1,0:T(8,128)(2,1)S(1)}, bf16[1280,512]{1,0:T(8,128)(2,1)S(1)}, u32[]{:S(2)}, u32[]{:S(2)}) %collective-permute-start.4) | collective-permute-done | bytes 1310752 | tf_op jit(solution)/shard_map/ppermute | solution.py:565
  82.6 2.4 %deltas.1 = (bf16[1280,384]{1,0:T(8,128)(2,1)S(1)}, bf16[640,256]{1,0:T(8,128)(2,1)S(1)}) custom-call(s32[1]{0:T(128)} %bitcast.number, bf16[1280,512]{1,0:T(8,128)(2,1)S(1)} %collective-permute-done.3.refs_0_.refs_3_, bf16[1280,512]{1,0:T(8,128)(2,1)S(1)} %constant_dynamic-update-slice_fusion.refs_1_.refs_2_, ...), custom_call_target="tpu_custom_call" | custom-call | tf_op jit(solution)/shard_map/deltas/pallas_call | solution.py:80
  85.0 0.0 copy-done.1
  85.0 0.0 copy-done.4
  85.1 0.0 copy-start.7
  85.1 2.3 %all-gather = bf16[1280,256]{1,0:T(8,128)(2,1)S(1)} all-gather(bf16[640,256]{1,0:T(8,128)(2,1)S(1)} %get-tuple-element.50), channel_id=2, replica_groups=mesh['z'=8,'x'=4,'y'=8,'c'=2] {'c'}, dimensions={0}, use_global_device_ids=true | all-gather | bytes 983040 | tf_op jit(solution)/shard_map/all_gather | solution.py:580
  87.3 0.8 partials.1
  88.2 42.5 %all_to_all.25 = bf16[64,80,128]{2,1,0:T(8,128)(2,1)S(1)} all-to-all(bf16[64,80,128]{2,1,0:T(8,128)(2,1)S(1)} %bitcast.39), channel_id=1, replica_groups=mesh['z'=8,'x'=4,'y'=8,'c'=2] {'z','y'}, dimensions={0} | all-to-all | bytes 2621440 | tf_op jit(solution)/shard_map/all_to_all | solution.py:589
  130.7 0.0 copy-start.11
  130.7 0.0 copy-start.13
  130.7 0.0 copy-start.19
  130.7 0.2 sums.1
  130.9 9.3 %all_to_all.26 = bf16[4,192,128]{2,1,0:T(8,128)(2,1)S(1)} all-to-all(bf16[4,192,128]{2,1,0:T(8,128)(2,1)S(1)} %bitcast.44), channel_id=1, replica_groups=mesh['z'=8,'x'=4,'y'=8,'c'=2] {'x'}, dimensions={0} | all-to-all | bytes 393216 | tf_op jit(solution)/shard_map/all_to_all | solution.py:593
  140.2 0.6 collect.1
  140.8 17.1 %all-gather.1 = bf16[2048,128]{1,0:T(8,128)(2,1)S(1)} all-gather(bf16[128,128]{1,0:T(8,128)(2,1)S(1)} %collect.1), channel_id=3, replica_groups=mesh['z'=8,'x'=4,'y'=8,'c'=2] {'y','c'}, dimensions={0}, use_global_device_ids=true | all-gather | bytes 557056 | tf_op jit(solution)/shard_map/all_gather | solution.py:604
  157.9 0.0 copy-done.8
  157.9 0.6 head.1
  158.5 0.0 copy-start.10
  158.5 0.0 copy-start.12
  158.5 0.0 copy-start.14
  158.6 0.0 copy-start.16
  158.6 13.6 %all_to_all.27.refs_0_ = bf16[4,584,128]{2,1,0:T(8,128)(2,1)S(1)} all-to-all(bf16[4,584,128]{2,1,0:T(8,128)(2,1)S(1)} %get-tuple-element.55), channel_id=1, replica_groups=mesh['z'=8,'x'=4,'y'=8,'c'=2] {'x'}, dimensions={0} | all-to-all | bytes 1196032 | tf_op jit(solution)/shard_map/all_to_all | solution.py:618
  172.2 1.0 group.1
  173.1 4.0 %all-to-all-start.4 = ((bf16[8,136,128]{2,1,0:T(8,128)(2,1)}), bf16[8,136,128]{2,1,0:T(8,128)(2,1)S(1)}, u32[]{:S(2)}, u32[]{:S(2)}) async-start(bf16[8,136,128]{2,1,0:T(8,128)(2,1)} %get-tuple-element.60), calls=%async_computation.4 | async-start | bytes 557056 | tf_op jit(solution)/shard_map/all_to_all | solution.py:631
  177.2 1.7 local.1
  178.9 6.3 %weights.1 = (bf16[1,2048,128]{2,1,0:T(8,128)(2,1)}, bf16[1,2048,128]{2,1,0:T(8,128)(2,1)}, bf16[1,128,2048]{2,1,0:T(8,128)(2,1)}) custom-call(s32[1]{0:T(128)} %bitcast.number, bf16[1280,384]{1,0:T(8,128)(2,1)} %copy-done.7, bf16[1280,512]{1,0:T(8,128)(2,1)} %bitcast.38, bf16[1280,512]{1,0:T(8,128)(2,1)} %copy-done.1, bf16[1280,512]{1,0:T(8,128)(2,1)} %copy-done.3, ...), custom_call_target="tpu_custom_call" | custom-call | tf_op jit(solution)/shard_map/weights/pallas_call | solution.py:80
  185.2 3.9 %all-to-all-done.4.refs_0_ = bf16[8,136,128]{2,1,0:T(8,128)(2,1)S(1)} async-done(((bf16[8,136,128]{2,1,0:T(8,128)(2,1)}), bf16[8,136,128]{2,1,0:T(8,128)(2,1)S(1)}, u32[]{:S(2)}, u32[]{:S(2)}) %all-to-all-start.4) | async-done | bytes 278560 | tf_op jit(solution)/shard_map/all_to_all | solution.py:631
  189.0 1.4 last.1
  (35 shorter events, 0.2 us)
Async XLA Ops:
  3.4 13.6 %copy-start.20 = (bf16[1,2048,128]{2,1,0:T(8,128)(2,1)S(1)}, bf16[1,2048,128]{2,1,0:T(8,128)(2,1)}, u32[]{:S(2)}) copy-start(bf16[1,2048,128]{2,1,0:T(8,128)(2,1)} %refs_0_.1) | copy-start | bytes 1572868
  3.4 13.6 %copy-start.21 = (bf16[1,2048,128]{2,1,0:T(8,128)(2,1)S(1)}, bf16[1,2048,128]{2,1,0:T(8,128)(2,1)}, u32[]{:S(2)}) copy-start(bf16[1,2048,128]{2,1,0:T(8,128)(2,1)} %refs_1_.2) | copy-start | bytes 1572868
  3.4 46.5 %all-to-all-start = ((bf16[32,40,512]{2,1,0:T(8,128)(2,1)}), bf16[32,40,512]{2,1,0:T(8,128)(2,1)S(1)}, u32[]{:S(2)}, u32[]{:S(2)}) async-start(bf16[32,40,512]{2,1,0:T(8,128)(2,1)} %dispatch.1.refs_5_), calls=%async_computation | async-start | bytes 2621440 | tf_op jit(solution)/shard_map/all_to_all | solution.py:506
  17.2 4.4 %collective-permute-start = (bf16[2,8,128,128]{3,2,1,0:T(8,128)(2,1)S(1)}, bf16[2,8,128,128]{3,2,1,0:T(8,128)(2,1)S(1)}, u32[]{:S(2)}, u32[]{:S(2)}) collective-permute-start(bf16[2,8,128,128]{3,2,1,0:T(8,128)(2,1)S(1)} %dynamic-slice_bitcast_fusion), channel_id=1, source_target_pairs={{0,1},{1,0},{2,3},{3,2},{4,5},{5,4},{6,7},{7,6},{8,9},{9,8},{10,11... | collective-permute-start | bytes 1572872 | tf_op jit(solution)/shard_map/ppermute | solution.py:510
  21.6 0.8 copy-start.22
  49.9 9.6 %copy-start = (bf16[32,40,512]{2,1,0:T(8,128)(2,1)}, bf16[32,40,512]{2,1,0:T(8,128)(2,1)S(1)}, u32[]{:S(2)}) copy-start(bf16[32,40,512]{2,1,0:T(8,128)(2,1)S(1)} %all-to-all-done) | copy-start | bytes 3932164
  49.9 9.6 %copy-start.2 = (bf16[2048,384]{1,0:T(8,128)(2,1)S(1)}, bf16[2048,384]{1,0:T(8,128)(2,1)}, u32[]{:S(2)}) copy-start(bf16[2048,384]{1,0:T(8,128)(2,1)} %get-tuple-element.44.refs_1_.refs_3_) | copy-start | bytes 4718596
  49.9 27.6 %collective-permute-start.3 = (bf16[1280,512]{1,0:T(8,128)(2,1)S(1)}, bf16[1280,512]{1,0:T(8,128)(2,1)S(1)}, u32[]{:S(2)}, u32[]{:S(2)}) collective-permute-start(bf16[1280,512]{1,0:T(8,128)(2,1)S(1)} %bitcast.35), channel_id=1, source_target_pairs={{0,1},{1,0},{2,3},{3,2},{4,5},{5,4},{6,7},{7,6},{8,9},{9,8},{10,11... | collective-permute-start | bytes 3932168 | tf_op jit(solution)/shard_map/ppermute | solution.py:548
  52.2 20.0 %collective-permute-start.2 = (bf16[640,512]{1,0:T(8,128)(2,1)S(1)}, bf16[640,512]{1,0:T(8,128)(2,1)S(1)}, u32[]{:S(2)}, u32[]{:S(2)}) collective-permute-start(bf16[640,512]{1,0:T(8,128)(2,1)S(1)} %get-tuple-element.74), channel_id=1, source_target_pairs={{0,14},{2,0},{4,2},{6,4},{8,6},{10,8},{12,10},{14,12},{1,15},{3,1}... | collective-permute-start | bytes 1966088 | tf_op jit(solution)/shard_map/ppermute | solution.py:547
  57.6 20.0 %collective-permute-start.1 = (bf16[640,512]{1,0:T(8,128)(2,1)S(1)}, bf16[640,512]{1,0:T(8,128)(2,1)S(1)}, u32[]{:S(2)}, u32[]{:S(2)}) collective-permute-start(bf16[640,512]{1,0:T(8,128)(2,1)S(1)} %get-tuple-element.75), channel_id=1, source_target_pairs={{0,2},{2,4},{4,6},{6,8},{8,10},{10,12},{12,14},{14,0},{1,3},{3,5},... | collective-permute-start | bytes 1966088 | tf_op jit(solution)/shard_map/ppermute | solution.py:546
  77.5 5.0 %copy-start.3 = (bf16[1280,512]{1,0:T(8,128)(2,1)}, bf16[1280,512]{1,0:T(8,128)(2,1)S(1)}, u32[]{:S(2)}) copy-start(bf16[1280,512]{1,0:T(8,128)(2,1)S(1)} %collective-permute-done.3.refs_0_.refs_3_) | copy-start | bytes 3932164
  77.6 7.4 %copy-start.1 = (bf16[1280,512]{1,0:T(8,128)(2,1)}, bf16[1280,512]{1,0:T(8,128)(2,1)S(1)}, u32[]{:S(2)}) copy-start(bf16[1280,512]{1,0:T(8,128)(2,1)S(1)} %constant_dynamic-update-slice_fusion.refs_1_.refs_2_) | copy-start | bytes 3932164
  77.7 4.9 %collective-permute-start.4 = (bf16[1280,512]{1,0:T(8,128)(2,1)S(1)}, bf16[1280,512]{1,0:T(8,128)(2,1)S(1)}, u32[]{:S(2)}, u32[]{:S(2)}) collective-permute-start(bf16[1280,512]{1,0:T(8,128)(2,1)S(1)} %constant_dynamic-update-slice_fusion.refs_1_.refs_2_), channel_id=1, source_target_pairs={{0,1},{1,0},{2,3},{3,2},{4,5},{5,4},{6,7},{7,6},{8,9},{9,8},{10,11... | collective-permute-start | bytes 3932168 | tf_op jit(solution)/shard_map/ppermute | solution.py:565
  82.6 2.5 %copy-start.4 = (bf16[1280,512]{1,0:T(8,128)(2,1)}, bf16[1280,512]{1,0:T(8,128)(2,1)S(1)}, u32[]{:S(2)}) copy-start(bf16[1280,512]{1,0:T(8,128)(2,1)S(1)} %collective-permute-done.4.refs_2_.refs_4_) | copy-start | bytes 3932164
  82.6 4.8 %copy-start.6 = (bf16[512,1024]{1,0:T(8,128)(2,1)S(1)}, bf16[512,1024]{1,0:T(8,128)(2,1)}, u32[]{:S(2)}) copy-start(bf16[512,1024]{1,0:T(8,128)(2,1)} %get-tuple-element.51.refs_1_) | copy-start | bytes 3145732
  85.1 3.1 %copy-start.7 = (bf16[1280,384]{1,0:T(8,128)(2,1)}, bf16[1280,384]{1,0:T(8,128)(2,1)S(1)}, u32[]{:S(2)}) copy-start(bf16[1280,384]{1,0:T(8,128)(2,1)S(1)} %get-tuple-element.49.refs_0_) | copy-start | bytes 2949124
  130.7 9.5 %copy-start.5 = (bf16[128,2048]{1,0:T(8,128)(2,1)S(1)}, bf16[128,2048]{1,0:T(8,128)(2,1)}, u32[]{:S(2)}) copy-start(bf16[128,2048]{1,0:T(8,128)(2,1)} %refs_2_.5) | copy-start | bytes 1572868
  130.7 9.5 %copy-start.18 = (s32[128,2]{0,1:T(2,128)S(1)}, s32[128,2]{0,1:T(2,128)}, u32[]{:S(2)}) copy-start(s32[128,2]{0,1:T(2,128)} %param.15) | copy-start | bytes 3076
  130.7 27.2 %copy-start.8 = (bf16[2048,128]{1,0:T(8,128)(2,1)S(1)}, bf16[2048,128]{1,0:T(8,128)(2,1)}, u32[]{:S(2)}) copy-start(bf16[2048,128]{1,0:T(8,128)(2,1)} %refs_1_.3) | copy-start | bytes 1572868
  130.7 27.2 %copy-start.9 = (f32[64,128]{1,0:T(8,128)S(1)}, f32[64,128]{1,0:T(8,128)}, u32[]{:S(2)}) copy-start(f32[64,128]{1,0:T(8,128)} %get-tuple-element.52.refs_3_.refs_4_.refs_5_) | copy-start | bytes 98308
  130.7 27.2 %copy-start.11 = (bf16[128,1,64]{0,2,1:T(8,128)(2,1)S(1)}, bf16[128,1,64]{0,2,1:T(8,128)(2,1)}, u32[]{:S(2)}) copy-start(bf16[128,1,64]{0,2,1:T(8,128)(2,1)} %param.21) | copy-start | bytes 49156
  130.7 27.2 %copy-start.13 = (bf16[128,128]{1,0:T(8,128)(2,1)S(1)}, bf16[128,128]{1,0:T(8,128)(2,1)}, u32[]{:S(2)}) copy-start(bf16[128,128]{1,0:T(8,128)(2,1)} %get-tuple-element.53.refs_4_) | copy-start | bytes 98308
  130.7 27.2 %copy-start.19 = (bf16[8,128]{1,0:T(8,128)(2,1)S(1)}, bf16[8,128]{1,0:T(8,128)(2,1)}, u32[]{:S(2)}) copy-start(bf16[8,128]{1,0:T(8,128)(2,1)} %get-tuple-element.54.refs_5_) | copy-start | bytes 6148
  158.5 18.6 %copy-start.10 = (bf16[128,1,128]{2,0,1:T(8,128)(2,1)S(1)}, bf16[128,1,128]{2,0,1:T(8,128)(2,1)}, u32[]{:S(2)}) copy-start(bf16[128,1,128]{2,0,1:T(8,128)(2,1)} %param.23) | copy-start | bytes 98308
  158.5 18.6 %copy-start.12 = (bf16[128,1,64]{0,2,1:T(8,128)(2,1)S(1)}, bf16[128,1,64]{0,2,1:T(8,128)(2,1)}, u32[]{:S(2)}) copy-start(bf16[128,1,64]{0,2,1:T(8,128)(2,1)} %param.22) | copy-start | bytes 49156
  158.5 18.6 %copy-start.14 = (f32[1,1,64,128]{3,2,1,0:T(8,128)S(1)}, f32[1,1,64,128]{3,2,1,0:T(8,128)}, u32[]{:S(2)}) copy-start(f32[1,1,64,128]{3,2,1,0:T(8,128)} %refs_5_.1) | copy-start | bytes 98308
  158.6 18.6 %copy-start.16 = (bf16[128,128]{1,0:T(8,128)(2,1)S(1)}, bf16[128,128]{1,0:T(8,128)(2,1)}, u32[]{:S(2)}) copy-start(bf16[128,128]{1,0:T(8,128)(2,1)} %get-tuple-element.65.refs_6_) | copy-start | bytes 98308
  173.1 5.8 %copy-start.17 = (f32[8,128]{1,0:T(8,128)}, f32[8,128]{1,0:T(8,128)S(1)}, u32[]{:S(2)}) copy-start(f32[8,128]{1,0:T(8,128)S(1)} %get-tuple-element.56.refs_5_.refs_7_) | copy-start | bytes 12292
  173.1 15.9 %all-to-all-start.4 = ((bf16[8,136,128]{2,1,0:T(8,128)(2,1)}), bf16[8,136,128]{2,1,0:T(8,128)(2,1)S(1)}, u32[]{:S(2)}, u32[]{:S(2)}) async-start(bf16[8,136,128]{2,1,0:T(8,128)(2,1)} %get-tuple-element.60), calls=%async_computation.4 | async-start | bytes 557056 | tf_op jit(solution)/shard_map/all_to_all | solution.py:631
  178.9 10.1 %copy-start.15 = (f32[64,128]{1,0:T(8,128)S(1)}, f32[64,128]{1,0:T(8,128)}, u32[]{:S(2)}) copy-start(f32[64,128]{1,0:T(8,128)} %get-tuple-element.63.refs_6_) | copy-start | bytes 98308

commit v8 on v7

--- a/solution.py
+++ b/solution.py
@@ -560,9 +560,9 @@
         out_blocks={0: acc_block},
         grid=TILES,
     )
-    low, high, acc, other = lax.optimization_barrier((low, high, acc, other))
+    low, acc, other = lax.optimization_barrier((low, acc, other))
+    beside = jnp.concatenate([lax.ppermute(low, "c", swap), lax.ppermute(high, "c", swap)], axis=0)
     rest = jnp.concatenate([low, high], axis=0)
-    beside = lax.ppermute(rest, "c", swap)
     delta, pack = call(
         delta_kernel,
         "deltas",

time: 191 us -> 191 us (level)
  waiting for transfers between devices: 47.8 us -> 41.6 us
  blocking collectives: 84.7 us -> 87.3 us
  starting transfers between devices: 30.9 us -> 33.3 us
    ppermute x1, waiting for transfers between devices: 11.6 us -> 0.01 us  [on_device(): high = lax.ppermute(own[rows_all // 2:], 'y', down)]
    ppermute x1, waiting for transfers between devices: 5.33 us -> 12.4 us  [on_device(): low = lax.ppermute(own[:rows_all // 2], 'y', up)]
    all_to_all x1, blocking collectives: 42.5 us -> 45.1 us  [on_device(): lax.all_to_all(terms.reshape(nz * ny, nx * 20, 128), ('z', 'y'), 0, 0, ti...]
    ppermute x1 -> x2, starting transfers between devices: 1.92 us -> 4.32 us  [the longest x1 2.41 us: on_device(): lax.ppermute(high, 'c', swap)]
  transfers between devices with their start and end apart: 7 -> 8, of which waited for: 5 -> 4; matrix products, arithmetic and copies ran while one was open for 0% -> 0% of each run, Pallas kernels for 8% -> 8%
where the time goes in v8:
time: 191 us; the launch traced here: 190 us
  blocking collectives  87.3 us (46%)
  waiting for transfers between devices  41.6 us (22%)
  starting transfers between devices  33.3 us (17%)
  Pallas kernels  24.9 us (13%)
    all_to_all x1, blocking collectives, on_device(): lax.all_to_all(terms.reshape(nz * ny, nx * 20, 128), ('z', 'y'), 0, 0, ti...  45.1 us
    pallas_call x13, Pallas kernels, call(): pl.pallas_call(body, name=name, out_shape=outs, grid_spec=pltpu.PrefetchS...  24.9 us
    all_to_all x1, waiting for transfers between devices, on_device(): own = lax.all_to_all(sent, SP, 0, 0, tiled=True).reshape(spans * 40, part)  23.9 us
    all_gather x1, blocking collectives, on_device(): total_grad = lax.all_gather(slice_grad, TP, axis=0)  17.2 us
    all_to_all x1, starting transfers between devices, on_device(): own = lax.all_to_all(sent, SP, 0, 0, tiled=True).reshape(spans * 40, part)  13.6 us
    all_to_all x1, blocking collectives, on_device(): crossing = lax.all_to_all(leaving, 'x', 0, 0, tiled=True)  13.5 us
    ppermute x1, waiting for transfers between devices, on_device(): low = lax.ppermute(own[:rows_all // 2], 'y', up)  12.4 us
    all_to_all x1, blocking collectives, on_device(): lax.all_to_all(summed.reshape(nx, nz * 24, 128), 'x', 0, 0, tiled=True)  9.31 us
  transfers between devices with their start and end apart: 8, of which 4 were waited for; matrix products, arithmetic and copies ran while one was open for 0% of the time, Pallas kernels for 8%

profile of v8, /device:TPU:2, one launch (start us, length us, event | category | flops | bytes accessed | tf_op | source)
XLA Modules:
  0.0 190.1 jit_solution(5325597336813793444)
XLA Ops:
  0.6 2.8 %dispatch.1.refs_5_ = bf16[32,40,512]{2,1,0:T(8,128)(2,1)} custom-call(s32[1]{0:T(128)} %bitcast.number, s32[2,128]{1,0:T(2,128)} %bitcast.54, f32[2,128]{1,0:T(2,128)} %bitcast.58, bf16[128,2048]{1,0:T(8,128)(2,1)} %refs_2_.3, bf16[128,2048]{1,0:T(8,128)(2,1)} %refs_2_.5), custom_call_target="tpu_custom_call" | custom-call | tf_op jit(solution)/shard_map/dispatch/pallas_call | solution.py:80
  3.4 13.6 %all-to-all-start = ((bf16[32,40,512]{2,1,0:T(8,128)(2,1)}), bf16[32,40,512]{2,1,0:T(8,128)(2,1)S(1)}, u32[]{:S(2)}, u32[]{:S(2)}) async-start(bf16[32,40,512]{2,1,0:T(8,128)(2,1)} %dispatch.1.refs_5_), calls=%async_computation | async-start | bytes 2621440 | tf_op jit(solution)/shard_map/all_to_all | solution.py:506
  17.0 0.1 pad_maximum_fusion
  17.2 1.9 %collective-permute-start = (bf16[2,8,128,128]{3,2,1,0:T(8,128)(2,1)S(1)}, bf16[2,8,128,128]{3,2,1,0:T(8,128)(2,1)S(1)}, u32[]{:S(2)}, u32[]{:S(2)}) collective-permute-start(bf16[2,8,128,128]{3,2,1,0:T(8,128)(2,1)S(1)} %dynamic-slice_bitcast_fusion), channel_id=1, source_target_pairs={{0,1},{1,0},{2,3},{3,2},{4,5},{5,4},{6,7},{7,6},{8,9},{9,8},{10,11... | collective-permute-start | bytes 1572872 | tf_op jit(solution)/shard_map/ppermute | solution.py:510
  19.1 2.5 %forward.1 = (bf16[128,128]{1,0:T(8,128)(2,1)}, bf16[128,128]{1,0:T(8,128)(2,1)}, f32[64,128]{1,0:T(8,128)}, f32[64,128]{1,0:T(8,128)}, bf16[8,128]{1,0:T(8,128)(2,1)}) custom-call(s32[1]{0:T(128)} %bitcast.number, bf16[64,128]{1,0:T(8,128)(2,1)} %bitcast.48, bf16[64,128]{1,0:T(8,128)(2,1)} %bitcast.51, bf16[128,128]{1,0:T(8,128)(2,1)} %bitcast.45, ...), custom_call_target="tpu_custom_call" | custom-call | tf_op jit(solution)/shard_map/forward/pallas_call | solution.py:80
  21.6 0.0 collective-permute-done.refs_3_
  21.6 0.8 copy-done.23
  22.4 3.6 %layout.1 = (bf16[2048,384]{1,0:T(8,128)(2,1)}, bf16[512,1024]{1,0:T(8,128)(2,1)}) custom-call(s32[1]{0:T(128)} %bitcast.number, bf16[1,2048,128]{2,1,0:T(8,128)(2,1)} %refs_0_.1, bf16[1,2048,128]{2,1,0:T(8,128)(2,1)} %refs_1_.2, bf16[1,128,2048]{2,1,0:T(8,128)(2,1)} %refs_2_.4, bf16[2,8,128,128]{3,2,1,0:T(8,128)(2,1)} %copy-done.23, ...), custom_call_target="tpu_custom_call" | custom-call | tf_op jit(solution)/shard_map/layout/pallas_call | solution.py:80
  26.0 23.9 %all-to-all-done = bf16[32,40,512]{2,1,0:T(8,128)(2,1)S(1)} async-done(((bf16[32,40,512]{2,1,0:T(8,128)(2,1)}), bf16[32,40,512]{2,1,0:T(8,128)(2,1)S(1)}, u32[]{:S(2)}, u32[]{:S(2)}) %all-to-all-start) | async-done | bytes 1310752 | tf_op jit(solution)/shard_map/all_to_all | solution.py:506
  49.9 2.2 %collective-permute-start.2 = (bf16[1280,512]{1,0:T(8,128)(2,1)S(1)}, bf16[1280,512]{1,0:T(8,128)(2,1)S(1)}, u32[]{:S(2)}, u32[]{:S(2)}) collective-permute-start(bf16[1280,512]{1,0:T(8,128)(2,1)S(1)} %bitcast.35), channel_id=1, source_target_pairs={{0,1},{1,0},{2,3},{3,2},{4,5},{5,4},{6,7},{7,6},{8,9},{9,8},{10,11... | collective-permute-start | bytes 3932168 | tf_op jit(solution)/shard_map/ppermute | solution.py:548
  52.1 0.1 fusion
  52.2 3.5 %collective-permute-start.1 = (bf16[640,512]{1,0:T(8,128)(2,1)S(1)}, bf16[640,512]{1,0:T(8,128)(2,1)S(1)}, u32[]{:S(2)}, u32[]{:S(2)}) collective-permute-start(bf16[640,512]{1,0:T(8,128)(2,1)S(1)} %get-tuple-element.73), channel_id=1, source_target_pairs={{0,2},{2,4},{4,6},{6,8},{8,10},{10,12},{12,14},{14,0},{1,3},{3,5},... | collective-permute-start | bytes 1966088 | tf_op jit(solution)/shard_map/ppermute | solution.py:546
  55.7 3.8 %collective-permute-start.3 = (bf16[640,512]{1,0:T(8,128)(2,1)S(1)}, bf16[640,512]{1,0:T(8,128)(2,1)S(1)}, u32[]{:S(2)}, u32[]{:S(2)}) collective-permute-start(bf16[640,512]{1,0:T(8,128)(2,1)S(1)} %get-tuple-element.72), channel_id=1, source_target_pairs={{0,14},{2,0},{4,2},{6,4},{8,6},{10,8},{12,10},{14,12},{1,15},{3,1}... | collective-permute-start | bytes 1966088 | tf_op jit(solution)/shard_map/ppermute | solution.py:547
  59.5 1.0 first.1.refs_4_
  60.6 12.4 %collective-permute-done.1 = bf16[640,512]{1,0:T(8,128)(2,1)S(1)} collective-permute-done((bf16[640,512]{1,0:T(8,128)(2,1)S(1)}, bf16[640,512]{1,0:T(8,128)(2,1)S(1)}, u32[]{:S(2)}, u32[]{:S(2)}) %collective-permute-start.1) | collective-permute-done | bytes 655392 | tf_op jit(solution)/shard_map/ppermute | solution.py:546
  73.0 0.0 collective-permute-done.2.refs_0_.refs_3_
  73.0 1.9 %collective-permute-start.4 = (bf16[640,512]{1,0:T(8,128)(2,1)S(1)}, bf16[640,512]{1,0:T(8,128)(2,1)S(1)}, u32[]{:S(2)}, u32[]{:S(2)}) collective-permute-start(bf16[640,512]{1,0:T(8,128)(2,1)S(1)} %collective-permute-done.1), channel_id=1, source_target_pairs={{0,1},{1,0},{2,3},{3,2},{4,5},{5,4},{6,7},{7,6},{8,9},{9,8},{10,11... | collective-permute-start | bytes 1966088 | tf_op jit(solution)/shard_map/ppermute | solution.py:564
  74.9 0.0 collective-permute-done.3
  74.9 2.4 %collective-permute-start.5 = (bf16[640,512]{1,0:T(8,128)(2,1)S(1)}, bf16[640,512]{1,0:T(8,128)(2,1)S(1)}, u32[]{:S(2)}, u32[]{:S(2)}) collective-permute-start(bf16[640,512]{1,0:T(8,128)(2,1)S(1)} %collective-permute-done.3), channel_id=1, source_target_pairs={{0,1},{1,0},{2,3},{3,2},{4,5},{5,4},{6,7},{7,6},{8,9},{9,8},{10,11... | collective-permute-start | bytes 1966088 | tf_op jit(solution)/shard_map/ppermute | solution.py:564
  77.4 0.0 copy-start.2
  77.4 0.0 collective-permute-done.4
  77.5 1.5 collective-permute-done.5
  79.1 2.5 %deltas.1 = (bf16[1280,384]{1,0:T(8,128)(2,1)S(1)}, bf16[640,256]{1,0:T(8,128)(2,1)S(1)}) custom-call(s32[1]{0:T(128)} %bitcast.number, bf16[1280,512]{1,0:T(8,128)(2,1)S(1)} %collective-permute-done.2.refs_0_.refs_3_, bf16[1280,512]{1,0:T(8,128)(2,1)S(1)} %constant_dynamic-update-slice_fusion.refs_1_.refs_2_, ...), custom_call_target="tpu_custom_call" | custom-call | tf_op jit(solution)/shard_map/deltas/pallas_call | solution.py:80
  81.6 2.3 %all-gather = bf16[1280,256]{1,0:T(8,128)(2,1)S(1)} all-gather(bf16[640,256]{1,0:T(8,128)(2,1)S(1)} %get-tuple-element.48), channel_id=2, replica_groups=mesh['z'=8,'x'=4,'y'=8,'c'=2] {'c'}, dimensions={0}, use_global_device_ids=true | all-gather | bytes 983040 | tf_op jit(solution)/shard_map/all_gather | solution.py:580
  83.9 0.0 copy-done.6
  83.9 0.8 partials.1
  84.7 45.1 %all_to_all.25 = bf16[64,80,128]{2,1,0:T(8,128)(2,1)S(1)} all-to-all(bf16[64,80,128]{2,1,0:T(8,128)(2,1)S(1)} %bitcast.39), channel_id=1, replica_groups=mesh['z'=8,'x'=4,'y'=8,'c'=2] {'z','y'}, dimensions={0} | all-to-all | bytes 2621440 | tf_op jit(solution)/shard_map/all_to_all | solution.py:589
  129.8 0.0 copy-start.11
  129.9 0.0 copy-start.13
  129.9 0.0 copy-start.20
  129.9 0.2 sums.1
  130.1 9.3 %all_to_all.26 = bf16[4,192,128]{2,1,0:T(8,128)(2,1)S(1)} all-to-all(bf16[4,192,128]{2,1,0:T(8,128)(2,1)S(1)} %bitcast.44), channel_id=1, replica_groups=mesh['z'=8,'x'=4,'y'=8,'c'=2] {'x'}, dimensions={0} | all-to-all | bytes 393216 | tf_op jit(solution)/shard_map/all_to_all | solution.py:593
  139.4 0.6 collect.1
  140.0 17.2 %all-gather.1 = bf16[2048,128]{1,0:T(8,128)(2,1)S(1)} all-gather(bf16[128,128]{1,0:T(8,128)(2,1)S(1)} %collect.1), channel_id=3, replica_groups=mesh['z'=8,'x'=4,'y'=8,'c'=2] {'y','c'}, dimensions={0}, use_global_device_ids=true | all-gather | bytes 557056 | tf_op jit(solution)/shard_map/all_gather | solution.py:604
  157.2 0.6 head.1
  157.8 13.5 %all_to_all.27.refs_0_ = bf16[4,584,128]{2,1,0:T(8,128)(2,1)S(1)} all-to-all(bf16[4,584,128]{2,1,0:T(8,128)(2,1)S(1)} %get-tuple-element.53), channel_id=1, replica_groups=mesh['z'=8,'x'=4,'y'=8,'c'=2] {'x'}, dimensions={0} | all-to-all | bytes 1196032 | tf_op jit(solution)/shard_map/all_to_all | solution.py:618
  171.2 1.0 group.1
  172.2 0.6 copy-done.17
  172.8 4.0 %all-to-all-start.4 = ((bf16[8,136,128]{2,1,0:T(8,128)(2,1)}), bf16[8,136,128]{2,1,0:T(8,128)(2,1)S(1)}, u32[]{:S(2)}, u32[]{:S(2)}) async-start(bf16[8,136,128]{2,1,0:T(8,128)(2,1)} %get-tuple-element.58), calls=%async_computation.4 | async-start | bytes 557056 | tf_op jit(solution)/shard_map/all_to_all | solution.py:631
  176.8 0.0 copy-start.12
  176.8 0.0 copy-start.14
  176.8 0.0 copy-start.16
  176.8 0.0 copy-start.18
  176.9 0.0 copy-start.15
  176.9 6.3 %weights.1 = (bf16[1,2048,128]{2,1,0:T(8,128)(2,1)}, bf16[1,2048,128]{2,1,0:T(8,128)(2,1)}, bf16[1,128,2048]{2,1,0:T(8,128)(2,1)}) custom-call(s32[1]{0:T(128)} %bitcast.number, bf16[1280,384]{1,0:T(8,128)(2,1)} %copy-done.7, bf16[1280,512]{1,0:T(8,128)(2,1)} %bitcast.38, bf16[1280,512]{1,0:T(8,128)(2,1)} %copy-done.2, bf16[1280,512]{1,0:T(8,128)(2,1)} %copy-done.4, ...), custom_call_target="tpu_custom_call" | custom-call | tf_op jit(solution)/shard_map/weights/pallas_call | solution.py:80
  183.2 1.7 local.1
  184.9 3.8 %all-to-all-done.4.refs_0_ = bf16[8,136,128]{2,1,0:T(8,128)(2,1)S(1)} async-done(((bf16[8,136,128]{2,1,0:T(8,128)(2,1)}), bf16[8,136,128]{2,1,0:T(8,128)(2,1)S(1)}, u32[]{:S(2)}, u32[]{:S(2)}) %all-to-all-start.4) | async-done | bytes 278560 | tf_op jit(solution)/shard_map/all_to_all | solution.py:631
  188.7 1.4 last.1
  (41 shorter events, 0.3 us)
Async XLA Ops:
  3.4 13.6 %copy-start.21 = (bf16[1,2048,128]{2,1,0:T(8,128)(2,1)S(1)}, bf16[1,2048,128]{2,1,0:T(8,128)(2,1)}, u32[]{:S(2)}) copy-start(bf16[1,2048,128]{2,1,0:T(8,128)(2,1)} %refs_0_.1) | copy-start | bytes 1572868
  3.4 13.6 %copy-start.22 = (bf16[1,2048,128]{2,1,0:T(8,128)(2,1)S(1)}, bf16[1,2048,128]{2,1,0:T(8,128)(2,1)}, u32[]{:S(2)}) copy-start(bf16[1,2048,128]{2,1,0:T(8,128)(2,1)} %refs_1_.2) | copy-start | bytes 1572868
  3.4 46.5 %all-to-all-start = ((bf16[32,40,512]{2,1,0:T(8,128)(2,1)}), bf16[32,40,512]{2,1,0:T(8,128)(2,1)S(1)}, u32[]{:S(2)}, u32[]{:S(2)}) async-start(bf16[32,40,512]{2,1,0:T(8,128)(2,1)} %dispatch.1.refs_5_), calls=%async_computation | async-start | bytes 2621440 | tf_op jit(solution)/shard_map/all_to_all | solution.py:506
  17.2 4.4 %collective-permute-start = (bf16[2,8,128,128]{3,2,1,0:T(8,128)(2,1)S(1)}, bf16[2,8,128,128]{3,2,1,0:T(8,128)(2,1)S(1)}, u32[]{:S(2)}, u32[]{:S(2)}) collective-permute-start(bf16[2,8,128,128]{3,2,1,0:T(8,128)(2,1)S(1)} %dynamic-slice_bitcast_fusion), channel_id=1, source_target_pairs={{0,1},{1,0},{2,3},{3,2},{4,5},{5,4},{6,7},{7,6},{8,9},{9,8},{10,11... | collective-permute-start | bytes 1572872 | tf_op jit(solution)/shard_map/ppermute | solution.py:510
  21.6 0.8 copy-start.23
  49.9 9.6 %copy-start = (bf16[32,40,512]{2,1,0:T(8,128)(2,1)}, bf16[32,40,512]{2,1,0:T(8,128)(2,1)S(1)}, u32[]{:S(2)}) copy-start(bf16[32,40,512]{2,1,0:T(8,128)(2,1)S(1)} %all-to-all-done) | copy-start | bytes 3932164
  49.9 9.6 %copy-start.3 = (bf16[2048,384]{1,0:T(8,128)(2,1)S(1)}, bf16[2048,384]{1,0:T(8,128)(2,1)}, u32[]{:S(2)}) copy-start(bf16[2048,384]{1,0:T(8,128)(2,1)} %get-tuple-element.43.refs_1_.refs_3_) | copy-start | bytes 4718596
  49.9 23.0 %collective-permute-start.2 = (bf16[1280,512]{1,0:T(8,128)(2,1)S(1)}, bf16[1280,512]{1,0:T(8,128)(2,1)S(1)}, u32[]{:S(2)}, u32[]{:S(2)}) collective-permute-start(bf16[1280,512]{1,0:T(8,128)(2,1)S(1)} %bitcast.35), channel_id=1, source_target_pairs={{0,1},{1,0},{2,3},{3,2},{4,5},{5,4},{6,7},{7,6},{8,9},{9,8},{10,11... | collective-permute-start | bytes 3932168 | tf_op jit(solution)/shard_map/ppermute | solution.py:548
  52.2 20.8 %collective-permute-start.1 = (bf16[640,512]{1,0:T(8,128)(2,1)S(1)}, bf16[640,512]{1,0:T(8,128)(2,1)S(1)}, u32[]{:S(2)}, u32[]{:S(2)}) collective-permute-start(bf16[640,512]{1,0:T(8,128)(2,1)S(1)} %get-tuple-element.73), channel_id=1, source_target_pairs={{0,2},{2,4},{4,6},{6,8},{8,10},{10,12},{12,14},{14,0},{1,3},{3,5},... | collective-permute-start | bytes 1966088 | tf_op jit(solution)/shard_map/ppermute | solution.py:546
  55.7 19.2 %collective-permute-start.3 = (bf16[640,512]{1,0:T(8,128)(2,1)S(1)}, bf16[640,512]{1,0:T(8,128)(2,1)S(1)}, u32[]{:S(2)}, u32[]{:S(2)}) collective-permute-start(bf16[640,512]{1,0:T(8,128)(2,1)S(1)} %get-tuple-element.72), channel_id=1, source_target_pairs={{0,14},{2,0},{4,2},{6,4},{8,6},{10,8},{12,10},{14,12},{1,15},{3,1}... | collective-permute-start | bytes 1966088 | tf_op jit(solution)/shard_map/ppermute | solution.py:547
  73.0 6.1 %copy-start.4 = (bf16[1280,512]{1,0:T(8,128)(2,1)}, bf16[1280,512]{1,0:T(8,128)(2,1)S(1)}, u32[]{:S(2)}) copy-start(bf16[1280,512]{1,0:T(8,128)(2,1)S(1)} %collective-permute-done.2.refs_0_.refs_3_) | copy-start | bytes 3932164
  73.0 4.5 %collective-permute-start.4 = (bf16[640,512]{1,0:T(8,128)(2,1)S(1)}, bf16[640,512]{1,0:T(8,128)(2,1)S(1)}, u32[]{:S(2)}, u32[]{:S(2)}) collective-permute-start(bf16[640,512]{1,0:T(8,128)(2,1)S(1)} %collective-permute-done.1), channel_id=1, source_target_pairs={{0,1},{1,0},{2,3},{3,2},{4,5},{5,4},{6,7},{7,6},{8,9},{9,8},{10,11... | collective-permute-start | bytes 1966088 | tf_op jit(solution)/shard_map/ppermute | solution.py:564
  74.9 4.1 %collective-permute-start.5 = (bf16[640,512]{1,0:T(8,128)(2,1)S(1)}, bf16[640,512]{1,0:T(8,128)(2,1)S(1)}, u32[]{:S(2)}, u32[]{:S(2)}) collective-permute-start(bf16[640,512]{1,0:T(8,128)(2,1)S(1)} %collective-permute-done.3), channel_id=1, source_target_pairs={{0,1},{1,0},{2,3},{3,2},{4,5},{5,4},{6,7},{7,6},{8,9},{9,8},{10,11... | collective-permute-start | bytes 1966088 | tf_op jit(solution)/shard_map/ppermute | solution.py:564
  77.4 1.7 copy-start.2
  79.1 2.5 %copy-start.1 = (bf16[1280,512]{1,0:T(8,128)(2,1)}, bf16[1280,512]{1,0:T(8,128)(2,1)S(1)}, u32[]{:S(2)}) copy-start(bf16[1280,512]{1,0:T(8,128)(2,1)S(1)} %constant_dynamic-update-slice_fusion.2.refs_2_.refs_4_) | copy-start | bytes 3932164
  79.1 4.8 %copy-start.6 = (bf16[512,1024]{1,0:T(8,128)(2,1)S(1)}, bf16[512,1024]{1,0:T(8,128)(2,1)}, u32[]{:S(2)}) copy-start(bf16[512,1024]{1,0:T(8,128)(2,1)} %get-tuple-element.49.refs_1_) | copy-start | bytes 3145732
  81.6 3.1 %copy-start.7 = (bf16[1280,384]{1,0:T(8,128)(2,1)}, bf16[1280,384]{1,0:T(8,128)(2,1)S(1)}, u32[]{:S(2)}) copy-start(bf16[1280,384]{1,0:T(8,128)(2,1)S(1)} %get-tuple-element.47.refs_0_) | copy-start | bytes 2949124
  129.8 9.5 %copy-start.5 = (bf16[128,2048]{1,0:T(8,128)(2,1)S(1)}, bf16[128,2048]{1,0:T(8,128)(2,1)}, u32[]{:S(2)}) copy-start(bf16[128,2048]{1,0:T(8,128)(2,1)} %refs_2_.5) | copy-start | bytes 1572868
  129.8 9.5 %copy-start.19 = (s32[128,2]{0,1:T(2,128)S(1)}, s32[128,2]{0,1:T(2,128)}, u32[]{:S(2)}) copy-start(s32[128,2]{0,1:T(2,128)} %param.15) | copy-start | bytes 3076
  129.8 27.3 %copy-start.8 = (bf16[2048,128]{1,0:T(8,128)(2,1)S(1)}, bf16[2048,128]{1,0:T(8,128)(2,1)}, u32[]{:S(2)}) copy-start(bf16[2048,128]{1,0:T(8,128)(2,1)} %refs_1_.3) | copy-start | bytes 1572868
  129.8 27.3 %copy-start.9 = (f32[64,128]{1,0:T(8,128)S(1)}, f32[64,128]{1,0:T(8,128)}, u32[]{:S(2)}) copy-start(f32[64,128]{1,0:T(8,128)} %get-tuple-element.50.refs_3_.refs_4_.refs_5_) | copy-start | bytes 98308
  129.8 27.3 %copy-start.11 = (bf16[128,1,64]{0,2,1:T(8,128)(2,1)S(1)}, bf16[128,1,64]{0,2,1:T(8,128)(2,1)}, u32[]{:S(2)}) copy-start(bf16[128,1,64]{0,2,1:T(8,128)(2,1)} %param.21) | copy-start | bytes 49156
  129.9 27.3 %copy-start.13 = (bf16[128,128]{1,0:T(8,128)(2,1)S(1)}, bf16[128,128]{1,0:T(8,128)(2,1)}, u32[]{:S(2)}) copy-start(bf16[128,128]{1,0:T(8,128)(2,1)} %get-tuple-element.51.refs_4_) | copy-start | bytes 98308
  129.9 27.3 %copy-start.20 = (bf16[8,128]{1,0:T(8,128)(2,1)S(1)}, bf16[8,128]{1,0:T(8,128)(2,1)}, u32[]{:S(2)}) copy-start(bf16[8,128]{1,0:T(8,128)(2,1)} %get-tuple-element.52.refs_5_) | copy-start | bytes 6148
  172.2 0.6 copy-start.17
  172.8 15.9 %all-to-all-start.4 = ((bf16[8,136,128]{2,1,0:T(8,128)(2,1)}), bf16[8,136,128]{2,1,0:T(8,128)(2,1)S(1)}, u32[]{:S(2)}, u32[]{:S(2)}) async-start(bf16[8,136,128]{2,1,0:T(8,128)(2,1)} %get-tuple-element.58), calls=%async_computation.4 | async-start | bytes 557056 | tf_op jit(solution)/shard_map/all_to_all | solution.py:631
  176.8 6.4 %copy-start.10 = (bf16[128,1,128]{2,0,1:T(8,128)(2,1)S(1)}, bf16[128,1,128]{2,0,1:T(8,128)(2,1)}, u32[]{:S(2)}) copy-start(bf16[128,1,128]{2,0,1:T(8,128)(2,1)} %param.23) | copy-start | bytes 98308
  176.8 6.3 %copy-start.12 = (bf16[128,1,64]{0,2,1:T(8,128)(2,1)S(1)}, bf16[128,1,64]{0,2,1:T(8,128)(2,1)}, u32[]{:S(2)}) copy-start(bf16[128,1,64]{0,2,1:T(8,128)(2,1)} %param.22) | copy-start | bytes 49156
  176.8 6.3 %copy-start.14 = (f32[1,1,64,128]{3,2,1,0:T(8,128)S(1)}, f32[1,1,64,128]{3,2,1,0:T(8,128)}, u32[]{:S(2)}) copy-start(f32[1,1,64,128]{3,2,1,0:T(8,128)} %refs_5_.1) | copy-start | bytes 98308
  176.8 6.3 %copy-start.16 = (bf16[128,128]{1,0:T(8,128)(2,1)S(1)}, bf16[128,128]{1,0:T(8,128)(2,1)}, u32[]{:S(2)}) copy-start(bf16[128,128]{1,0:T(8,128)(2,1)} %get-tuple-element.63.refs_6_) | copy-start | bytes 98308
  176.8 6.3 %copy-start.18 = (f32[8,128]{1,0:T(8,128)S(1)}, f32[8,128]{1,0:T(8,128)}, u32[]{:S(2)}) copy-start(f32[8,128]{1,0:T(8,128)} %copy-done.17) | copy-start | bytes 12292
  176.9 11.8 %copy-start.15 = (f32[64,128]{1,0:T(8,128)S(1)}, f32[64,128]{1,0:T(8,128)}, u32[]{:S(2)}) copy-start(f32[64,128]{1,0:T(8,128)} %get-tuple-element.61.refs_6_) | copy-start | bytes 98308
